TPU v7x, 128 devices: a whole 4x4x4 slice. The times are simulated.
128 devices in a mesh: sp: 32 (over z, y, core), tp: 4 (over x).
Axes of the slice: x: 4, y: 4, z: 4, core: 2. Of those that a mesh axis runs over, the one named last changes fastest.
Arguments:
- d_out: bfloat16 [16384, 2048], P('sp'), may hold values from -6 to 6
- route_expert: int32 [16384, 2], P('sp'), may hold values from 0 to 31, all different within a row; in each aligned block of 512 rows (0 to 511, 512 to 1023, ...) at most 36 rows name the same one
- route_weight: float32 [16384, 2], P('sp'), may hold values from 0.2 to 1
- expert_inputs: bfloat16 [32, 1152, 2048], P('sp'), may hold values from -6 to 6
- w_gate: bfloat16 [32, 2048, 2816], P('sp', None, 'tp'), may hold values from -0.125 to 0.125
- w_up: bfloat16 [32, 2048, 2816], P('sp', None, 'tp'), may hold values from -0.125 to 0.125
- w_down: bfloat16 [32, 2816, 2048], P('sp', 'tp'), may hold values from -0.109375 to 0.109375
- w_out: bfloat16 [2048, 1024], P(None, 'tp'), may hold values from -0.1875 to 0.1875
- queries: bfloat16 [16384, 4, 128], P('sp', 'tp'), may hold values from -6 to 6
- keys: bfloat16 [16384, 4, 128], P('sp', 'tp'), may hold values from -1.25 to 1.25
- values: bfloat16 [16384, 4, 256], P('sp', 'tp'), may hold values from -6 to 6
- log_decay: float32 [16384, 4, 128], P('sp', 'tp'), may hold values from -1 to 0
Outputs:
- grad_gate: bfloat16 [32, 2048, 2816], P('sp', None, 'tp')
- grad_up: bfloat16 [32, 2048, 2816], P('sp', None, 'tp')
- grad_down: bfloat16 [32, 2816, 2048], P('sp', 'tp')
- grad_proj: float32 [2048, 1024], P('sp', 'tp')
- grad_queries: bfloat16 [16384, 4, 128], P('sp', 'tp')
- grad_keys: bfloat16 [16384, 4, 128], P('sp', 'tp')
- grad_values: bfloat16 [16384, 4, 256], P('sp', 'tp')
- grad_log_decay: float32 [16384, 4, 128], P('sp', 'tp')
Inputs may be any that keep to these rules, and one draw needn't show every extreme that they name: `route_expert`: the two experts of a token differ. Among the rows of one device no expert is named more than 36 times, and in every draw some device names some expert exactly 36 times.
All inputs are finite; a program needn't handle non-finite values.
Results may differ from a plain program's by a relative error of at most 0.02.
Values may be sent and summed in bfloat16 or wider, within the bound.
No kernel may reach another device: no remote copies, remote signals or barrier semaphores. Data moves between devices by JAX's collectives and lax.ppermute only.
A program may use at most 128 MiB of HBM per device.

v0:
```python
import jax
import jax.numpy as jnp
from jax import lax
from jax.experimental import pallas as pl
from jax.experimental.pallas import tpu as pltpu
from jax.sharding import Mesh
from jax.sharding import PartitionSpec as P

BLK = 64
PAD = 8
SP = ("sp_0", "sp_1", "sp_2")
INNER = ("sp_1", "sp_2")
OUTER = "sp_0"
F32 = jnp.float32
BF16 = jnp.bfloat16

NN = (((1,), (0,)), ((), ()))
NT = (((1,), (1,)), ((), ()))
TN = (((0,), (0,)), ((), ()))


def dot(a, b, dims):
    return lax.dot_general(a, b, dims, preferred_element_type=F32)


def halves(x):
    high = x.astype(BF16)
    return high, (x - high.astype(F32)).astype(BF16)


def thirds(x):
    high = x.astype(BF16)
    rest = x - high.astype(F32)
    middle = rest.astype(BF16)
    return high, middle, (rest - middle.astype(F32)).astype(BF16)


def dot_parts(a, b, dims):
    out = dot(a[0], b[0], dims)
    if len(a) > 1:
        out = out + dot(a[1], b[0], dims)
    if len(b) > 1:
        out = out + dot(a[0], b[1], dims)
    return out


def dot_exact(mask, x, dims):
    high, middle, low = thirds(x)
    return dot(mask, high, dims) + (dot(mask, middle, dims) + dot(mask, low, dims))


def grid_of(shape, dim):
    return lax.broadcasted_iota(jnp.int32, shape, dim)


def vmem_call(kernel, outs, **options):
    return pl.pallas_call(
        kernel,
        out_shape=outs,
        compiler_params=pltpu.CompilerParams(vmem_limit_bytes=56 * 1024 * 1024),
        **options,
    )


def route_body(d_out, experts_t, weight, outbox, pick):
    tokens = d_out.shape[0]
    slots, experts = outbox.shape[0], lax.axis_size(SP)
    stride = slots // experts
    first, second = experts_t[0:1, :], experts_t[1:2, :]
    ids = grid_of((experts, tokens), 0)
    is_first, is_second = ids == first, ids == second
    chosen = jnp.where(is_first | is_second, 1.0, 0.0).astype(BF16)
    earlier = jnp.where(
        grid_of((tokens, tokens), 0) < grid_of((tokens, tokens), 1), 1.0, 0.0
    ).astype(BF16)
    before = dot(chosen, earlier, NN)
    rank_a = jnp.sum(jnp.where(is_first, before, 0.0), axis=0, keepdims=True).astype(jnp.int32)
    rank_b = jnp.sum(jnp.where(is_second, before, 0.0), axis=0, keepdims=True).astype(jnp.int32)
    slot_a = first * stride + rank_a
    slot_b = second * stride + rank_b
    weights_a = jnp.concatenate(thirds(weight[:, 0:1]), axis=1)
    weights_b = jnp.concatenate(thirds(weight[:, 1:2]), axis=1)
    rows = d_out[...]
    step = 256
    for start in range(0, slots, step):
        slot = grid_of((step, tokens), 0) + start
        one_a = jnp.where(slot == slot_a, 1.0, 0.0).astype(BF16)
        one_b = jnp.where(slot == slot_b, 1.0, 0.0).astype(BF16)
        both = one_a + one_b
        factor = jnp.sum(dot(one_a, weights_a, NN) + dot(one_b, weights_b, NN), axis=1, keepdims=True)
        pick[start : start + step, :] = both
        outbox[start : start + step, :] = (dot(both, rows, NN) * factor).astype(BF16)


def expert_body(routed, active, slope, down_w, gate_w, up_w, d_gate, d_up, partial):
    d_hidden = dot(routed[...], down_w[...], NT)
    to_gate = (d_hidden * slope[...]).astype(BF16)
    to_up = (d_hidden * active[...]).astype(BF16)
    d_gate[...] = to_gate
    d_up[...] = to_up
    parts, _, width = partial.shape
    for part in range(parts):
        cols = slice(part * width, (part + 1) * width)
        term = dot(to_gate, gate_w[cols, :], NT) + dot(to_up, up_w[cols, :], NT)
        partial[part] = term.astype(BF16)


def expert_cotangents(routed, active, slope, down_w, gate_w, up_w, parts):
    rows, width = routed.shape
    units = down_w.shape[0]
    step = 256
    quarter = width // parts
    by_row = lambda i: (i, 0)
    whole = lambda i: (0, 0)
    return pl.pallas_call(
        expert_body,
        grid=(rows // step,),
        in_specs=[
            pl.BlockSpec((step, width), by_row),
            pl.BlockSpec((step, units), by_row),
            pl.BlockSpec((step, units), by_row),
            pl.BlockSpec((units, width), whole),
            pl.BlockSpec((width, units), whole),
            pl.BlockSpec((width, units), whole),
        ],
        out_specs=[
            pl.BlockSpec((step, units), by_row),
            pl.BlockSpec((step, units), by_row),
            pl.BlockSpec((parts, step, quarter), lambda i: (0, i, 0)),
        ],
        out_shape=[
            jax.ShapeDtypeStruct((rows, units), BF16),
            jax.ShapeDtypeStruct((rows, units), BF16),
            jax.ShapeDtypeStruct((parts, rows, quarter), BF16),
        ],
        compiler_params=pltpu.CompilerParams(vmem_limit_bytes=56 * 1024 * 1024),
    )(routed, active, slope, down_w, gate_w, up_w)


def triangle(reverse):
    row, col = grid_of((BLK, BLK), 0), grid_of((BLK, BLK), 1)
    return jnp.where((row <= col) if reverse else (row >= col), 1.0, 0.0).astype(BF16)


def local_state_body(keys, values, decay, cumulative, ends, gain, produced, ending):
    blocks = gain.shape[0]
    lower = triangle(False)
    for c in range(blocks):
        rows = slice(c * BLK, (c + 1) * BLK)
        cum = dot_exact(lower, decay[rows, :], NN)
        cumulative[rows, :] = cum
        end = cum[BLK - 1 : BLK, :]
        ends[c : c + 1, :] = end
        faded = keys[rows, :].astype(F32) * jnp.exp(end - cum)
        gain[c] = dot_parts((values[rows, :],), halves(faded), TN)
    state = gain[0]
    total = ends[0:1, :]
    for c in range(1, blocks):
        state = state * jnp.exp(ends[c : c + 1, :]) + gain[c]
        total = total + ends[c : c + 1, :]
    produced[...] = state.astype(BF16)
    ending[...] = total


def local_states(keys, values, decay):
    tokens, channels = keys.shape
    width = values.shape[1]
    blocks = tokens // BLK
    return vmem_call(
        local_state_body,
        [
            jax.ShapeDtypeStruct((tokens, channels), F32),
            jax.ShapeDtypeStruct((blocks, channels), F32),
            jax.ShapeDtypeStruct((blocks, width, channels), F32),
            jax.ShapeDtypeStruct((width, channels), BF16),
            jax.ShapeDtypeStruct((1, channels), F32),
        ],
    )(keys, values, decay)


def forward_body(queries, keys, values, cumulative, ends, gain, start, mixed, states, scores):
    blocks = gain.shape[0]
    scale = queries.shape[1] ** (-0.5)
    causal = grid_of((BLK, BLK), 0) >= grid_of((BLK, BLK), 1)
    state = start[...]
    for c in range(blocks):
        rows = slice(c * BLK, (c + 1) * BLK)
        cum = cumulative[rows, :]
        middle = cum[BLK // 2 - 1 : BLK // 2, :]
        query = queries[rows, :].astype(F32) * scale
        near_q = halves(query * jnp.exp(cum - middle))
        near_k = halves(keys[rows, :].astype(F32) * jnp.exp(middle - cum))
        score = jnp.where(causal, dot_parts(near_q, near_k, NT), 0.0)
        scores[rows, :] = score
        states[c] = state
        out = dot_parts(halves(query * jnp.exp(cum)), halves(state), NT)
        out = out + dot_parts(halves(score), (values[rows, :],), NN)
        mixed[rows, :] = out.astype(BF16)
        state = state * jnp.exp(ends[c : c + 1, :]) + gain[c]
    states[blocks] = state


def forward(queries, keys, values, cumulative, ends, gain, start):
    tokens, channels = keys.shape
    width = values.shape[1]
    blocks = tokens // BLK
    return vmem_call(
        forward_body,
        [
            jax.ShapeDtypeStruct((tokens, width), BF16),
            jax.ShapeDtypeStruct((blocks + 1, width, channels), F32),
            jax.ShapeDtypeStruct((tokens, BLK), F32),
        ],
    )(queries, keys, values, cumulative, ends, gain, start)


def cotangent_body(tiles, w_out, queries, cumulative, ends, d_mixed, back, own):
    blocks = back.shape[0]
    scale = queries.shape[1] ** (-0.5)
    quarter = tiles.shape[2]
    total = dot(tiles[0], w_out[0:quarter, :], NN)
    for part in range(1, tiles.shape[0]):
        total = total + dot(tiles[part], w_out[part * quarter : (part + 1) * quarter, :], NN)
    d_mixed[...] = total
    for c in range(blocks):
        rows = slice(c * BLK, (c + 1) * BLK)
        query = queries[rows, :].astype(F32) * (scale * jnp.exp(cumulative[rows, :]))
        back[c] = dot_parts(halves(d_mixed[rows, :]), halves(query), TN)
    state = back[blocks - 1]
    for c in reversed(range(blocks - 1)):
        state = state * jnp.exp(ends[c : c + 1, :]) + back[c]
    own[...] = state.astype(BF16)


def cotangents(tiles, w_out, queries, cumulative, ends):
    tokens, channels = queries.shape
    width = w_out.shape[1]
    blocks = tokens // BLK
    return vmem_call(
        cotangent_body,
        [
            jax.ShapeDtypeStruct((tokens, width), F32),
            jax.ShapeDtypeStruct((blocks, width, channels), F32),
            jax.ShapeDtypeStruct((width, channels), BF16),
        ],
    )(tiles, w_out, queries, cumulative, ends)


def inside_body(queries, keys, values, cumulative, scores, d_mixed, to_q, to_k, to_v):
    blocks = queries.shape[0] // BLK
    scale = queries.shape[1] ** (-0.5)
    causal = grid_of((BLK, BLK), 0) >= grid_of((BLK, BLK), 1)
    for c in range(blocks):
        rows = slice(c * BLK, (c + 1) * BLK)
        cum = cumulative[rows, :]
        middle = cum[BLK // 2 - 1 : BLK // 2, :]
        rising, falling = jnp.exp(cum - middle), jnp.exp(middle - cum)
        near_q = halves(queries[rows, :].astype(F32) * scale * rising)
        near_k = halves(keys[rows, :].astype(F32) * falling)
        incoming = halves(d_mixed[rows, :])
        d_score = jnp.where(causal, dot_parts(incoming, (values[rows, :],), NT), 0.0)
        d_score = halves(d_score)
        to_q[rows, :] = rising * dot_parts(d_score, near_k, NN)
        to_k[rows, :] = falling * dot_parts(d_score, near_q, TN)
        to_v[rows, :] = dot_parts(halves(scores[rows, :]), incoming, TN)


def inside_blocks(queries, keys, values, cumulative, scores, d_mixed):
    tokens, channels = queries.shape
    return vmem_call(
        inside_body,
        [
            jax.ShapeDtypeStruct((tokens, channels), F32),
            jax.ShapeDtypeStruct((tokens, channels), F32),
            jax.ShapeDtypeStruct(values.shape, F32),
        ],
    )(queries, keys, values, cumulative, scores, d_mixed)


def backward_body(
    queries, keys, values, cumulative, ends, d_mixed, states, back, to_q, to_k, to_v, later,
    grad_q, grad_k, grad_v, grad_g,
):
    blocks = back.shape[0]
    scale = queries.shape[1] ** (-0.5)
    upper = triangle(True)
    after = later[...]
    carry = jnp.sum(after * states[blocks], axis=0, keepdims=True)
    for c in reversed(range(blocks)):
        rows = slice(c * BLK, (c + 1) * BLK)
        cum = cumulative[rows, :]
        end = ends[c : c + 1, :]
        fading = jnp.exp(end - cum)
        key = keys[rows, :].astype(F32)
        after_parts = halves(after)
        d_query = jnp.exp(cum) * dot_parts(halves(d_mixed[rows, :]), halves(states[c]), NN)
        d_query = (d_query + to_q[rows, :]) * scale
        d_key = fading * dot_parts((values[rows, :],), after_parts, NN) + to_k[rows, :]
        d_value = dot_parts(halves(key * fading), after_parts, NT) + to_v[rows, :]
        grad_q[rows, :] = d_query.astype(BF16)
        grad_k[rows, :] = d_key.astype(BF16)
        grad_v[rows, :] = d_value.astype(BF16)
        change = queries[rows, :].astype(F32) * d_query - key * d_key
        summed = dot_exact(upper, change, NN) + carry
        grad_g[rows, :] = summed
        carry = summed[0:1, :]
        after = after * jnp.exp(end) + back[c]


def backward(queries, keys, values, cumulative, ends, d_mixed, states, back, inside, later):
    return vmem_call(
        backward_body,
        [
            jax.ShapeDtypeStruct(queries.shape, BF16),
            jax.ShapeDtypeStruct(keys.shape, BF16),
            jax.ShapeDtypeStruct(values.shape, BF16),
            jax.ShapeDtypeStruct(queries.shape, F32),
        ],
    )(queries, keys, values, cumulative, ends, d_mixed, states, back, *inside, later)


def sent_to_all(x, axis):
    count = lax.axis_size(axis)
    return lax.all_to_all(jnp.broadcast_to(x[None], (count, *x.shape)), axis, 0, 0, tiled=True)


def masked_sums(logs, mask):
    return jnp.sum(jnp.where(mask[:, :, None], logs[None], 0.0), axis=1)


def between(logs, index, reverse):
    count = logs.shape[0]
    row, col = grid_of((count, count), 0), grid_of((count, count), 1)
    if reverse:
        inner, outer = (col > index) & (col < row), col < row
        passed = jnp.arange(count) > index
        own = jnp.arange(count) > index
    else:
        inner, outer = (col < index) & (col > row), col > row
        passed = jnp.arange(count) < index
        own = jnp.arange(count) < index
    near = jnp.where(passed[:, None], jnp.exp(masked_sums(logs, inner)), 0.0)
    whole = jnp.exp(masked_sums(logs, outer))
    own = jnp.exp(jnp.sum(jnp.where(own[:, None], logs, 0.0), axis=0))
    return near, whole, own


def state_weights(endings, reverse):
    inner, outer = lax.axis_size(INNER), lax.axis_size(OUTER)
    grouped = endings.reshape(outer, inner, -1)
    place = lax.axis_index(OUTER)
    mine = jnp.sum(
        jnp.where((jnp.arange(outer) == place)[:, None, None], grouped, 0.0), axis=0
    )
    near, whole, own = between(mine, lax.axis_index(INNER), reverse)
    far, _, _ = between(jnp.sum(grouped, axis=1), place, reverse)
    return near, whole, own, far


def state_from_others(part, weights):
    near, whole, own, far = weights
    pieces = sent_to_all(part, INNER).astype(F32)
    group = jnp.sum(pieces * whole[:, None, :], axis=0).astype(BF16)
    inside = jnp.sum(pieces * near[:, None, :], axis=0)
    groups = sent_to_all(group, OUTER).astype(F32)
    return inside + own[None] * jnp.sum(groups * far[:, None, :], axis=0)


def local(
    d_out,
    route_expert,
    route_weight,
    expert_inputs,
    w_gate,
    w_up,
    w_down,
    w_out,
    queries,
    keys,
    values,
    log_decay,
):
    tok_rows, model_width = d_out.shape
    experts = lax.axis_size(SP)
    tp = lax.axis_size("tp")
    capacity = expert_inputs.shape[1] // experts
    stride = -(-capacity // PAD) * PAD
    slots = experts * stride
    quarter = model_width // tp

    outbox, pick = vmem_call(
        route_body,
        [
            jax.ShapeDtypeStruct((slots, model_width), BF16),
            jax.ShapeDtypeStruct((slots, tok_rows), BF16),
        ],
    )(d_out, route_expert.T, route_weight)
    routed = lax.all_to_all(
        outbox.reshape(experts, stride, model_width), SP, split_axis=0, concat_axis=0, tiled=True
    ).reshape(slots, model_width)

    query, key, value, decay = queries[:, 0], keys[:, 0], values[:, 0], log_decay[:, 0]
    cumulative, ends, gain, produced, ending = local_states(key, value, decay)
    endings = lax.all_gather(ending[0], SP)
    start = state_from_others(produced, state_weights(endings, False))
    mixed, states, scores = forward(query, key, value, cumulative, ends, gain, start)

    rows_in = expert_inputs[0].reshape(experts, capacity, model_width)
    rows_in = jnp.pad(rows_in, ((0, 0), (0, stride - capacity), (0, 0))).reshape(
        slots, model_width
    )
    gate_w, up_w, down_w = w_gate[0], w_up[0], w_down[0]
    gate_pre = dot(rows_in, gate_w, NN)
    up_pre = dot(rows_in, up_w, NN)
    sigmoid_gate = jax.nn.sigmoid(gate_pre)
    active = gate_pre * sigmoid_gate
    hidden = (active * up_pre).astype(BF16)
    slope = up_pre * sigmoid_gate * (1.0 + gate_pre * (1.0 - sigmoid_gate))
    d_gate, d_up, partial = expert_cotangents(routed, active, slope, down_w, gate_w, up_w, tp)
    arrived = lax.all_to_all(partial, "tp", 0, 0, tiled=True)
    grad_gate = dot(rows_in, d_gate, TN).astype(BF16)
    grad_up = dot(rows_in, d_up, TN).astype(BF16)
    grad_down = dot(hidden, routed, TN).astype(BF16)
    summed = jnp.sum(arrived.astype(F32), axis=0).astype(BF16)
    returned = lax.all_to_all(
        summed.reshape(experts, stride, quarter), SP, split_axis=0, concat_axis=0, tiled=True
    ).reshape(slots, quarter)

    own_cols = lax.dynamic_slice_in_dim(d_out, lax.axis_index("tp") * quarter, quarter, 1)
    mix_cols = (own_cols.astype(F32) + dot(pick, returned, TN)).astype(BF16)
    tiles = sent_to_all(mix_cols, "tp")

    d_mixed, back, own_term = cotangents(tiles, w_out, query, cumulative, ends)
    later = state_from_others(own_term, state_weights(endings, True))
    inside = inside_blocks(query, key, value, cumulative, scores, d_mixed)
    grad_q, grad_k, grad_v, grad_g = backward(
        query, key, value, cumulative, ends, d_mixed, states, back, inside, later
    )

    proj = jnp.einsum("ptc,te->pce", tiles, mixed, preferred_element_type=F32).astype(BF16)
    proj = proj.reshape(experts, model_width // experts, -1)
    grad_proj = jnp.sum(lax.all_to_all(proj, SP, 0, 0, tiled=True).astype(F32), axis=0)
    return (
        grad_gate[None],
        grad_up[None],
        grad_down[None],
        grad_proj,
        grad_q[:, None],
        grad_k[:, None],
        grad_v[:, None],
        grad_g[:, None],
    )


def solution(mesh):
    finer = Mesh(mesh.devices.reshape(4, 4, 2, mesh.shape["tp"]), ("sp_0", "sp_1", "sp_2", "tp"))
    return jax.shard_map(
        local,
        mesh=finer,
        in_specs=(
            P(SP, None),
            P(SP, None),
            P(SP, None),
            P(SP, None, None),
            P(SP, None, "tp"),
            P(SP, None, "tp"),
            P(SP, "tp", None),
            P(None, "tp"),
            P(SP, "tp", None),
            P(SP, "tp", None),
            P(SP, "tp", None),
            P(SP, "tp", None),
        ),
        out_specs=(
            P(SP, None, "tp"),
            P(SP, None, "tp"),
            P(SP, "tp", None),
            P(SP, "tp"),
            P(SP, "tp", None),
            P(SP, "tp", None),
            P(SP, "tp", None),
            P(SP, "tp", None),
        ),
        check_vma=False,
    )
```

profile of v0, /device:TPU:1, one launch (start us, length us, event | category | flops | bytes accessed | tf_op | source)
XLA Modules:
  0.0 326.6 jit_solution(1413887047546210998)
XLA Ops:
  2.2 8.1 %shard_map.179 = (bf16[1280,2048]{1,0:T(8,128)(2,1)}, bf16[1280,512]{1,0:T(8,128)(2,1)}) custom-call(bf16[512,2048]{1,0:T(8,128)(2,1)} %d_out.1, s32[2,512]{1,0:T(2,128)} %bitcast.77, f32[512,2]{1,0:T(8,128)} %copy.60.weight), custom_call_target="tpu_custom_call" | custom-call | tf_op jit(solution)/shard_map/pallas_call | solution.py:391
  10.3 10.3 %all-to-all-start = ((bf16[32,40,2048]{2,1,0:T(8,128)(2,1)}), bf16[32,40,2048]{2,1,0:T(8,128)(2,1)}, u32[]{:S(2)}, u32[]{:S(2)}) async-start(bf16[32,40,2048]{2,1,0:T(8,128)(2,1)} %bitcast.56), calls=%async_computation | async-start | bytes 10485760 | tf_op jit(solution)/shard_map/all_to_all | solution.py:398
  20.6 4.8 %copy.61 = bf16[1,2048,704]{2,1,0:T(8,128)(2,1)} copy(bf16[1,2048,704]{1,2,0:T(8,128)(2,1)} %param.16) | data formatting | bytes 5767168 | tf_op args[4]
  28.3 7.2 %reshape_squeeze.3 = bf16[32,36,2048]{2,1,0:T(8,128)(2,1)} reshape(bf16[1,1152,2048]{2,1,0:T(8,128)(2,1)} %param.15) | data formatting | bytes 9437184 | tf_op jit(solution)/shard_map/reshape;squeeze | solution.py:408
  35.5 3.3 %pad.4 = bf16[32,40,2048]{2,1,0:T(8,128)(2,1)S(1)} pad(bf16[32,36,2048]{2,1,0:T(8,128)(2,1)} %reshape_squeeze.3, bf16[]{:T(256)} %constant.9.clone.1), padding=0_0x0_4x0_0 | pad | bytes 9961474 | tf_op jit(solution)/shard_map/jit(_pad)/pad | solution.py:409
  38.8 4.3 %fusion.4 = f32[1280,704]{1,0:T(8,128)S(1)} fusion(bf16[1280,2048]{1,0:T(8,128)(2,1)S(1)} %bitcast.57, bf16[1,2048,704]{1,2,0:T(8,128)(2,1)S(1)} %copy-done.3), kind=kOutput, calls=%fused_computation.10 | convolution fusion | flops 3690987520 | bytes 11730944 | tf_op jit(solution)/shard_map/dot_general | solution.py:23
  44.9 7.7 %add_multiply_fusion = (f32[1280,704]{1,0:T(8,128)}, f32[1280,704]{1,0:T(8,128)}, f32[1280,704]{1,0:T(8,128)}) fusion(f32[1280,704]{1,0:T(8,128)S(1)} %fusion.4, bf16[1280,2048]{1,0:T(8,128)(2,1)S(1)} %bitcast.58, bf16[1,2048,704]{1,2,0:T(8,128)(2,1)S(1)} %copy-done.4), kind=kOutput, calls=%fused_computation.1 | convolution fusion | flops 3699097600 | bytes 22544384 | tf_op jit(solution)/shard_map/dot_general | solution.py:23
  52.7 29.7 %all-to-all-done = bf16[32,40,2048]{2,1,0:T(8,128)(2,1)} async-done(((bf16[32,40,2048]{2,1,0:T(8,128)(2,1)}), bf16[32,40,2048]{2,1,0:T(8,128)(2,1)}, u32[]{:S(2)}, u32[]{:S(2)}) %all-to-all-start) | async-done | bytes 5242912 | tf_op jit(solution)/shard_map/all_to_all | solution.py:398
  82.3 19.1 %shard_map.180 = (bf16[1280,704]{1,0:T(8,128)(2,1)}, bf16[1280,704]{1,0:T(8,128)(2,1)}, bf16[4,1280,512]{2,1,0:T(8,128)(2,1)}) custom-call(bf16[1280,2048]{1,0:T(8,128)(2,1)} %bitcast.3.routed, f32[1280,704]{1,0:T(8,128)} %get-tuple-element.109.active, f32[1280,704]{1,0:T(8,128)} %get-tuple-element.108.slope, bf16[704,2048]{1,0:T(8,128)(2,1)} %bitcast.65, ...), custom_call_target="tpu_custom_call" | custom-call | tf_op jit(solution)/shard_map/pallas_call | solution.py:115
  101.5 5.0 %all-to-all-start.1 = ((bf16[4,1280,512]{2,1,0:T(8,128)(2,1)}), bf16[4,1280,512]{2,1,0:T(8,128)(2,1)}, u32[]{:S(2)}, u32[]{:S(2)}) async-start(bf16[4,1280,512]{2,1,0:T(8,128)(2,1)} %get-tuple-element.35), calls=%async_computation.1 | async-start | bytes 10485760 | tf_op jit(solution)/shard_map/all_to_all | solution.py:420
  106.5 3.2 shard_map.181
  109.7 52.7 %all-to-all-done.1 = bf16[4,1280,512]{2,1,0:T(8,128)(2,1)} async-done(((bf16[4,1280,512]{2,1,0:T(8,128)(2,1)}), bf16[4,1280,512]{2,1,0:T(8,128)(2,1)}, u32[]{:S(2)}, u32[]{:S(2)}) %all-to-all-start.1) | async-done | bytes 5242912 | tf_op jit(solution)/shard_map/all_to_all | solution.py:420
  164.2 9.2 %all-to-all-start.4 = ((bf16[8,256,128]{2,1,0:T(8,128)(2,1)}), bf16[8,256,128]{2,1,0:T(8,128)(2,1)S(1)}, u32[]{:S(2)}, u32[]{:S(2)}) async-start(bf16[8,256,128]{2,1,0:T(8,128)(2,1)} %broadcast_in_dim.219), calls=%async_computation.4 | async-start | bytes 1048576 | tf_op jit(solution)/shard_map/all_to_all | solution.py:324
  173.5 23.2 %all-gather = f32[32,1,128]{2,1,0:T(1,128)S(1)} all-gather(f32[1,1,128]{2,1,0:T(1,128)} %bitcast.78), channel_id=1, replica_groups=mesh['sp_0'=4,'sp_1'=4,'sp_2'=2,'tp'=4] {'sp_0','sp_1','sp_2'}, dimensions={0}, use_global_device_ids=true | all-gather | bytes 16896 | tf_op jit(solution)/shard_map/all_gather | solution.py:404
  196.8 4.7 %reduce_sum.173 = bf16[1280,512]{1,0:T(8,128)(2,1)} reduce(bf16[4,1280,512]{2,1,0:T(8,128)(2,1)} %all-to-all-done.1, bf16[]{:T(256)} %constant.9.clone.1), dimensions={0}, to_apply=%region_0.1 | reduce | flops 1966080 | bytes 6553602 | tf_op jit(solution)/shard_map/reduce_sum | solution.py:424
  201.6 4.9 %all-to-all-start.2 = ((bf16[32,40,512]{2,1,0:T(8,128)(2,1)}), bf16[32,40,512]{2,1,0:T(8,128)(2,1)S(1)}, u32[]{:S(2)}, u32[]{:S(2)}) async-start(bf16[32,40,512]{2,1,0:T(8,128)(2,1)} %bitcast.10), calls=%async_computation.2 | async-start | bytes 2621440 | tf_op jit(solution)/shard_map/all_to_all | solution.py:425
  207.1 18.7 %all-to-all-done.2 = bf16[32,40,512]{2,1,0:T(8,128)(2,1)S(1)} async-done(((bf16[32,40,512]{2,1,0:T(8,128)(2,1)}), bf16[32,40,512]{2,1,0:T(8,128)(2,1)S(1)}, u32[]{:S(2)}, u32[]{:S(2)}) %all-to-all-start.2) | async-done | bytes 1310752 | tf_op jit(solution)/shard_map/all_to_all | solution.py:425
  226.6 3.4 %all-to-all-start.5 = ((bf16[4,256,128]{2,1,0:T(8,128)(2,1)}), bf16[4,256,128]{2,1,0:T(8,128)(2,1)S(1)}, u32[]{:S(2)}, u32[]{:S(2)}) async-start(bf16[4,256,128]{2,1,0:T(8,128)(2,1)} %broadcast_in_dim.228), calls=%async_computation.5 | async-start | bytes 524288 | tf_op jit(solution)/shard_map/all_to_all | solution.py:324
  232.3 3.2 all-to-all-done.5
  237.0 3.6 %all-to-all-start.3 = ((bf16[4,512,512]{2,1,0:T(8,128)(2,1)}), bf16[4,512,512]{2,1,0:T(8,128)(2,1)S(1)}, u32[]{:S(2)}, u32[]{:S(2)}) async-start(bf16[4,512,512]{2,1,0:T(8,128)(2,1)} %broadcast_in_dim.218), calls=%async_computation.3 | async-start | bytes 4194304 | tf_op jit(solution)/shard_map/all_to_all | solution.py:324
  241.3 3.4 %shard_map.182 = (bf16[512,256]{1,0:T(8,128)(2,1)}, f32[9,256,128]{2,1,0:T(8,128)}, f32[512,64]{1,0:T(8,128)}) custom-call(bf16[512,128]{1,0:T(8,128)(2,1)} %bitcast.66, bf16[512,128]{1,0:T(8,128)(2,1)} %bitcast.71, bf16[512,256]{1,0:T(8,128)(2,1)} %bitcast.62, f32[512,128]{1,0:T(8,128)} %get-tuple-element.36.cumulative, f32[8,128]{1,0:T(8,128)} %get-tuple-element.37.ends, ...), custom_call_target="tpu_custom_call" | custom-call | tf_op jit(solution)/shard_map/pallas_call | solution.py:207
  244.7 10.6 %fusion.3 = bf16[1,704,2048]{2,1,0:T(8,128)(2,1)} fusion(bf16[1280,2048]{1,0:T(8,128)(2,1)} %bitcast.3.routed, f32[1280,704]{1,0:T(8,128)} %copy-done.6, f32[1280,704]{1,0:T(8,128)} %get-tuple-element.112), kind=kOutput, calls=%fused_computation.9 | convolution fusion | flops 3697836032 | bytes 15335424 | tf_op jit(solution)/shard_map/dot_general | solution.py:23
  255.2 9.1 %all-to-all-done.3.tiles = bf16[4,512,512]{2,1,0:T(8,128)(2,1)S(1)} async-done(((bf16[4,512,512]{2,1,0:T(8,128)(2,1)}), bf16[4,512,512]{2,1,0:T(8,128)(2,1)S(1)}, u32[]{:S(2)}, u32[]{:S(2)}) %all-to-all-start.3) | async-done | bytes 2097184 | tf_op jit(solution)/shard_map/all_to_all | solution.py:324
  265.7 5.0 %shard_map.183 = (f32[512,256]{1,0:T(8,128)}, f32[8,256,128]{2,1,0:T(8,128)}, bf16[256,128]{1,0:T(8,128)(2,1)}) custom-call(bf16[4,512,512]{2,1,0:T(8,128)(2,1)} %copy-done, bf16[2048,256]{1,0:T(8,128)(2,1)} %w_out.1, bf16[512,128]{1,0:T(8,128)(2,1)} %bitcast.67, f32[512,128]{1,0:T(8,128)} %get-tuple-element.36.cumulative, f32[8,128]{1,0:T(8,128)} %get-tuple-element.37.ends), custom_call_target="tpu_custom_call" | custom-call | tf_op jit(solution)/shard_map/pallas_call | solution.py:239
  272.4 8.1 %all-to-all-start.7 = ((bf16[8,256,128]{2,1,0:T(8,128)(2,1)}), bf16[8,256,128]{2,1,0:T(8,128)(2,1)S(1)}, u32[]{:S(2)}, u32[]{:S(2)}) async-start(bf16[8,256,128]{2,1,0:T(8,128)(2,1)} %broadcast_in_dim.234), calls=%async_computation.7 | async-start | bytes 1048576 | tf_op jit(solution)/shard_map/all_to_all | solution.py:324
  280.5 8.8 %fusion.1 = bf16[1,2048,704]{1,2,0:T(8,128)(2,1)} fusion(bf16[1280,2048]{1,0:T(8,128)(2,1)} %bitcast.59, bf16[1280,704]{1,0:T(8,128)(2,1)} %get-tuple-element.32), kind=kOutput, calls=%fused_computation.7 | convolution fusion | flops 3692429312 | bytes 9928704 | tf_op jit(solution)/shard_map/dot_general | solution.py:23
  290.6 3.4 %all-to-all-start.8 = ((bf16[4,256,128]{2,1,0:T(8,128)(2,1)}), bf16[4,256,128]{2,1,0:T(8,128)(2,1)S(1)}, u32[]{:S(2)}, u32[]{:S(2)}) async-start(bf16[4,256,128]{2,1,0:T(8,128)(2,1)} %broadcast_in_dim.238), calls=%async_computation.8 | async-start | bytes 524288 | tf_op jit(solution)/shard_map/all_to_all | solution.py:324
  295.8 3.8 %all-to-all-done.8 = bf16[4,256,128]{2,1,0:T(8,128)(2,1)S(1)} async-done(((bf16[4,256,128]{2,1,0:T(8,128)(2,1)}), bf16[4,256,128]{2,1,0:T(8,128)(2,1)S(1)}, u32[]{:S(2)}, u32[]{:S(2)}) %all-to-all-start.8) | async-done | bytes 262176 | tf_op jit(solution)/shard_map/all_to_all | solution.py:324
  299.6 7.1 %all-to-all-start.6 = ((bf16[32,64,256]{2,1,0:T(8,128)(2,1)}), bf16[32,64,256]{2,1,0:T(8,128)(2,1)S(1)}, u32[]{:S(2)}, u32[]{:S(2)}) async-start(bf16[32,64,256]{2,1,0:T(8,128)(2,1)} %bitcast.19), calls=%async_computation.6 | async-start | bytes 2097152 | tf_op jit(solution)/shard_map/all_to_all | solution.py:442
  306.7 8.6 %fusion.2 = bf16[1,2048,704]{1,2,0:T(8,128)(2,1)} fusion(bf16[1280,2048]{1,0:T(8,128)(2,1)} %bitcast.60, bf16[1280,704]{1,0:T(8,128)(2,1)} %get-tuple-element.33), kind=kOutput, calls=%fused_computation.8 | convolution fusion | flops 3692429312 | bytes 9928704 | tf_op jit(solution)/shard_map/dot_general | solution.py:23
  315.3 4.4 %shard_map.184 = (f32[512,128]{1,0:T(8,128)}, f32[512,128]{1,0:T(8,128)}, f32[512,256]{1,0:T(8,128)}) custom-call(bf16[512,128]{1,0:T(8,128)(2,1)} %bitcast.68, bf16[512,128]{1,0:T(8,128)(2,1)} %bitcast.72, bf16[512,256]{1,0:T(8,128)(2,1)} %bitcast.63, f32[512,128]{1,0:T(8,128)} %get-tuple-element.36.cumulative, f32[512,64]{1,0:T(8,128)} %get-tuple-element.45.scores, ...), custom_call_target="tpu_custom_call" | custom-call | tf_op jit(solution)/shard_map/pallas_call | solution.py:270
  320.4 5.1 %shard_map.185 = (bf16[512,128]{1,0:T(8,128)(2,1)}, bf16[512,128]{1,0:T(8,128)(2,1)}, bf16[512,256]{1,0:T(8,128)(2,1)}, f32[512,128]{1,0:T(8,128)}) custom-call(bf16[512,128]{1,0:T(8,128)(2,1)} %bitcast.69, bf16[512,128]{1,0:T(8,128)(2,1)} %bitcast.73, bf16[512,256]{1,0:T(8,128)(2,1)} %bitcast.64, f32[512,128]{1,0:T(8,128)} %get-tuple-element.36.cumulative, ...), custom_call_target="tpu_custom_call" | custom-call | tf_op jit(solution)/shard_map/pallas_call | solution.py:311
  (51 shorter events, 21.7 us)
Async XLA Ops:
  10.3 72.1 %all-to-all-start = ((bf16[32,40,2048]{2,1,0:T(8,128)(2,1)}), bf16[32,40,2048]{2,1,0:T(8,128)(2,1)}, u32[]{:S(2)}, u32[]{:S(2)}) async-start(bf16[32,40,2048]{2,1,0:T(8,128)(2,1)} %bitcast.56), calls=%async_computation | async-start | bytes 10485760 | tf_op jit(solution)/shard_map/all_to_all | solution.py:398
  20.6 4.8 %copy-start.3 = (bf16[1,2048,704]{1,2,0:T(8,128)(2,1)S(1)}, bf16[1,2048,704]{1,2,0:T(8,128)(2,1)}, u32[]{:S(2)}) copy-start(bf16[1,2048,704]{1,2,0:T(8,128)(2,1)} %param.17) | copy-start | bytes 8650756
  38.7 4.3 %copy-start.2 = (bf16[32,40,2048]{2,1,0:T(8,128)(2,1)}, bf16[32,40,2048]{2,1,0:T(8,128)(2,1)S(1)}, u32[]{:S(2)}) copy-start(bf16[32,40,2048]{2,1,0:T(8,128)(2,1)S(1)} %pad.4) | copy-start | bytes 15728644
  38.8 6.2 %copy-start.4 = (bf16[1,2048,704]{1,2,0:T(8,128)(2,1)S(1)}, bf16[1,2048,704]{1,2,0:T(8,128)(2,1)}, u32[]{:S(2)}) copy-start(bf16[1,2048,704]{1,2,0:T(8,128)(2,1)} %param.16) | copy-start | bytes 8650756
  43.1 1.9 copy-start.6
  101.5 61.0 %all-to-all-start.1 = ((bf16[4,1280,512]{2,1,0:T(8,128)(2,1)}), bf16[4,1280,512]{2,1,0:T(8,128)(2,1)}, u32[]{:S(2)}, u32[]{:S(2)}) async-start(bf16[4,1280,512]{2,1,0:T(8,128)(2,1)} %get-tuple-element.35), calls=%async_computation.1 | async-start | bytes 10485760 | tf_op jit(solution)/shard_map/all_to_all | solution.py:420
  164.2 37.4 %all-to-all-start.4 = ((bf16[8,256,128]{2,1,0:T(8,128)(2,1)}), bf16[8,256,128]{2,1,0:T(8,128)(2,1)S(1)}, u32[]{:S(2)}, u32[]{:S(2)}) async-start(bf16[8,256,128]{2,1,0:T(8,128)(2,1)} %broadcast_in_dim.219), calls=%async_computation.4 | async-start | bytes 1048576 | tf_op jit(solution)/shard_map/all_to_all | solution.py:324
  201.6 24.2 %all-to-all-start.2 = ((bf16[32,40,512]{2,1,0:T(8,128)(2,1)}), bf16[32,40,512]{2,1,0:T(8,128)(2,1)S(1)}, u32[]{:S(2)}, u32[]{:S(2)}) async-start(bf16[32,40,512]{2,1,0:T(8,128)(2,1)} %bitcast.10), calls=%async_computation.2 | async-start | bytes 2621440 | tf_op jit(solution)/shard_map/all_to_all | solution.py:425
  226.6 8.9 %all-to-all-start.5 = ((bf16[4,256,128]{2,1,0:T(8,128)(2,1)}), bf16[4,256,128]{2,1,0:T(8,128)(2,1)S(1)}, u32[]{:S(2)}, u32[]{:S(2)}) async-start(bf16[4,256,128]{2,1,0:T(8,128)(2,1)} %broadcast_in_dim.228), calls=%async_computation.5 | async-start | bytes 524288 | tf_op jit(solution)/shard_map/all_to_all | solution.py:324
  237.0 27.4 %all-to-all-start.3 = ((bf16[4,512,512]{2,1,0:T(8,128)(2,1)}), bf16[4,512,512]{2,1,0:T(8,128)(2,1)S(1)}, u32[]{:S(2)}, u32[]{:S(2)}) async-start(bf16[4,512,512]{2,1,0:T(8,128)(2,1)} %broadcast_in_dim.218), calls=%async_computation.3 | async-start | bytes 4194304 | tf_op jit(solution)/shard_map/all_to_all | solution.py:324
  264.3 1.3 copy-start
  272.4 17.4 %all-to-all-start.7 = ((bf16[8,256,128]{2,1,0:T(8,128)(2,1)}), bf16[8,256,128]{2,1,0:T(8,128)(2,1)S(1)}, u32[]{:S(2)}, u32[]{:S(2)}) async-start(bf16[8,256,128]{2,1,0:T(8,128)(2,1)} %broadcast_in_dim.234), calls=%async_computation.7 | async-start | bytes 1048576 | tf_op jit(solution)/shard_map/all_to_all | solution.py:324
  280.4 13.6 %copy-start.1 = (bf16[4,512,512]{2,1,0:T(8,128)(2,1)S(1)}, bf16[4,512,512]{2,1,0:T(8,128)(2,1)}, u32[]{:S(2)}) copy-start(bf16[4,512,512]{2,1,0:T(8,128)(2,1)} %copy-done) | copy-start | bytes 6291460
  280.4 13.6 %copy-start.5 = (bf16[512,256]{1,0:T(8,128)(2,1)S(1)}, bf16[512,256]{1,0:T(8,128)(2,1)}, u32[]{:S(2)}) copy-start(bf16[512,256]{1,0:T(8,128)(2,1)} %get-tuple-element.41) | copy-start | bytes 786436
  290.6 8.9 %all-to-all-start.8 = ((bf16[4,256,128]{2,1,0:T(8,128)(2,1)}), bf16[4,256,128]{2,1,0:T(8,128)(2,1)S(1)}, u32[]{:S(2)}, u32[]{:S(2)}) async-start(bf16[4,256,128]{2,1,0:T(8,128)(2,1)} %broadcast_in_dim.238), calls=%async_computation.8 | async-start | bytes 524288 | tf_op jit(solution)/shard_map/all_to_all | solution.py:324
  299.6 26.0 %all-to-all-start.6 = ((bf16[32,64,256]{2,1,0:T(8,128)(2,1)}), bf16[32,64,256]{2,1,0:T(8,128)(2,1)S(1)}, u32[]{:S(2)}, u32[]{:S(2)}) async-start(bf16[32,64,256]{2,1,0:T(8,128)(2,1)} %bitcast.19), calls=%async_computation.6 | async-start | bytes 2097152 | tf_op jit(solution)/shard_map/all_to_all | solution.py:442
where the time goes:
time: 331 us; the launch traced here: 327 us
  waiting for transfers between devices  118 us (36%)
  starting transfers between devices  55.2 us (17%)
  Pallas kernels  48.2 us (15%)
  matrix products  44 us (13%)
  local copies, waits for them, and re-layouts  29.3 us (9%)
  blocking collectives  23.2 us (7%)
  other arithmetic  7.88 us (2%)
    all_to_all x1, waiting for transfers between devices, local(): arrived = lax.all_to_all(partial, 'tp', 0, 0, tiled=True)  52.7 us
    dot_general x6, matrix products, dot(): return lax.dot_general(a, b, dims, preferred_element_type=F32)  42.3 us
    all_to_all x1, waiting for transfers between devices, local(): lax.all_to_all(outbox.reshape(experts, stride, model_width), SP, split_ax...  29.7 us
    all_to_all x5, starting transfers between devices, sent_to_all(): lax.all_to_all(jnp.broadcast_to(x[None], (count, *x.shape)), axis, 0, 0,...  27.7 us
    all_gather x1, blocking collectives, local(): endings = lax.all_gather(ending[0], SP)  23.2 us
    pallas_call x1, Pallas kernels, expert_cotangents(): pl.pallas_call(expert_body, grid=(rows // step,), in_specs=[pl.BlockSpec(...  19.1 us
    all_to_all x1, waiting for transfers between devices, local(): lax.all_to_all(summed.reshape(experts, stride, quarter), SP, split_axis=0...  18.7 us
    all_to_all x5, waiting for transfers between devices, sent_to_all(): lax.all_to_all(jnp.broadcast_to(x[None], (count, *x.shape)), axis, 0, 0,...  16.6 us
  transfers between devices with their start and end apart: 9, of which 7 were waited for; matrix products, arithmetic and copies ran while one was open for 21% of the time, Pallas kernels for 5%

commit v1 on v0

--- a/solution.py
+++ b/solution.py
@@ -1,3 +1,5 @@
+import functools
+
 import jax
 import jax.numpy as jnp
 from jax import lax
@@ -6,11 +8,10 @@
 from jax.sharding import Mesh
 from jax.sharding import PartitionSpec as P
 
+
 BLK = 64
 PAD = 8
 SP = ("sp_0", "sp_1", "sp_2")
-INNER = ("sp_1", "sp_2")
-OUTER = "sp_0"
 F32 = jnp.float32
 BF16 = jnp.bfloat16
 
@@ -62,24 +63,10 @@
     )
 
 
-def route_body(d_out, experts_t, weight, outbox, pick):
-    tokens = d_out.shape[0]
-    slots, experts = outbox.shape[0], lax.axis_size(SP)
-    stride = slots // experts
-    first, second = experts_t[0:1, :], experts_t[1:2, :]
-    ids = grid_of((experts, tokens), 0)
-    is_first, is_second = ids == first, ids == second
-    chosen = jnp.where(is_first | is_second, 1.0, 0.0).astype(BF16)
-    earlier = jnp.where(
-        grid_of((tokens, tokens), 0) < grid_of((tokens, tokens), 1), 1.0, 0.0
-    ).astype(BF16)
-    before = dot(chosen, earlier, NN)
-    rank_a = jnp.sum(jnp.where(is_first, before, 0.0), axis=0, keepdims=True).astype(jnp.int32)
-    rank_b = jnp.sum(jnp.where(is_second, before, 0.0), axis=0, keepdims=True).astype(jnp.int32)
-    slot_a = first * stride + rank_a
-    slot_b = second * stride + rank_b
-    weights_a = jnp.concatenate(thirds(weight[:, 0:1]), axis=1)
-    weights_b = jnp.concatenate(thirds(weight[:, 1:2]), axis=1)
+def fill_outbox(d_out, weight, slot_a, slot_b, outbox, pick):
+    slots, tokens = pick.shape
+    weights_a = jnp.concatenate(thirds(weight[0:1, :]), axis=0)
+    weights_b = jnp.concatenate(thirds(weight[1:2, :]), axis=0)
     rows = d_out[...]
     step = 256
     for start in range(0, slots, step):
@@ -87,54 +74,134 @@
         one_a = jnp.where(slot == slot_a, 1.0, 0.0).astype(BF16)
         one_b = jnp.where(slot == slot_b, 1.0, 0.0).astype(BF16)
         both = one_a + one_b
-        factor = jnp.sum(dot(one_a, weights_a, NN) + dot(one_b, weights_b, NN), axis=1, keepdims=True)
+        factor = dot(one_a, weights_a, NT) + dot(one_b, weights_b, NT)
+        factor = jnp.sum(factor, axis=1, keepdims=True)
         pick[start : start + step, :] = both
         outbox[start : start + step, :] = (dot(both, rows, NN) * factor).astype(BF16)
 
 
-def expert_body(routed, active, slope, down_w, gate_w, up_w, d_gate, d_up, partial):
+def slots_of(chosen, ranks, least, most, stride):
+    inside = (ranks >= least) & (ranks < most)
+    return jnp.where(inside, chosen * stride + ranks - least, -1)
+
+
+def route_body(d_out, chosen, weight, outbox, pick, ranks, *, experts, most, stride):
+    tokens = d_out.shape[0]
+    first, second = chosen[0:1, :], chosen[1:2, :]
+    ids = grid_of((experts, tokens), 0)
+    is_first, is_second = ids == first, ids == second
+    named = jnp.where(is_first | is_second, 1.0, 0.0).astype(BF16)
+    earlier = jnp.where(
+        grid_of((tokens, tokens), 0) < grid_of((tokens, tokens), 1), 1.0, 0.0
+    ).astype(BF16)
+    before = dot(named, earlier, NN)
+    rank_a = jnp.sum(jnp.where(is_first, before, 0.0), axis=0, keepdims=True).astype(jnp.int32)
+    rank_b = jnp.sum(jnp.where(is_second, before, 0.0), axis=0, keepdims=True).astype(jnp.int32)
+    ranks[0:1, :] = rank_a
+    ranks[1:2, :] = rank_b
+    slot_a = slots_of(first, rank_a, 0, most, stride)
+    slot_b = slots_of(second, rank_b, 0, most, stride)
+    fill_outbox(d_out, weight, slot_a, slot_b, outbox, pick)
+
+
+def refill_body(d_out, chosen, weight, ranks, outbox, pick, *, least, most, stride):
+    slot_a = slots_of(chosen[0:1, :], ranks[0:1, :], least, most, stride)
+    slot_b = slots_of(chosen[1:2, :], ranks[1:2, :], least, most, stride)
+    fill_outbox(d_out, weight, slot_a, slot_b, outbox, pick)
+
+
+def expert_body(place, routed, active, slope, down_w, gate_w, up_w, *refs):
+    d_gate, d_up, keep_a, send_a, keep_b, send_b = refs[-6:]
     d_hidden = dot(routed[...], down_w[...], NT)
     to_gate = (d_hidden * slope[...]).astype(BF16)
     to_up = (d_hidden * active[...]).astype(BF16)
     d_gate[...] = to_gate
     d_up[...] = to_up
-    parts, _, width = partial.shape
-    for part in range(parts):
-        cols = slice(part * width, (part + 1) * width)
-        term = dot(to_gate, gate_w[cols, :], NT) + dot(to_up, up_w[cols, :], NT)
-        partial[part] = term.astype(BF16)
-
-
-def expert_cotangents(routed, active, slope, down_w, gate_w, up_w, parts):
+    half = keep_a.shape[2]
+    homes = (
+        ((keep_a, 0), (keep_b, 0)),
+        ((send_a, 0), (keep_b, 1)),
+        ((send_a, 1), (send_b, 1)),
+        ((keep_a, 1), (send_b, 0)),
+    )
+    for k, (home_a, home_b) in enumerate(homes):
+        start = pl.multiple_of((place[0] ^ k) * (2 * half), 2 * half)
+        cols = pl.ds(start, 2 * half)
+        term = dot(to_gate, gate_w[:, cols], NN) + dot(to_up, up_w[:, cols], NN)
+        term = term.astype(BF16)
+        home_a[0][home_a[1]] = term[:, :half]
+        home_b[0][home_b[1]] = term[:, half:]
+
+
+def expert_cotangents(place, routed, active, slope, down_w, gate_w, up_w, first_row, earlier):
     rows, width = routed.shape
     units = down_w.shape[0]
     step = 256
-    quarter = width // parts
-    by_row = lambda i: (i, 0)
-    whole = lambda i: (0, 0)
+    half = width // 8
+    skipped = first_row // step
+    by_row = lambda i, *_: (i, 0)
+    later_row = lambda i, *_: (i + skipped, 0)
+    whole = lambda i, *_: (0, 0)
+    in_specs = [
+        pl.BlockSpec((step, width), by_row),
+        pl.BlockSpec((step, units), later_row),
+        pl.BlockSpec((step, units), later_row),
+        pl.BlockSpec((units, width), whole),
+        pl.BlockSpec((units, width), whole),
+        pl.BlockSpec((units, width), whole),
+    ]
+    in_specs += [pl.BlockSpec(memory_space=pl.ANY)] * len(earlier)
+    pair = pl.BlockSpec((2, step, half), lambda i, *_: (0, i, 0))
     return pl.pallas_call(
         expert_body,
-        grid=(rows // step,),
-        in_specs=[
-            pl.BlockSpec((step, width), by_row),
-            pl.BlockSpec((step, units), by_row),
-            pl.BlockSpec((step, units), by_row),
-            pl.BlockSpec((units, width), whole),
-            pl.BlockSpec((width, units), whole),
-            pl.BlockSpec((width, units), whole),
-        ],
-        out_specs=[
-            pl.BlockSpec((step, units), by_row),
-            pl.BlockSpec((step, units), by_row),
-            pl.BlockSpec((parts, step, quarter), lambda i: (0, i, 0)),
-        ],
-        out_shape=[
-            jax.ShapeDtypeStruct((rows, units), BF16),
-            jax.ShapeDtypeStruct((rows, units), BF16),
-            jax.ShapeDtypeStruct((parts, rows, quarter), BF16),
-        ],
+        grid_spec=pltpu.PrefetchScalarGridSpec(
+            num_scalar_prefetch=1,
+            grid=(rows // step,),
+            in_specs=in_specs,
+            out_specs=[pl.BlockSpec((step, units), later_row)] * 2 + [pair] * 4,
+        ),
+        out_shape=[jax.ShapeDtypeStruct(active.shape, BF16)] * 2
+        + [jax.ShapeDtypeStruct((2, rows, half), BF16)] * 4,
+        input_output_aliases={7 + i: i for i in range(len(earlier))},
         compiler_params=pltpu.CompilerParams(vmem_limit_bytes=56 * 1024 * 1024),
-    )(routed, active, slope, down_w, gate_w, up_w)
+    )(place, routed, active, slope, down_w, gate_w, up_w, *earlier)
+
+
+def swapped(x, flip):
+    count = lax.axis_size("tp")
+    return lax.ppermute(x, "tp", [(i, i ^ flip) for i in range(count)])
+
+
+def plus(*terms):
+    total = terms[0].astype(F32)
+    for term in terms[1:]:
+        total = total + term.astype(F32)
+    return total.astype(BF16)
+
+
+def summed_over_tp(keep_a, send_a, keep_b, send_b):
+    got_a = swapped(send_a, 1)
+    got_b = swapped(send_b, 3)
+    last_a, last_b = plus(keep_a[1], got_a[1]), plus(keep_b[1], got_b[1])
+    last_a = swapped(last_a, 3)
+    last_b = swapped(last_b, 1)
+    return jnp.concatenate(
+        [plus(keep_a[0], got_a[0], last_a), plus(keep_b[0], got_b[0], last_b)], axis=1
+    )
+
+
+def shifted(x, axis, by):
+    count = lax.axis_size(axis)
+    return lax.ppermute(x, axis, [(i, (i + by) % count) for i in range(count)])
+
+
+def gathered_ring(x):
+    half = x.shape[0] // 2
+    below, above = shifted(x, "tp", 1), shifted(x, "tp", -1)
+    across = jnp.concatenate(
+        [shifted(below[:half], "tp", 1), shifted(above[half:], "tp", -1)], axis=0
+    )
+    return x, below, above, across
 
 
 def triangle(reverse):
@@ -142,7 +209,7 @@
     return jnp.where((row <= col) if reverse else (row >= col), 1.0, 0.0).astype(BF16)
 
 
-def local_state_body(keys, values, decay, cumulative, ends, gain, produced, ending):
+def local_state_body(keys, values, decay, cumulative, ends, gain, produced):
     blocks = gain.shape[0]
     lower = triangle(False)
     for c in range(blocks):
@@ -158,8 +225,10 @@
     for c in range(1, blocks):
         state = state * jnp.exp(ends[c : c + 1, :]) + gain[c]
         total = total + ends[c : c + 1, :]
-    produced[...] = state.astype(BF16)
-    ending[...] = total
+    width = state.shape[0]
+    produced[0:width, :] = state
+    spare = produced.shape[0] - width
+    produced[width:, :] = jnp.where(grid_of((spare, total.shape[1]), 0) == 0, total, 0.0)
 
 
 def local_states(keys, values, decay):
@@ -172,8 +241,7 @@
             jax.ShapeDtypeStruct((tokens, channels), F32),
             jax.ShapeDtypeStruct((blocks, channels), F32),
             jax.ShapeDtypeStruct((blocks, width, channels), F32),
-            jax.ShapeDtypeStruct((width, channels), BF16),
-            jax.ShapeDtypeStruct((1, channels), F32),
+            jax.ShapeDtypeStruct((width + 8, channels), F32),
         ],
     )(keys, values, decay)
 
@@ -214,13 +282,15 @@
     )(queries, keys, values, cumulative, ends, gain, start)
 
 
-def cotangent_body(tiles, w_out, queries, cumulative, ends, d_mixed, back, own):
+def cotangent_body(place, a, b, c, d, w_out, queries, cumulative, ends, d_mixed, back, own):
     blocks = back.shape[0]
     scale = queries.shape[1] ** (-0.5)
-    quarter = tiles.shape[2]
-    total = dot(tiles[0], w_out[0:quarter, :], NN)
-    for part in range(1, tiles.shape[0]):
-        total = total + dot(tiles[part], w_out[part * quarter : (part + 1) * quarter, :], NN)
+    quarter = a.shape[1]
+    total = None
+    for tile, offset in ((a, 0), (b, 3), (c, 1), (d, 2)):
+        start = pl.multiple_of(((place[0] + offset) & 3) * quarter, quarter)
+        term = dot(tile[...], w_out[pl.ds(start, quarter), :], NN)
+        total = term if total is None else total + term
     d_mixed[...] = total
     for c in range(blocks):
         rows = slice(c * BLK, (c + 1) * BLK)
@@ -232,7 +302,11 @@
     own[...] = state.astype(BF16)
 
 
-def cotangents(tiles, w_out, queries, cumulative, ends):
+SMEM = pl.BlockSpec(memory_space=pltpu.SMEM)
+VMEM = pl.BlockSpec(memory_space=pltpu.VMEM)
+
+
+def cotangents(place, tiles, w_out, queries, cumulative, ends):
     tokens, channels = queries.shape
     width = w_out.shape[1]
     blocks = tokens // BLK
@@ -243,7 +317,23 @@
             jax.ShapeDtypeStruct((blocks, width, channels), F32),
             jax.ShapeDtypeStruct((width, channels), BF16),
         ],
-    )(tiles, w_out, queries, cumulative, ends)
+        in_specs=[SMEM] + [VMEM] * 8,
+    )(place, *tiles, w_out, queries, cumulative, ends)
+
+
+def projection_body(place, a, b, c, d, mixed, out):
+    quarter = a.shape[1]
+    for tile, offset in ((a, 0), (b, 3), (c, 1), (d, 2)):
+        start = pl.multiple_of(((place[0] + offset) & 3) * quarter, quarter)
+        out[pl.ds(start, quarter), :] = dot(tile[...], mixed[...], TN).astype(BF16)
+
+
+def projection(place, tiles, mixed):
+    return vmem_call(
+        projection_body,
+        jax.ShapeDtypeStruct((4 * tiles[0].shape[1], mixed.shape[1]), BF16),
+        in_specs=[SMEM] + [VMEM] * 5,
+    )(place, *tiles, mixed)
 
 
 def inside_body(queries, keys, values, cumulative, scores, d_mixed, to_q, to_k, to_v):
@@ -319,51 +409,65 @@
     )(queries, keys, values, cumulative, ends, d_mixed, states, back, *inside, later)
 
 
-def sent_to_all(x, axis):
-    count = lax.axis_size(axis)
-    return lax.all_to_all(jnp.broadcast_to(x[None], (count, *x.shape)), axis, 0, 0, tiled=True)
-
-
-def masked_sums(logs, mask):
-    return jnp.sum(jnp.where(mask[:, :, None], logs[None], 0.0), axis=1)
-
-
-def between(logs, index, reverse):
+def order_weights(logs, index, reverse):
     count = logs.shape[0]
-    row, col = grid_of((count, count), 0), grid_of((count, count), 1)
+    place = lax.rem(index - jnp.arange(count, dtype=jnp.int32) + count, count)
+    row, col = place[:, None], place[None, :]
     if reverse:
-        inner, outer = (col > index) & (col < row), col < row
-        passed = jnp.arange(count) > index
-        own = jnp.arange(count) > index
+        inner, outer, passed = (col < row) & (col > index), col < row, place > index
     else:
-        inner, outer = (col < index) & (col > row), col > row
-        passed = jnp.arange(count) < index
-        own = jnp.arange(count) < index
-    near = jnp.where(passed[:, None], jnp.exp(masked_sums(logs, inner)), 0.0)
-    whole = jnp.exp(masked_sums(logs, outer))
-    own = jnp.exp(jnp.sum(jnp.where(own[:, None], logs, 0.0), axis=0))
+        inner, outer, passed = (col > row) & (col < index), col > row, place < index
+    masked = lambda mask: jnp.sum(jnp.where(mask[:, :, None], logs[None], 0.0), axis=1)
+    near = jnp.where(passed[:, None], jnp.exp(masked(inner)), 0.0)
+    whole = jnp.exp(masked(outer))
+    own = jnp.exp(jnp.sum(jnp.where(passed[:, None], logs, 0.0), axis=0))
     return near, whole, own
 
 
-def state_weights(endings, reverse):
-    inner, outer = lax.axis_size(INNER), lax.axis_size(OUTER)
-    grouped = endings.reshape(outer, inner, -1)
-    place = lax.axis_index(OUTER)
-    mine = jnp.sum(
-        jnp.where((jnp.arange(outer) == place)[:, None, None], grouped, 0.0), axis=0
-    )
-    near, whole, own = between(mine, lax.axis_index(INNER), reverse)
-    far, _, _ = between(jnp.sum(grouped, axis=1), place, reverse)
-    return near, whole, own, far
-
-
-def state_from_others(part, weights):
-    near, whole, own, far = weights
-    pieces = sent_to_all(part, INNER).astype(F32)
-    group = jnp.sum(pieces * whole[:, None, :], axis=0).astype(BF16)
-    inside = jnp.sum(pieces * near[:, None, :], axis=0)
-    groups = sent_to_all(group, OUTER).astype(F32)
-    return inside + own[None] * jnp.sum(groups * far[:, None, :], axis=0)
+def everyone(x, axis):
+    return [x] + [shifted(x, axis, k) for k in range(1, lax.axis_size(axis))]
+
+
+def weighted(pieces, weights):
+    total = 0.0
+    for k, piece in enumerate(pieces):
+        total = total + piece.astype(F32) * weights[k][None, :]
+    return total
+
+
+def states_before(payload):
+    width = payload.shape[0] - 8
+    levels, kept = [], []
+    for axis in reversed(SP):
+        pieces = everyone(payload, axis)
+        logs = jnp.stack([piece[width] for piece in pieces])
+        index = lax.axis_index(axis)
+        near, whole, own = order_weights(logs, index, False)
+        states = [piece[:width] for piece in pieces]
+        levels.append((weighted(states, near), own))
+        kept.append(order_weights(logs, index, True))
+        if axis != SP[0]:
+            row = jnp.sum(logs, axis=0)[None]
+            row = jnp.pad(row, ((0, 7), (0, 0)))
+            payload = jnp.concatenate([weighted(states, whole), row], axis=0)
+    return chained(levels), kept
+
+
+def chained(levels):
+    state = levels[-1][0]
+    for inside, own in reversed(levels[:-1]):
+        state = inside + own[None] * state
+    return state
+
+
+def states_after(part, kept):
+    levels = []
+    for axis, (near, whole, own) in zip(reversed(SP), kept):
+        pieces = everyone(part, axis)
+        levels.append((weighted(pieces, near), own))
+        if axis != SP[0]:
+            part = weighted(pieces, whole).astype(BF16)
+    return chained(levels)
 
 
 def local(
@@ -382,63 +486,78 @@
 ):
     tok_rows, model_width = d_out.shape
     experts = lax.axis_size(SP)
-    tp = lax.axis_size("tp")
     capacity = expert_inputs.shape[1] // experts
-    stride = -(-capacity // PAD) * PAD
-    slots = experts * stride
-    quarter = model_width // tp
-
-    outbox, pick = vmem_call(
-        route_body,
+    cut = capacity * 2 // 3 // PAD * PAD
+    tail = -(-(capacity - cut) // PAD) * PAD
+    quarter = model_width // lax.axis_size("tp")
+    place = lax.axis_index("tp").reshape(1)
+    chosen, weight = route_expert.T, route_weight.T
+
+    def exchanged(box, stride):
+        box = box.reshape(experts, stride, box.shape[1])
+        box = lax.all_to_all(box, SP, split_axis=0, concat_axis=0, tiled=True)
+        return box.reshape(experts * stride, box.shape[2])
+
+    outbox_a, pick_a, ranks = vmem_call(
+        functools.partial(route_body, experts=experts, most=cut, stride=cut),
         [
-            jax.ShapeDtypeStruct((slots, model_width), BF16),
-            jax.ShapeDtypeStruct((slots, tok_rows), BF16),
+            jax.ShapeDtypeStruct((experts * cut, model_width), BF16),
+            jax.ShapeDtypeStruct((experts * cut, tok_rows), BF16),
+            jax.ShapeDtypeStruct((2, tok_rows), jnp.int32),
         ],
-    )(d_out, route_expert.T, route_weight)
-    routed = lax.all_to_all(
-        outbox.reshape(experts, stride, model_width), SP, split_axis=0, concat_axis=0, tiled=True
-    ).reshape(slots, model_width)
-
-    query, key, value, decay = queries[:, 0], keys[:, 0], values[:, 0], log_decay[:, 0]
-    cumulative, ends, gain, produced, ending = local_states(key, value, decay)
-    endings = lax.all_gather(ending[0], SP)
-    start = state_from_others(produced, state_weights(endings, False))
-    mixed, states, scores = forward(query, key, value, cumulative, ends, gain, start)
+    )(d_out, chosen, weight)
+    routed_a = exchanged(outbox_a, cut)
+    outbox_b, pick_b = vmem_call(
+        functools.partial(refill_body, least=cut, most=capacity, stride=tail),
+        [
+            jax.ShapeDtypeStruct((experts * tail, model_width), BF16),
+            jax.ShapeDtypeStruct((experts * tail, tok_rows), BF16),
+        ],
+    )(d_out, chosen, weight, ranks)
+    routed_b = exchanged(outbox_b, tail)
 
     rows_in = expert_inputs[0].reshape(experts, capacity, model_width)
-    rows_in = jnp.pad(rows_in, ((0, 0), (0, stride - capacity), (0, 0))).reshape(
-        slots, model_width
-    )
-    gate_w, up_w, down_w = w_gate[0], w_up[0], w_down[0]
-    gate_pre = dot(rows_in, gate_w, NN)
-    up_pre = dot(rows_in, up_w, NN)
+    rows_a = rows_in[:, :cut].reshape(experts * cut, model_width)
+    rows_b = jnp.pad(rows_in[:, cut:], ((0, 0), (0, cut + tail - capacity), (0, 0)))
+    rows_in = jnp.concatenate([rows_a, rows_b.reshape(experts * tail, model_width)], axis=0)
+    gate_w, up_w, down_w = w_gate[0].T, w_up[0].T, w_down[0]
+    gate_pre = dot(rows_in, gate_w, NT)
+    up_pre = dot(rows_in, up_w, NT)
     sigmoid_gate = jax.nn.sigmoid(gate_pre)
     active = gate_pre * sigmoid_gate
     hidden = (active * up_pre).astype(BF16)
     slope = up_pre * sigmoid_gate * (1.0 + gate_pre * (1.0 - sigmoid_gate))
-    d_gate, d_up, partial = expert_cotangents(routed, active, slope, down_w, gate_w, up_w, tp)
-    arrived = lax.all_to_all(partial, "tp", 0, 0, tiled=True)
-    grad_gate = dot(rows_in, d_gate, TN).astype(BF16)
-    grad_up = dot(rows_in, d_up, TN).astype(BF16)
+
+    query, key, value, decay = queries[:, 0], keys[:, 0], values[:, 0], log_decay[:, 0]
+    cumulative, ends, gain, produced = local_states(key, value, decay)
+    start, kept = states_before(produced)
+    mixed, states, scores = forward(query, key, value, cumulative, ends, gain, start)
+
+    weights = (active, slope, down_w, gate_w, up_w)
+    d_gate, d_up, *parts_a = expert_cotangents(place, routed_a, *weights, 0, ())
+    d_gate, d_up, *parts_b = expert_cotangents(
+        place, routed_b, *weights, experts * cut, (d_gate, d_up)
+    )
+    returned_a = exchanged(summed_over_tp(*parts_a), cut)
+    returned_b = exchanged(summed_over_tp(*parts_b), tail)
+    routed = jnp.concatenate([routed_a, routed_b], axis=0)
+    grad_gate = dot(d_gate, rows_in, TN).astype(BF16).T
+    grad_up = dot(d_up, rows_in, TN).astype(BF16).T
     grad_down = dot(hidden, routed, TN).astype(BF16)
-    summed = jnp.sum(arrived.astype(F32), axis=0).astype(BF16)
-    returned = lax.all_to_all(
-        summed.reshape(experts, stride, quarter), SP, split_axis=0, concat_axis=0, tiled=True
-    ).reshape(slots, quarter)
-
-    own_cols = lax.dynamic_slice_in_dim(d_out, lax.axis_index("tp") * quarter, quarter, 1)
-    mix_cols = (own_cols.astype(F32) + dot(pick, returned, TN)).astype(BF16)
-    tiles = sent_to_all(mix_cols, "tp")
-
-    d_mixed, back, own_term = cotangents(tiles, w_out, query, cumulative, ends)
-    later = state_from_others(own_term, state_weights(endings, True))
+
+    own_cols = lax.dynamic_slice_in_dim(d_out, place[0] * quarter, quarter, 1)
+    picked = own_cols.astype(F32) + dot(pick_a, returned_a, TN)
+    picked = picked + dot(pick_b, returned_b, TN)
+    tiles = gathered_ring(picked.astype(BF16))
+
+    d_mixed, back, own_term = cotangents(place, tiles, w_out, query, cumulative, ends)
+    later = states_after(own_term, kept)
     inside = inside_blocks(query, key, value, cumulative, scores, d_mixed)
     grad_q, grad_k, grad_v, grad_g = backward(
         query, key, value, cumulative, ends, d_mixed, states, back, inside, later
     )
 
-    proj = jnp.einsum("ptc,te->pce", tiles, mixed, preferred_element_type=F32).astype(BF16)
-    proj = proj.reshape(experts, model_width // experts, -1)
+    proj = projection(place, tiles, mixed).reshape(experts, model_width // experts, -1)
     grad_proj = jnp.sum(lax.all_to_all(proj, SP, 0, 0, tiled=True).astype(F32), axis=0)
     return (
         grad_gate[None],

time: 331 us -> 287 us (0.87)
  waiting for transfers between devices: 118 us -> 61.5 us
  blocking collectives: 23.2 us -> 0 us
  starting transfers between devices: 55.2 us -> 73.8 us
  Pallas kernels: 48.2 us -> 59.7 us
  other arithmetic: 7.88 us -> 16 us
    all_to_all x8 -> x4, waiting for transfers between devices: 118 us -> 21.7 us  [exchanged(): box = lax.all_to_all(box, SP, split_axis=0, concat_axis=0, tiled=True)]
    ppermute x0 -> x26, waiting for transfers between devices: none -> 39.7 us  [the longest x8 27.2 us: swapped(): return lax.ppermute(x, 'tp', [(i, i ^ flip) for i in range(count)])]
    ppermute x0 -> x26, starting transfers between devices: none -> 39.1 us  [the longest x18 27.4 us: shifted(): return lax.ppermute(x, axis, [(i, (i + by) % count) for i in range(count)])]
    all_gather x1 -> x0, blocking collectives: 23.2 us -> none  [local(): endings = lax.all_gather(ending[0], SP)]
    all_to_all x8 -> x4, starting transfers between devices: 48 us -> 28.3 us  [exchanged(): box = lax.all_to_all(box, SP, split_axis=0, concat_axis=0, tiled=True)]
    pallas_call x2 -> x5, Pallas kernels: 27.2 us -> 38.7 us  [the longest x2 24.8 us: expert_cotangents(): pl.pallas_call(expert_body, grid_spec=pltpu.PrefetchScalarGridSpec(num_sc...]
    unnamed x17 -> x97, local copies, waits for them, and re-layouts: 12.3 us -> 4.41 us
    slice x0 -> x8, local copies, waits for them, and re-layouts: none -> 7.2 us  [the longest x1 4.09 us: local(): rows_a = rows_in[:, :cut].reshape(experts * cut, model_width)]
  transfers between devices with their start and end apart: 9 -> 31, of which waited for: 7 -> 9; matrix products, arithmetic and copies ran while one was open for 21% -> 28% of each run, Pallas kernels for 5% -> 18%
where the time goes in v1:
time: 287 us; the launch traced here: 282 us
  starting transfers between devices  73.8 us (26%)
  waiting for transfers between devices  61.5 us (21%)
  Pallas kernels  59.7 us (21%)
  matrix products  42.5 us (15%)
  local copies, waits for them, and re-layouts  26.7 us (9%)
  other arithmetic  16 us (6%)
    dot_general x7, matrix products, dot(): return lax.dot_general(a, b, dims, preferred_element_type=F32)  42.5 us
    all_to_all x4, starting transfers between devices, exchanged(): box = lax.all_to_all(box, SP, split_axis=0, concat_axis=0, tiled=True)  28.3 us
    ppermute x18, starting transfers between devices, shifted(): return lax.ppermute(x, axis, [(i, (i + by) % count) for i in range(count)])  27.4 us
    ppermute x8, waiting for transfers between devices, swapped(): return lax.ppermute(x, 'tp', [(i, i ^ flip) for i in range(count)])  27.2 us
    pallas_call x2, Pallas kernels, expert_cotangents(): pl.pallas_call(expert_body, grid_spec=pltpu.PrefetchScalarGridSpec(num_sc...  24.8 us
    all_to_all x4, waiting for transfers between devices, exchanged(): box = lax.all_to_all(box, SP, split_axis=0, concat_axis=0, tiled=True)  21.7 us
    ppermute x18, waiting for transfers between devices, shifted(): return lax.ppermute(x, axis, [(i, (i + by) % count) for i in range(count)])  12.6 us
    ppermute x8, starting transfers between devices, swapped(): return lax.ppermute(x, 'tp', [(i, i ^ flip) for i in range(count)])  11.6 us
  transfers between devices with their start and end apart: 31, of which 9 were waited for; matrix products, arithmetic and copies ran while one was open for 28% of the time, Pallas kernels for 18%

profile of v1, /device:TPU:1, one launch (start us, length us, event | category | flops | bytes accessed | tf_op | source)
XLA Modules:
  0.0 281.8 jit_solution(11955393284288211754)
XLA Ops:
  0.6 3.2 %shard_map.183 = (f32[512,128]{1,0:T(8,128)}, f32[8,128]{1,0:T(8,128)}, f32[8,256,128]{2,1,0:T(8,128)}, f32[264,128]{1,0:T(8,128)}) custom-call(bf16[512,128]{1,0:T(8,128)(2,1)} %bitcast.166, bf16[512,256]{1,0:T(8,128)(2,1)} %bitcast.146, f32[512,128]{1,0:T(8,128)} %bitcast.170), custom_call_target="tpu_custom_call" | custom-call | tf_op jit(solution)/shard_map/pallas_call | solution.py:238
  5.2 5.9 %shard_map.179 = (bf16[768,2048]{1,0:T(8,128)(2,1)}, bf16[768,512]{1,0:T(8,128)(2,1)}, s32[2,512]{1,0:T(2,128)}) custom-call(bf16[512,2048]{1,0:T(8,128)(2,1)} %d_out.3, s32[2,512]{1,0:T(2,128)} %bitcast.171, f32[2,512]{1,0:T(2,128)} %bitcast.173), custom_call_target="tpu_custom_call" | custom-call | tf_op jit(solution)/shard_map/pallas_call | solution.py:501
  11.2 9.1 %all-to-all-start.1 = ((bf16[32,24,2048]{2,1,0:T(8,128)(2,1)}), bf16[32,24,2048]{2,1,0:T(8,128)(2,1)}, u32[]{:S(2)}, u32[]{:S(2)}) async-start(bf16[32,24,2048]{2,1,0:T(8,128)(2,1)} %bitcast.154), calls=%async_computation.1 | async-start | bytes 6291456 | tf_op jit(solution)/shard_map/all_to_all | solution.py:498
  20.4 7.2 %reshape_squeeze.3 = bf16[32,36,2048]{2,1,0:T(8,128)(2,1)} reshape(bf16[1,1152,2048]{2,1,0:T(8,128)(2,1)} %param.15) | data formatting | bytes 9437184 | tf_op jit(solution)/shard_map/reshape;squeeze | solution.py:519
  27.6 4.1 %slice.274 = bf16[32,24,2048]{2,1,0:T(8,128)(2,1)} slice(bf16[32,36,2048]{2,1,0:T(8,128)(2,1)} %reshape_squeeze.3), slice={[0:32], [0:24], [0:2048]} | slice | bytes 6291456 | tf_op jit(solution)/shard_map/slice | solution.py:520
  31.6 4.6 %shard_map.180 = (bf16[512,2048]{1,0:T(8,128)(2,1)}, bf16[512,512]{1,0:T(8,128)(2,1)}) custom-call(bf16[512,2048]{1,0:T(8,128)(2,1)} %d_out.3, s32[2,512]{1,0:T(2,128)} %bitcast.172, f32[2,512]{1,0:T(2,128)} %bitcast.174, s32[2,512]{1,0:T(2,128)} %get-tuple-element.42.ranks), custom_call_target="tpu_custom_call" | custom-call | tf_op jit(solution)/shard_map/pallas_call | solution.py:510
  38.8 6.4 %fusion.13 = f32[1280,704]{1,0:T(8,128)S(1)} fusion(bf16[1,2048,704]{1,2,0:T(8,128)(2,1)S(1)} %copy-done, bf16[512,2048]{1,0:T(8,128)(2,1)S(1)} %bitcast.157, bf16[768,2048]{1,0:T(8,128)(2,1)} %bitcast.150), kind=kOutput, calls=%fused_computation.15 | convolution fusion | flops 3701473280 | bytes 11730944 | tf_op jit(solution)/shard_map/dot_general | solution.py:24
  45.2 9.5 %add_multiply_fusion = (f32[1280,704]{1,0:T(8,128)}, f32[1280,704]{1,0:T(8,128)}, f32[1280,704]{1,0:T(8,128)}) fusion(f32[1280,704]{1,0:T(8,128)S(1)} %fusion.13, bf16[1,2048,704]{1,2,0:T(8,128)(2,1)S(1)} %copy-done.1, bf16[512,2048]{1,0:T(8,128)(2,1)S(1)} %bitcast.158, bf16[768,2048]{1,0:T(8,128)(2,1)S(1)} %bitcast.152), kind=kOutput, calls=%fused_computation.6 | convolution fusion | flops 3709583360 | bytes 22544384 | tf_op jit(solution)/shard_map/dot_general | solution.py:24
  55.7 2.6 collective-permute-start.15
  60.7 7.5 %all-to-all-start = ((bf16[32,16,2048]{2,1,0:T(8,128)(2,1)}), bf16[32,16,2048]{2,1,0:T(8,128)(2,1)S(1)}, u32[]{:S(2)}, u32[]{:S(2)}) async-start(bf16[32,16,2048]{2,1,0:T(8,128)(2,1)} %bitcast.161), calls=%async_computation | async-start | bytes 4194304 | tf_op jit(solution)/shard_map/all_to_all | solution.py:498
  74.8 13.7 %shard_map.181 = (bf16[1280,704]{1,0:T(8,128)(2,1)}, bf16[1280,704]{1,0:T(8,128)(2,1)}, bf16[2,768,256]{2,1,0:T(8,128)(2,1)}, bf16[2,768,256]{2,1,0:T(8,128)(2,1...) custom-call(s32[1]{0:T(128)} %bitcast.2.place, bf16[768,2048]{1,0:T(8,128)(2,1)} %bitcast.13.routed, ...), custom_call_target="tpu_custom_call" | custom-call | tf_op jit(solution)/shard_map/pallas_call | solution.py:155
  88.5 8.3 %all-to-all-done = bf16[32,16,2048]{2,1,0:T(8,128)(2,1)S(1)} async-done(((bf16[32,16,2048]{2,1,0:T(8,128)(2,1)}), bf16[32,16,2048]{2,1,0:T(8,128)(2,1)S(1)}, u32[]{:S(2)}, u32[]{:S(2)}) %all-to-all-start) | async-done | bytes 2097184 | tf_op jit(solution)/shard_map/all_to_all | solution.py:498
  98.1 11.2 %shard_map.182 = (bf16[1280,704]{1,0:T(8,128)(2,1)}, bf16[1280,704]{1,0:T(8,128)(2,1)}, bf16[2,512,256]{2,1,0:T(8,128)(2,1)}, bf16[2,512,256]{2,1,0:T(8,128)(2,1...) custom-call(s32[1]{0:T(128)} %bitcast.2.place, ...), custom_call_target="tpu_custom_call", output_to_operand_aliasing={{0}: (7, {}), {1}: (8, {})} | custom-call | tf_op jit(solution)/shard_map/pallas_call | solution.py:155
  114.5 6.7 %collective-permute-done.4 = bf16[2,512,256]{2,1,0:T(8,128)(2,1)S(1)} collective-permute-done((bf16[2,512,256]{2,1,0:T(8,128)(2,1)}, bf16[2,512,256]{2,1,0:T(8,128)(2,1)S(1)}, u32[]{:S(2)}, u32[]{:S(2)}) %collective-permute-start.4) | collective-permute-done | bytes 524320 | tf_op jit(solution)/shard_map/ppermute | solution.py:172
  124.7 13.4 %collective-permute-done = bf16[2,768,256]{2,1,0:T(8,128)(2,1)S(1)} collective-permute-done((bf16[2,768,256]{2,1,0:T(8,128)(2,1)S(1)}, bf16[2,768,256]{2,1,0:T(8,128)(2,1)S(1)}, u32[]{:S(2)}, u32[]{:S(2)}) %collective-permute-start) | collective-permute-done | bytes 786464 | tf_op jit(solution)/shard_map/ppermute | solution.py:172
  144.1 7.1 %collective-permute-done.1 = bf16[768,256]{1,0:T(8,128)(2,1)S(1)} collective-permute-done((bf16[768,256]{1,0:T(8,128)(2,1)S(1)}, bf16[768,256]{1,0:T(8,128)(2,1)S(1)}, u32[]{:S(2)}, u32[]{:S(2)}) %collective-permute-start.1) | collective-permute-done | bytes 393248 | tf_op jit(solution)/shard_map/ppermute | solution.py:172
  155.1 7.7 %all-to-all-start.2 = ((bf16[32,24,512]{2,1,0:T(8,128)(2,1)}), bf16[32,24,512]{2,1,0:T(8,128)(2,1)S(1)}, u32[]{:S(2)}, u32[]{:S(2)}) async-start(bf16[32,24,512]{2,1,0:T(8,128)(2,1)} %bitcast.23), calls=%async_computation.2 | async-start | bytes 1572864 | tf_op jit(solution)/shard_map/all_to_all | solution.py:498
  172.0 5.1 %all-to-all-done.2 = bf16[32,24,512]{2,1,0:T(8,128)(2,1)S(1)} async-done(((bf16[32,24,512]{2,1,0:T(8,128)(2,1)}), bf16[32,24,512]{2,1,0:T(8,128)(2,1)S(1)}, u32[]{:S(2)}, u32[]{:S(2)}) %all-to-all-start.2) | async-done | bytes 786464 | tf_op jit(solution)/shard_map/all_to_all | solution.py:498
  177.1 4.1 %all-to-all-start.3 = ((bf16[32,16,512]{2,1,0:T(8,128)(2,1)}), bf16[32,16,512]{2,1,0:T(8,128)(2,1)S(1)}, u32[]{:S(2)}, u32[]{:S(2)}) async-start(bf16[32,16,512]{2,1,0:T(8,128)(2,1)} %bitcast.29), calls=%async_computation.3 | async-start | bytes 1048576 | tf_op jit(solution)/shard_map/all_to_all | solution.py:498
  184.2 8.4 %all-to-all-done.3 = bf16[32,16,512]{2,1,0:T(8,128)(2,1)S(1)} async-done(((bf16[32,16,512]{2,1,0:T(8,128)(2,1)}), bf16[32,16,512]{2,1,0:T(8,128)(2,1)S(1)}, u32[]{:S(2)}, u32[]{:S(2)}) %all-to-all-start.3) | async-done | bytes 524320 | tf_op jit(solution)/shard_map/all_to_all | solution.py:498
  199.6 8.9 %collective-permute-done.8.b = bf16[512,512]{1,0:T(8,128)(2,1)S(1)} collective-permute-done((bf16[512,512]{1,0:T(8,128)(2,1)S(1)}, bf16[512,512]{1,0:T(8,128)(2,1)S(1)}, u32[]{:S(2)}, u32[]{:S(2)}) %collective-permute-start.8) | collective-permute-done | bytes 524320 | tf_op jit(solution)/shard_map/ppermute | solution.py:195
  209.8 3.4 %shard_map.184 = (bf16[512,256]{1,0:T(8,128)(2,1)}, f32[9,256,128]{2,1,0:T(8,128)}, f32[512,64]{1,0:T(8,128)}) custom-call(bf16[512,128]{1,0:T(8,128)(2,1)} %bitcast.162, bf16[512,128]{1,0:T(8,128)(2,1)} %bitcast.167, bf16[512,256]{1,0:T(8,128)(2,1)} %bitcast.147, f32[512,128]{1,0:T(8,128)} %get-tuple-element.59.cumulative, ...), custom_call_target="tpu_custom_call" | custom-call | tf_op jit(solution)/shard_map/pallas_call | solution.py:275
  216.5 3.3 %collective-permute-done.11 = bf16[256,512]{1,0:T(8,128)(2,1)S(1)} collective-permute-done((bf16[256,512]{1,0:T(8,128)(2,1)S(1)}, bf16[256,512]{1,0:T(8,128)(2,1)S(1)}, u32[]{:S(2)}, u32[]{:S(2)}) %collective-permute-start.11) | collective-permute-done | bytes 262176 | tf_op jit(solution)/shard_map/ppermute | solution.py:195
  220.7 4.9 %shard_map.186 = (f32[512,256]{1,0:T(8,128)}, f32[8,256,128]{2,1,0:T(8,128)}, bf16[256,128]{1,0:T(8,128)(2,1)}) custom-call(s32[1]{0:T(128)} %bitcast.2.place, bf16[512,512]{1,0:T(8,128)(2,1)} %copy-done.4, bf16[512,512]{1,0:T(8,128)(2,1)} %copy-done.5, bf16[512,512]{1,0:T(8,128)(2,1)} %copy-done.6, bf16[512,512]{1,0:T(8,128)(2,1)} %copy-done.7, ...), custom_call_target="tpu_custom_call" | custom-call | tf_op jit(solution)/shard_map/pallas_call | solution.py:313
  228.0 10.0 %fusion.10 = bf16[1,704,2048]{2,1,0:T(8,128)(2,1)} fusion(bf16[512,2048]{1,0:T(8,128)(2,1)S(1)} %bitcast.144, bf16[768,2048]{1,0:T(8,128)(2,1)} %bitcast.13.routed, f32[1280,704]{1,0:T(8,128)} %copy-done.47, f32[1280,704]{1,0:T(8,128)} %get-tuple-element.175), kind=kOutput, calls=%fused_computation.14 | convolution fusion | flops 3708321792 | bytes 15335424 | tf_op jit(solution)/shard_map/dot_general | solution.py:24
  241.0 5.3 %fusion.8 = bf16[1,2048,704]{1,2,0:T(8,128)(2,1)} fusion(bf16[1280,704]{1,0:T(8,128)(2,1)S(1)} %copy-done.12, bf16[512,2048]{1,0:T(8,128)(2,1)S(1)} %bitcast.159, bf16[768,2048]{1,0:T(8,128)(2,1)S(1)} %bitcast.153), kind=kOutput, calls=%fused_computation.12 | convolution fusion | flops 3702915072 | bytes 9928704 | tf_op jit(solution)/shard_map/dot_general | solution.py:24
  246.4 3.3 %shard_map.185 = bf16[2048,256]{1,0:T(8,128)(2,1)} custom-call(s32[1]{0:T(128)} %bitcast.2.place, bf16[512,512]{1,0:T(8,128)(2,1)} %copy-done.4, bf16[512,512]{1,0:T(8,128)(2,1)} %copy-done.5, bf16[512,512]{1,0:T(8,128)(2,1)} %copy-done.6, bf16[512,512]{1,0:T(8,128)(2,1)} %copy-done.7, bf16[512,256]{1,0:T(8,128)(2,1)} %get-tuple-element.63.mixed), custom_call_target="tpu_custom_call" | custom-call | tf_op jit(solution)/shard_map/pallas_call | solution.py:332
  249.7 6.5 %all-to-all-start.4 = ((bf16[32,64,256]{2,1,0:T(8,128)(2,1)}), bf16[32,64,256]{2,1,0:T(8,128)(2,1)S(1)}, u32[]{:S(2)}, u32[]{:S(2)}) async-start(bf16[32,64,256]{2,1,0:T(8,128)(2,1)} %bitcast.145), calls=%async_computation.4 | async-start | bytes 2097152 | tf_op jit(solution)/shard_map/all_to_all | solution.py:561
  256.3 2.9 %collective-permute-start.24 = (bf16[256,128]{1,0:T(8,128)(2,1)S(1)}, bf16[256,128]{1,0:T(8,128)(2,1)S(1)}, u32[]{:S(2)}, u32[]{:S(2)}) collective-permute-start(bf16[256,128]{1,0:T(8,128)(2,1)S(1)} %fusion.38), channel_id=1, source_target_pairs={{0,64},{32,96},{64,0},{96,32},{1,65},{33,97},{65,1},{97,33},{2,66}... | collective-permute-start | bytes 196616 | tf_op jit(solution)/shard_map/ppermute | solution.py:195
  262.2 8.0 %fusion.9 = bf16[1,2048,704]{1,2,0:T(8,128)(2,1)} fusion(bf16[1280,704]{1,0:T(8,128)(2,1)} %get-tuple-element.48, bf16[512,2048]{1,0:T(8,128)(2,1)S(1)} %bitcast.160, bf16[768,2048]{1,0:T(8,128)(2,1)} %bitcast.151), kind=kOutput, calls=%fused_computation.13 | convolution fusion | flops 3702915072 | bytes 9928704 | tf_op jit(solution)/shard_map/dot_general | solution.py:24
  270.3 4.4 %shard_map.187 = (f32[512,128]{1,0:T(8,128)}, f32[512,128]{1,0:T(8,128)}, f32[512,256]{1,0:T(8,128)}) custom-call(bf16[512,128]{1,0:T(8,128)(2,1)} %bitcast.164, bf16[512,128]{1,0:T(8,128)(2,1)} %bitcast.168, bf16[512,256]{1,0:T(8,128)(2,1)} %bitcast.148, f32[512,128]{1,0:T(8,128)} %get-tuple-element.59.cumulative, f32[512,64]{1,0:T(8,128)} %get-tuple-element.67.scores, ...), custom_call_target="tpu_custom_call" | custom-call | tf_op jit(solution)/shard_map/pallas_call | solution.py:360
  275.6 5.1 %shard_map.188 = (bf16[512,128]{1,0:T(8,128)(2,1)}, bf16[512,128]{1,0:T(8,128)(2,1)}, bf16[512,256]{1,0:T(8,128)(2,1)}, f32[512,128]{1,0:T(8,128)}) custom-call(bf16[512,128]{1,0:T(8,128)(2,1)} %bitcast.165, bf16[512,128]{1,0:T(8,128)(2,1)} %bitcast.169, bf16[512,256]{1,0:T(8,128)(2,1)} %bitcast.149, f32[512,128]{1,0:T(8,128)} %get-tuple-element.59.cumulative, ...), custom_call_target="tpu_custom_call" | custom-call | tf_op jit(solution)/shard_map/pallas_call | solution.py:401
  (215 shorter events, 68.4 us)
Async XLA Ops:
  3.8 51.6 %collective-permute-start.12 = (f32[264,128]{1,0:T(8,128)}, f32[264,128]{1,0:T(8,128)S(1)}, u32[]{:S(2)}, u32[]{:S(2)}) collective-permute-start(f32[264,128]{1,0:T(8,128)} %get-tuple-element.62), channel_id=1, source_target_pairs={{0,4},{4,0},{1,5},{5,1},{2,6},{6,2},{3,7},{7,3},{8,12},{12,8},{9,1... | collective-permute-start | bytes 405512 | tf_op jit(solution)/shard_map/ppermute | solution.py:195
  11.2 49.5 %all-to-all-start.1 = ((bf16[32,24,2048]{2,1,0:T(8,128)(2,1)}), bf16[32,24,2048]{2,1,0:T(8,128)(2,1)}, u32[]{:S(2)}, u32[]{:S(2)}) async-start(bf16[32,24,2048]{2,1,0:T(8,128)(2,1)} %bitcast.154), calls=%async_computation.1 | async-start | bytes 6291456 | tf_op jit(solution)/shard_map/all_to_all | solution.py:498
  55.7 14.2 %collective-permute-start.15 = (f32[264,128]{1,0:T(8,128)S(1)}, f32[264,128]{1,0:T(8,128)S(1)}, u32[]{:S(2)}, u32[]{:S(2)}) collective-permute-start(f32[264,128]{1,0:T(8,128)S(1)} %select_maximum_fusion.1), channel_id=1, source_target_pairs={{0,24},{8,0},{16,8},{24,16},{1,25},{9,1},{17,9},{25,17},{2,26},{10... | collective-permute-start | bytes 405512 | tf_op jit(solution)/shard_map/ppermute | solution.py:195
  58.4 11.6 %collective-permute-start.14 = (f32[264,128]{1,0:T(8,128)S(1)}, f32[264,128]{1,0:T(8,128)S(1)}, u32[]{:S(2)}, u32[]{:S(2)}) collective-permute-start(f32[264,128]{1,0:T(8,128)S(1)} %select_maximum_fusion.1), channel_id=1, source_target_pairs={{0,16},{8,24},{16,0},{24,8},{1,17},{9,25},{17,1},{25,9},{2,18},{10... | collective-permute-start | bytes 405512 | tf_op jit(solution)/shard_map/ppermute | solution.py:195
  58.9 11.0 %collective-permute-start.13 = (f32[264,128]{1,0:T(8,128)S(1)}, f32[264,128]{1,0:T(8,128)S(1)}, u32[]{:S(2)}, u32[]{:S(2)}) collective-permute-start(f32[264,128]{1,0:T(8,128)S(1)} %select_maximum_fusion.1), channel_id=1, source_target_pairs={{0,8},{8,16},{16,24},{24,0},{1,9},{9,17},{17,25},{25,1},{2,10},{10... | collective-permute-start | bytes 405512 | tf_op jit(solution)/shard_map/ppermute | solution.py:195
  60.7 36.1 %all-to-all-start = ((bf16[32,16,2048]{2,1,0:T(8,128)(2,1)}), bf16[32,16,2048]{2,1,0:T(8,128)(2,1)S(1)}, u32[]{:S(2)}, u32[]{:S(2)}) async-start(bf16[32,16,2048]{2,1,0:T(8,128)(2,1)} %bitcast.161), calls=%async_computation | async-start | bytes 4194304 | tf_op jit(solution)/shard_map/all_to_all | solution.py:498
  71.5 94.3 %collective-permute-start.18 = (f32[264,128]{1,0:T(8,128)}, f32[264,128]{1,0:T(8,128)}, u32[]{:S(2)}, u32[]{:S(2)}) collective-permute-start(f32[264,128]{1,0:T(8,128)} %select_maximum_fusion), channel_id=1, source_target_pairs={{0,96},{32,0},{64,32},{96,64},{1,97},{33,1},{65,33},{97,65},{2,98}... | collective-permute-start | bytes 405512 | tf_op jit(solution)/shard_map/ppermute | solution.py:195
  74.1 92.4 %collective-permute-start.17 = (f32[264,128]{1,0:T(8,128)}, f32[264,128]{1,0:T(8,128)}, u32[]{:S(2)}, u32[]{:S(2)}) collective-permute-start(f32[264,128]{1,0:T(8,128)} %select_maximum_fusion), channel_id=1, source_target_pairs={{0,64},{32,96},{64,0},{96,32},{1,65},{33,97},{65,1},{97,33},{2,66}... | collective-permute-start | bytes 405512 | tf_op jit(solution)/shard_map/ppermute | solution.py:195
  98.1 44.6 %copy-start.13 = (bf16[2,768,256]{2,1,0:T(8,128)(2,1)S(1)}, bf16[2,768,256]{2,1,0:T(8,128)(2,1)}, u32[]{:S(2)}) copy-start(bf16[2,768,256]{2,1,0:T(8,128)(2,1)} %get-tuple-element.52) | copy-start | bytes 2359300
  109.3 11.9 %collective-permute-start.4 = (bf16[2,512,256]{2,1,0:T(8,128)(2,1)}, bf16[2,512,256]{2,1,0:T(8,128)(2,1)S(1)}, u32[]{:S(2)}, u32[]{:S(2)}) collective-permute-start(bf16[2,512,256]{2,1,0:T(8,128)(2,1)} %get-tuple-element.56), channel_id=1, source_target_pairs={{0,1},{1,0},{2,3},{3,2},{4,5},{5,4},{6,7},{7,6},{8,9},{9,8},{10,11... | collective-permute-start | bytes 1572872 | tf_op jit(solution)/shard_map/ppermute | solution.py:172
  110.5 27.5 %collective-permute-start = (bf16[2,768,256]{2,1,0:T(8,128)(2,1)S(1)}, bf16[2,768,256]{2,1,0:T(8,128)(2,1)S(1)}, u32[]{:S(2)}, u32[]{:S(2)}) collective-permute-start(bf16[2,768,256]{2,1,0:T(8,128)(2,1)S(1)} %copy-done.46), channel_id=1, source_target_pairs={{0,1},{1,0},{2,3},{3,2},{4,5},{5,4},{6,7},{7,6},{8,9},{9,8},{10,11... | collective-permute-start | bytes 2359304 | tf_op jit(solution)/shard_map/ppermute | solution.py:172
  110.9 29.3 %collective-permute-start.2 = (bf16[2,768,256]{2,1,0:T(8,128)(2,1)S(1)}, bf16[2,768,256]{2,1,0:T(8,128)(2,1)S(1)}, u32[]{:S(2)}, u32[]{:S(2)}) collective-permute-start(bf16[2,768,256]{2,1,0:T(8,128)(2,1)S(1)} %copy-done.45), channel_id=1, source_target_pairs={{0,3},{1,2},{2,1},{3,0},{4,7},{5,6},{6,5},{7,4},{8,11},{9,10},{10,... | collective-permute-start | bytes 2359304 | tf_op jit(solution)/shard_map/ppermute | solution.py:172
  121.2 21.7 %collective-permute-start.6 = (bf16[2,512,256]{2,1,0:T(8,128)(2,1)}, bf16[2,512,256]{2,1,0:T(8,128)(2,1)S(1)}, u32[]{:S(2)}, u32[]{:S(2)}) collective-permute-start(bf16[2,512,256]{2,1,0:T(8,128)(2,1)} %get-tuple-element.58), channel_id=1, source_target_pairs={{0,3},{1,2},{2,1},{3,0},{4,7},{5,6},{6,5},{7,4},{8,11},{9,10},{10,... | collective-permute-start | bytes 1572872 | tf_op jit(solution)/shard_map/ppermute | solution.py:172
  138.1 29.6 %collective-permute-start.16 = (f32[264,128]{1,0:T(8,128)}, f32[264,128]{1,0:T(8,128)}, u32[]{:S(2)}, u32[]{:S(2)}) collective-permute-start(f32[264,128]{1,0:T(8,128)} %select_maximum_fusion), channel_id=1, source_target_pairs={{0,32},{32,64},{64,96},{96,0},{1,33},{33,65},{65,97},{97,1},{2,34}... | collective-permute-start | bytes 405512 | tf_op jit(solution)/shard_map/ppermute | solution.py:195
  140.2 11.1 %collective-permute-start.1 = (bf16[768,256]{1,0:T(8,128)(2,1)S(1)}, bf16[768,256]{1,0:T(8,128)(2,1)S(1)}, u32[]{:S(2)}, u32[]{:S(2)}) collective-permute-start(bf16[768,256]{1,0:T(8,128)(2,1)S(1)} %fusion.22), channel_id=1, source_target_pairs={{0,3},{1,2},{2,1},{3,0},{4,7},{5,6},{6,5},{7,4},{8,11},{9,10},{10,... | collective-permute-start | bytes 1179656 | tf_op jit(solution)/shard_map/ppermute | solution.py:172
  142.9 11.0 %collective-permute-start.3 = (bf16[768,256]{1,0:T(8,128)(2,1)S(1)}, bf16[768,256]{1,0:T(8,128)(2,1)S(1)}, u32[]{:S(2)}, u32[]{:S(2)}) collective-permute-start(bf16[768,256]{1,0:T(8,128)(2,1)S(1)} %fusion.23), channel_id=1, source_target_pairs={{0,1},{1,0},{2,3},{3,2},{4,5},{5,4},{6,7},{7,6},{8,9},{9,8},{10,11... | collective-permute-start | bytes 1179656 | tf_op jit(solution)/shard_map/ppermute | solution.py:172
  151.3 17.6 %collective-permute-start.5 = (bf16[512,256]{1,0:T(8,128)(2,1)S(1)}, bf16[512,256]{1,0:T(8,128)(2,1)}, u32[]{:S(2)}, u32[]{:S(2)}) collective-permute-start(bf16[512,256]{1,0:T(8,128)(2,1)S(1)} %fusion.24), channel_id=1, source_target_pairs={{0,3},{1,2},{2,1},{3,0},{4,7},{5,6},{6,5},{7,4},{8,11},{9,10},{10,... | collective-permute-start | bytes 786440 | tf_op jit(solution)/shard_map/ppermute | solution.py:172
  153.9 16.1 %collective-permute-start.7 = (bf16[512,256]{1,0:T(8,128)(2,1)S(1)}, bf16[512,256]{1,0:T(8,128)(2,1)}, u32[]{:S(2)}, u32[]{:S(2)}) collective-permute-start(bf16[512,256]{1,0:T(8,128)(2,1)S(1)} %fusion.25), channel_id=1, source_target_pairs={{0,1},{1,0},{2,3},{3,2},{4,5},{5,4},{6,7},{7,6},{8,9},{9,8},{10,11... | collective-permute-start | bytes 786440 | tf_op jit(solution)/shard_map/ppermute | solution.py:172
  155.1 21.9 %all-to-all-start.2 = ((bf16[32,24,512]{2,1,0:T(8,128)(2,1)}), bf16[32,24,512]{2,1,0:T(8,128)(2,1)S(1)}, u32[]{:S(2)}, u32[]{:S(2)}) async-start(bf16[32,24,512]{2,1,0:T(8,128)(2,1)} %bitcast.23), calls=%async_computation.2 | async-start | bytes 1572864 | tf_op jit(solution)/shard_map/all_to_all | solution.py:498
  177.1 15.6 %all-to-all-start.3 = ((bf16[32,16,512]{2,1,0:T(8,128)(2,1)}), bf16[32,16,512]{2,1,0:T(8,128)(2,1)S(1)}, u32[]{:S(2)}, u32[]{:S(2)}) async-start(bf16[32,16,512]{2,1,0:T(8,128)(2,1)} %bitcast.29), calls=%async_computation.3 | async-start | bytes 1048576 | tf_op jit(solution)/shard_map/all_to_all | solution.py:498
  194.2 14.4 %collective-permute-start.8 = (bf16[512,512]{1,0:T(8,128)(2,1)S(1)}, bf16[512,512]{1,0:T(8,128)(2,1)S(1)}, u32[]{:S(2)}, u32[]{:S(2)}) collective-permute-start(bf16[512,512]{1,0:T(8,128)(2,1)S(1)} %fusion.17.a), channel_id=1, source_target_pairs={{0,1},{1,2},{2,3},{3,0},{4,5},{5,6},{6,7},{7,4},{8,9},{9,10},{10,1... | collective-permute-start | bytes 1572872 | tf_op jit(solution)/shard_map/ppermute | solution.py:195
  196.7 16.5 %collective-permute-start.9 = (bf16[512,512]{1,0:T(8,128)(2,1)S(1)}, bf16[512,512]{1,0:T(8,128)(2,1)S(1)}, u32[]{:S(2)}, u32[]{:S(2)}) collective-permute-start(bf16[512,512]{1,0:T(8,128)(2,1)S(1)} %fusion.17.a), channel_id=1, source_target_pairs={{0,3},{1,0},{2,1},{3,2},{4,7},{5,4},{6,5},{7,6},{8,11},{9,8},{10,9... | collective-permute-start | bytes 1572872 | tf_op jit(solution)/shard_map/ppermute | solution.py:195
  208.6 7.9 %collective-permute-start.10 = (bf16[256,512]{1,0:T(8,128)(2,1)S(1)}, bf16[256,512]{1,0:T(8,128)(2,1)S(1)}, u32[]{:S(2)}, u32[]{:S(2)}) collective-permute-start(bf16[256,512]{1,0:T(8,128)(2,1)S(1)} %slice.284), channel_id=1, source_target_pairs={{0,1},{1,2},{2,3},{3,0},{4,5},{5,6},{6,7},{7,4},{8,9},{9,10},{10,1... | collective-permute-start | bytes 786440 | tf_op jit(solution)/shard_map/ppermute | solution.py:195
  213.2 6.6 %collective-permute-start.11 = (bf16[256,512]{1,0:T(8,128)(2,1)S(1)}, bf16[256,512]{1,0:T(8,128)(2,1)S(1)}, u32[]{:S(2)}, u32[]{:S(2)}) collective-permute-start(bf16[256,512]{1,0:T(8,128)(2,1)S(1)} %slice.285), channel_id=1, source_target_pairs={{0,3},{1,0},{2,1},{3,2},{4,7},{5,4},{6,5},{7,6},{8,11},{9,8},{10,9... | collective-permute-start | bytes 786440 | tf_op jit(solution)/shard_map/ppermute | solution.py:195
  225.6 12.5 %collective-permute-start.19 = (bf16[256,128]{1,0:T(8,128)(2,1)}, bf16[256,128]{1,0:T(8,128)(2,1)S(1)}, u32[]{:S(2)}, u32[]{:S(2)}) collective-permute-start(bf16[256,128]{1,0:T(8,128)(2,1)} %get-tuple-element.71), channel_id=1, source_target_pairs={{0,4},{4,0},{1,5},{5,1},{2,6},{6,2},{3,7},{7,3},{8,12},{12,8},{9,1... | collective-permute-start | bytes 196616 | tf_op jit(solution)/shard_map/ppermute | solution.py:195
  238.1 18.0 %collective-permute-start.22 = (bf16[256,128]{1,0:T(8,128)(2,1)S(1)}, bf16[256,128]{1,0:T(8,128)(2,1)S(1)}, u32[]{:S(2)}, u32[]{:S(2)}) collective-permute-start(bf16[256,128]{1,0:T(8,128)(2,1)S(1)} %fusion.29), channel_id=1, source_target_pairs={{0,24},{8,0},{16,8},{24,16},{1,25},{9,1},{17,9},{25,17},{2,26},{10... | collective-permute-start | bytes 196616 | tf_op jit(solution)/shard_map/ppermute | solution.py:195
  240.4 15.8 %collective-permute-start.21 = (bf16[256,128]{1,0:T(8,128)(2,1)S(1)}, bf16[256,128]{1,0:T(8,128)(2,1)S(1)}, u32[]{:S(2)}, u32[]{:S(2)}) collective-permute-start(bf16[256,128]{1,0:T(8,128)(2,1)S(1)} %fusion.29), channel_id=1, source_target_pairs={{0,16},{8,24},{16,0},{24,8},{1,17},{9,25},{17,1},{25,9},{2,18},{10... | collective-permute-start | bytes 196616 | tf_op jit(solution)/shard_map/ppermute | solution.py:195
  240.9 15.2 %collective-permute-start.20 = (bf16[256,128]{1,0:T(8,128)(2,1)S(1)}, bf16[256,128]{1,0:T(8,128)(2,1)S(1)}, u32[]{:S(2)}, u32[]{:S(2)}) collective-permute-start(bf16[256,128]{1,0:T(8,128)(2,1)S(1)} %fusion.29), channel_id=1, source_target_pairs={{0,8},{8,16},{16,24},{24,0},{1,9},{9,17},{17,25},{25,1},{2,10},{10... | collective-permute-start | bytes 196616 | tf_op jit(solution)/shard_map/ppermute | solution.py:195
  249.7 31.0 %all-to-all-start.4 = ((bf16[32,64,256]{2,1,0:T(8,128)(2,1)}), bf16[32,64,256]{2,1,0:T(8,128)(2,1)S(1)}, u32[]{:S(2)}, u32[]{:S(2)}) async-start(bf16[32,64,256]{2,1,0:T(8,128)(2,1)} %bitcast.145), calls=%async_computation.4 | async-start | bytes 2097152 | tf_op jit(solution)/shard_map/all_to_all | solution.py:561
  256.3 18.4 %collective-permute-start.24 = (bf16[256,128]{1,0:T(8,128)(2,1)S(1)}, bf16[256,128]{1,0:T(8,128)(2,1)S(1)}, u32[]{:S(2)}, u32[]{:S(2)}) collective-permute-start(bf16[256,128]{1,0:T(8,128)(2,1)S(1)} %fusion.38), channel_id=1, source_target_pairs={{0,64},{32,96},{64,0},{96,32},{1,65},{33,97},{65,1},{97,33},{2,66}... | collective-permute-start | bytes 196616 | tf_op jit(solution)/shard_map/ppermute | solution.py:195
  259.2 15.4 %collective-permute-start.23 = (bf16[256,128]{1,0:T(8,128)(2,1)S(1)}, bf16[256,128]{1,0:T(8,128)(2,1)S(1)}, u32[]{:S(2)}, u32[]{:S(2)}) collective-permute-start(bf16[256,128]{1,0:T(8,128)(2,1)S(1)} %fusion.38), channel_id=1, source_target_pairs={{0,32},{32,64},{64,96},{96,0},{1,33},{33,65},{65,97},{97,1},{2,34}... | collective-permute-start | bytes 196616 | tf_op jit(solution)/shard_map/ppermute | solution.py:195
  259.5 15.1 %collective-permute-start.25 = (bf16[256,128]{1,0:T(8,128)(2,1)S(1)}, bf16[256,128]{1,0:T(8,128)(2,1)S(1)}, u32[]{:S(2)}, u32[]{:S(2)}) collective-permute-start(bf16[256,128]{1,0:T(8,128)(2,1)S(1)} %fusion.38), channel_id=1, source_target_pairs={{0,96},{32,0},{64,32},{96,64},{1,97},{33,1},{65,33},{97,65},{2,98}... | collective-permute-start | bytes 196616 | tf_op jit(solution)/shard_map/ppermute | solution.py:195
  (48 other events, 721.4 us)

commit v2 on v1

--- a/solution.py
+++ b/solution.py
@@ -54,13 +54,16 @@
     return lax.broadcasted_iota(jnp.int32, shape, dim)
 
 
-def vmem_call(kernel, outs, **options):
-    return pl.pallas_call(
-        kernel,
-        out_shape=outs,
-        compiler_params=pltpu.CompilerParams(vmem_limit_bytes=56 * 1024 * 1024),
-        **options,
-    )
+SMEM = pl.BlockSpec(memory_space=pltpu.SMEM)
+VMEM = pl.BlockSpec(memory_space=pltpu.VMEM)
+
+
+def limit(mebibytes):
+    return pltpu.CompilerParams(vmem_limit_bytes=mebibytes * 1024 * 1024)
+
+
+def vmem_call(kernel, outs, mebibytes=12, **options):
+    return pl.pallas_call(kernel, out_shape=outs, compiler_params=limit(mebibytes), **options)
 
 
 def fill_outbox(d_out, weight, slot_a, slot_b, outbox, pick):
@@ -110,11 +113,62 @@
     fill_outbox(d_out, weight, slot_a, slot_b, outbox, pick)
 
 
+def slot_order(group, capacity, cut, tail):
+    def placed(rows, stride, width, first):
+        row, col = grid_of((rows, group * capacity), 0), grid_of((rows, group * capacity), 1)
+        found = row < 0
+        for source in range(group):
+            start = source * stride
+            here = (row >= start) & (row < start + width)
+            found = found | (here & (col == row + (source * capacity + first - start)))
+        return jnp.where(found, 1.0, 0.0).astype(BF16)
+
+    return placed(group * cut, cut, cut, 0), placed(group * tail, tail, capacity - cut, cut)
+
+
+def expert_forward_body(
+    inputs, gate_w, up_w, rows_in, active, slope, hidden, *, experts, capacity, cut, tail
+):
+    group = 8
+    orders = slot_order(group, capacity, cut, tail)
+    for step in range(experts // group):
+        block = inputs[step * group * capacity : (step + 1) * group * capacity, :]
+        for order, start in zip(orders, (step * group * cut, experts * cut + step * group * tail)):
+            rows_in[start : start + order.shape[0], :] = dot(order, block, NN).astype(BF16)
+    units = gate_w.shape[0]
+    step = rows_in.shape[0] // 2
+    for first in range(0, units, 256):
+        cols = slice(first, min(first + 256, units))
+        for start in range(0, rows_in.shape[0], step):
+            rows = slice(start, start + step)
+            gate = dot(rows_in[rows, :], gate_w[cols, :], NT)
+            up = dot(rows_in[rows, :], up_w[cols, :], NT)
+            sigmoid = 1.0 / (1.0 + jnp.exp(-gate))
+            silu = gate * sigmoid
+            hidden[rows, cols] = (silu * up).astype(BF16)
+            active[rows, cols] = silu.astype(BF16)
+            slope[rows, cols] = (up * sigmoid * (1.0 + gate * (1.0 - sigmoid))).astype(BF16)
+
+
+def expert_forward(inputs, gate_w, up_w, experts, capacity, cut, tail):
+    slots = experts * (cut + tail)
+    units = gate_w.shape[0]
+    return vmem_call(
+        functools.partial(
+            expert_forward_body, experts=experts, capacity=capacity, cut=cut, tail=tail
+        ),
+        [jax.ShapeDtypeStruct((slots, inputs.shape[1]), BF16)]
+        + [jax.ShapeDtypeStruct((slots, units), BF16)] * 3,
+        mebibytes=56,
+    )(inputs, gate_w, up_w)
+
+
 def expert_body(place, routed, active, slope, down_w, gate_w, up_w, *refs):
-    d_gate, d_up, keep_a, send_a, keep_b, send_b = refs[-6:]
+    routed_out, d_gate, d_up, keep_a, send_a, keep_b, send_b = refs[-7:]
+    routed_out[...] = routed[...]
     d_hidden = dot(routed[...], down_w[...], NT)
-    to_gate = (d_hidden * slope[...]).astype(BF16)
-    to_up = (d_hidden * active[...]).astype(BF16)
+    to_gate = (d_hidden * slope[...].astype(F32)).astype(BF16)
+    to_up = (d_hidden * active[...].astype(F32)).astype(BF16)
     d_gate[...] = to_gate
     d_up[...] = to_up
     half = keep_a.shape[2]
@@ -158,12 +212,15 @@
             num_scalar_prefetch=1,
             grid=(rows // step,),
             in_specs=in_specs,
-            out_specs=[pl.BlockSpec((step, units), later_row)] * 2 + [pair] * 4,
+            out_specs=[pl.BlockSpec((step, width), later_row)]
+            + [pl.BlockSpec((step, units), later_row)] * 2
+            + [pair] * 4,
         ),
-        out_shape=[jax.ShapeDtypeStruct(active.shape, BF16)] * 2
+        out_shape=[jax.ShapeDtypeStruct((active.shape[0], width), BF16)]
+        + [jax.ShapeDtypeStruct(active.shape, BF16)] * 2
         + [jax.ShapeDtypeStruct((2, rows, half), BF16)] * 4,
         input_output_aliases={7 + i: i for i in range(len(earlier))},
-        compiler_params=pltpu.CompilerParams(vmem_limit_bytes=56 * 1024 * 1024),
+        compiler_params=limit(56),
     )(place, routed, active, slope, down_w, gate_w, up_w, *earlier)
 
 
@@ -197,7 +254,8 @@
 
 def gathered_ring(x):
     half = x.shape[0] // 2
-    below, above = shifted(x, "tp", 1), shifted(x, "tp", -1)
+    below = shifted(x, "tp", 1)
+    above = shifted(x, "tp", -1)
     across = jnp.concatenate(
         [shifted(below[:half], "tp", 1), shifted(above[half:], "tp", -1)], axis=0
     )
@@ -246,11 +304,15 @@
     )(keys, values, decay)
 
 
-def forward_body(queries, keys, values, cumulative, ends, gain, start, mixed, states, scores):
+def forward_body(index, queries, keys, values, cumulative, ends, gain, *refs):
+    *pieces, inside_0, inside_1, book_0, book_1, mixed, states, scores, book = refs
     blocks = gain.shape[0]
+    far, _, (near, _, _) = opened(pieces, index[0], book)
+    own = slice(BOOK_OWN + 1, BOOK_OWN + 2)
+    start = inside_0[...] + book_0[own, :] * (inside_1[...] + book_1[own, :] * weighted(far, near))
     scale = queries.shape[1] ** (-0.5)
     causal = grid_of((BLK, BLK), 0) >= grid_of((BLK, BLK), 1)
-    state = start[...]
+    state = start
     for c in range(blocks):
         rows = slice(c * BLK, (c + 1) * BLK)
         cum = cumulative[rows, :]
@@ -268,18 +330,22 @@
     states[blocks] = state
 
 
-def forward(queries, keys, values, cumulative, ends, gain, start):
+def forward(queries, keys, values, cumulative, ends, gain, before):
+    pieces, index, insides, books = before
     tokens, channels = keys.shape
     width = values.shape[1]
     blocks = tokens // BLK
+    operands = (*pieces, *insides, *books)
     return vmem_call(
         forward_body,
         [
             jax.ShapeDtypeStruct((tokens, width), BF16),
             jax.ShapeDtypeStruct((blocks + 1, width, channels), F32),
             jax.ShapeDtypeStruct((tokens, BLK), F32),
+            jax.ShapeDtypeStruct((BOOK_ROWS, channels), F32),
         ],
-    )(queries, keys, values, cumulative, ends, gain, start)
+        in_specs=[SMEM] + [VMEM] * (6 + len(operands)),
+    )(index, queries, keys, values, cumulative, ends, gain, *operands)
 
 
 def cotangent_body(place, a, b, c, d, w_out, queries, cumulative, ends, d_mixed, back, own):
@@ -302,10 +368,6 @@
     own[...] = state.astype(BF16)
 
 
-SMEM = pl.BlockSpec(memory_space=pltpu.SMEM)
-VMEM = pl.BlockSpec(memory_space=pltpu.VMEM)
-
-
 def cotangents(place, tiles, w_out, queries, cumulative, ends):
     tokens, channels = queries.shape
     width = w_out.shape[1]
@@ -368,13 +430,16 @@
 
 
 def backward_body(
-    queries, keys, values, cumulative, ends, d_mixed, states, back, to_q, to_k, to_v, later,
-    grad_q, grad_k, grad_v, grad_g,
+    queries, keys, values, cumulative, ends, d_mixed, states, back, to_q, to_k, to_v, *refs
 ):
+    *pieces, inside_0, inside_1, book_0, book_1, book, grad_q, grad_k, grad_v, grad_g = refs
+    own = slice(BOOK_OWN, BOOK_OWN + 1)
+    later = weighted([x[...] for x in pieces], [book[k : k + 1, :] for k in range(len(pieces))])
+    later = inside_0[...] + book_0[own, :] * (inside_1[...] + book_1[own, :] * later)
     blocks = back.shape[0]
     scale = queries.shape[1] ** (-0.5)
     upper = triangle(True)
-    after = later[...]
+    after = later
     carry = jnp.sum(after * states[blocks], axis=0, keepdims=True)
     for c in reversed(range(blocks)):
         rows = slice(c * BLK, (c + 1) * BLK)
@@ -397,7 +462,10 @@
         after = after * jnp.exp(end) + back[c]
 
 
-def backward(queries, keys, values, cumulative, ends, d_mixed, states, back, inside, later):
+def backward(
+    queries, keys, values, cumulative, ends, d_mixed, states, back, inside, after, books
+):
+    pieces, insides = after
     return vmem_call(
         backward_body,
         [
@@ -406,68 +474,112 @@
             jax.ShapeDtypeStruct(values.shape, BF16),
             jax.ShapeDtypeStruct(queries.shape, F32),
         ],
-    )(queries, keys, values, cumulative, ends, d_mixed, states, back, *inside, later)
-
-
-def order_weights(logs, index, reverse):
-    count = logs.shape[0]
-    place = lax.rem(index - jnp.arange(count, dtype=jnp.int32) + count, count)
-    row, col = place[:, None], place[None, :]
+    )(queries, keys, values, cumulative, ends, d_mixed, states, back, *inside, *pieces, *insides, *books)
+
+
+BOOK_WHOLE, BOOK_OWN, BOOK_ROWS = 8, 16, 24
+
+
+def stage_weights(logs, index, reverse):
+    count = len(logs)
+    place = [lax.rem(index - k + count, count) for k in range(count)]
+    none = jnp.zeros_like(logs[0])
+
+    def summed(condition):
+        total = none
+        for log, at in zip(logs, place):
+            total = total + jnp.where(condition(at), log, 0.0)
+        return total
+
     if reverse:
-        inner, outer, passed = (col < row) & (col > index), col < row, place > index
+        passed = lambda at: at > index
+        inner = lambda start: lambda at: (at < start) & (at > index)
+        outer = lambda start: lambda at: at < start
     else:
-        inner, outer, passed = (col > row) & (col < index), col > row, place < index
-    masked = lambda mask: jnp.sum(jnp.where(mask[:, :, None], logs[None], 0.0), axis=1)
-    near = jnp.where(passed[:, None], jnp.exp(masked(inner)), 0.0)
-    whole = jnp.exp(masked(outer))
-    own = jnp.exp(jnp.sum(jnp.where(passed[:, None], logs, 0.0), axis=0))
-    return near, whole, own
+        passed = lambda at: at < index
+        inner = lambda start: lambda at: (at > start) & (at < index)
+        outer = lambda start: lambda at: at > start
+    near = [jnp.where(passed(at), jnp.exp(summed(inner(at))), 0.0) for at in place]
+    whole = [jnp.exp(summed(outer(at))) for at in place]
+    return near, whole, jnp.exp(summed(passed))
+
+
+def weighted(pieces, weights):
+    total = pieces[0].astype(F32) * weights[0]
+    for piece, weight in zip(pieces[1:], weights[1:]):
+        total = total + piece.astype(F32) * weight
+    return total
+
+
+def opened(pieces, index, book):
+    width = pieces[0].shape[0] - 8
+    logs = [piece[width : width + 1, :] for piece in pieces]
+    states = [piece[0:width, :] for piece in pieces]
+    near, whole, own = stage_weights(logs, index, True)
+    for k in range(len(logs)):
+        book[k : k + 1, :] = near[k]
+        book[BOOK_WHOLE + k : BOOK_WHOLE + k + 1, :] = whole[k]
+    book[BOOK_OWN : BOOK_OWN + 1, :] = own
+    return states, logs, stage_weights(logs, index, False)
+
+
+def stage_before_body(index, *refs):
+    *pieces, inside, payload, book = refs
+    states, logs, (near, whole, own) = opened(pieces, index[0], book)
+    width = inside.shape[0]
+    book[BOOK_OWN + 1 : BOOK_OWN + 2, :] = own
+    inside[...] = weighted(states, near)
+    payload[0:width, :] = weighted(states, whole)
+    total = logs[0]
+    for log in logs[1:]:
+        total = total + log
+    payload[width:, :] = jnp.where(grid_of((8, total.shape[1]), 0) == 0, total, 0.0)
+
+
+def stage_after_body(*refs):
+    *pieces, book, inside, total = refs
+    pieces = [piece[...] for piece in pieces]
+    inside[...] = weighted(pieces, [book[k : k + 1, :] for k in range(len(pieces))])
+    wholes = [book[BOOK_WHOLE + k : BOOK_WHOLE + k + 1, :] for k in range(len(pieces))]
+    total[...] = weighted(pieces, wholes).astype(BF16)
 
 
 def everyone(x, axis):
     return [x] + [shifted(x, axis, k) for k in range(1, lax.axis_size(axis))]
 
 
-def weighted(pieces, weights):
-    total = 0.0
-    for k, piece in enumerate(pieces):
-        total = total + piece.astype(F32) * weights[k][None, :]
-    return total
-
-
 def states_before(payload):
-    width = payload.shape[0] - 8
-    levels, kept = [], []
+    rows, channels = payload.shape
+    insides, books = [], []
     for axis in reversed(SP):
         pieces = everyone(payload, axis)
-        logs = jnp.stack([piece[width] for piece in pieces])
-        index = lax.axis_index(axis)
-        near, whole, own = order_weights(logs, index, False)
-        states = [piece[:width] for piece in pieces]
-        levels.append((weighted(states, near), own))
-        kept.append(order_weights(logs, index, True))
-        if axis != SP[0]:
-            row = jnp.sum(logs, axis=0)[None]
-            row = jnp.pad(row, ((0, 7), (0, 0)))
-            payload = jnp.concatenate([weighted(states, whole), row], axis=0)
-    return chained(levels), kept
-
-
-def chained(levels):
-    state = levels[-1][0]
-    for inside, own in reversed(levels[:-1]):
-        state = inside + own[None] * state
-    return state
-
-
-def states_after(part, kept):
-    levels = []
-    for axis, (near, whole, own) in zip(reversed(SP), kept):
+        index = lax.axis_index(axis).reshape(1)
+        if axis == SP[0]:
+            return pieces, index, insides, books
+        inside, payload, book = vmem_call(
+            stage_before_body,
+            [
+                jax.ShapeDtypeStruct((rows - 8, channels), F32),
+                jax.ShapeDtypeStruct((rows, channels), F32),
+                jax.ShapeDtypeStruct((BOOK_ROWS, channels), F32),
+            ],
+            in_specs=[SMEM] + [VMEM] * len(pieces),
+        )(index, *pieces)
+        insides.append(inside)
+        books.append(book)
+
+
+def states_after(part, books):
+    insides = []
+    for axis, book in zip(reversed(SP), books):
         pieces = everyone(part, axis)
-        levels.append((weighted(pieces, near), own))
-        if axis != SP[0]:
-            part = weighted(pieces, whole).astype(BF16)
-    return chained(levels)
+        if axis == SP[0]:
+            return pieces, insides
+        inside, part = vmem_call(
+            stage_after_body,
+            [jax.ShapeDtypeStruct(part.shape, F32), jax.ShapeDtypeStruct(part.shape, BF16)],
+        )(*pieces, book)
+        insides.append(inside)
 
 
 def local(
@@ -505,6 +617,7 @@
             jax.ShapeDtypeStruct((experts * cut, tok_rows), BF16),
             jax.ShapeDtypeStruct((2, tok_rows), jnp.int32),
         ],
+        mebibytes=20,
     )(d_out, chosen, weight)
     routed_a = exchanged(outbox_a, cut)
     outbox_b, pick_b = vmem_call(
@@ -513,34 +626,31 @@
             jax.ShapeDtypeStruct((experts * tail, model_width), BF16),
             jax.ShapeDtypeStruct((experts * tail, tok_rows), BF16),
         ],
+        mebibytes=20,
     )(d_out, chosen, weight, ranks)
     routed_b = exchanged(outbox_b, tail)
 
-    rows_in = expert_inputs[0].reshape(experts, capacity, model_width)
-    rows_a = rows_in[:, :cut].reshape(experts * cut, model_width)
-    rows_b = jnp.pad(rows_in[:, cut:], ((0, 0), (0, cut + tail - capacity), (0, 0)))
-    rows_in = jnp.concatenate([rows_a, rows_b.reshape(experts * tail, model_width)], axis=0)
     gate_w, up_w, down_w = w_gate[0].T, w_up[0].T, w_down[0]
-    gate_pre = dot(rows_in, gate_w, NT)
-    up_pre = dot(rows_in, up_w, NT)
-    sigmoid_gate = jax.nn.sigmoid(gate_pre)
-    active = gate_pre * sigmoid_gate
-    hidden = (active * up_pre).astype(BF16)
-    slope = up_pre * sigmoid_gate * (1.0 + gate_pre * (1.0 - sigmoid_gate))
+    rows_in, active, slope, hidden = expert_forward(
+        expert_inputs[0], gate_w, up_w, experts, capacity, cut, tail
+    )
 
     query, key, value, decay = queries[:, 0], keys[:, 0], values[:, 0], log_decay[:, 0]
     cumulative, ends, gain, produced = local_states(key, value, decay)
-    start, kept = states_before(produced)
-    mixed, states, scores = forward(query, key, value, cumulative, ends, gain, start)
+    before = states_before(produced)
+    mixed, states, scores, book = forward(query, key, value, cumulative, ends, gain, before)
+    books = (*before[3], book)
 
     weights = (active, slope, down_w, gate_w, up_w)
-    d_gate, d_up, *parts_a = expert_cotangents(place, routed_a, *weights, 0, ())
-    d_gate, d_up, *parts_b = expert_cotangents(
-        place, routed_b, *weights, experts * cut, (d_gate, d_up)
+    *whole, keep_a, send_a, keep_b, send_b = expert_cotangents(
+        place, routed_a, *weights, 0, ()
+    )
+    parts_a = (keep_a, send_a, keep_b, send_b)
+    routed, d_gate, d_up, *parts_b = expert_cotangents(
+        place, routed_b, *weights, experts * cut, whole
     )
     returned_a = exchanged(summed_over_tp(*parts_a), cut)
     returned_b = exchanged(summed_over_tp(*parts_b), tail)
-    routed = jnp.concatenate([routed_a, routed_b], axis=0)
     grad_gate = dot(d_gate, rows_in, TN).astype(BF16).T
     grad_up = dot(d_up, rows_in, TN).astype(BF16).T
     grad_down = dot(hidden, routed, TN).astype(BF16)
@@ -551,14 +661,15 @@
     tiles = gathered_ring(picked.astype(BF16))
 
     d_mixed, back, own_term = cotangents(place, tiles, w_out, query, cumulative, ends)
-    later = states_after(own_term, kept)
+    after = states_after(own_term, books)
     inside = inside_blocks(query, key, value, cumulative, scores, d_mixed)
     grad_q, grad_k, grad_v, grad_g = backward(
-        query, key, value, cumulative, ends, d_mixed, states, back, inside, later
+        query, key, value, cumulative, ends, d_mixed, states, back, inside, after, books
     )
 
     proj = projection(place, tiles, mixed).reshape(experts, model_width // experts, -1)
-    grad_proj = jnp.sum(lax.all_to_all(proj, SP, 0, 0, tiled=True).astype(F32), axis=0)
+    proj = lax.all_to_all(proj, SP, 0, 0, tiled=True)
+    grad_proj = jnp.sum(proj.astype(F32), axis=0)
     return (
         grad_gate[None],
         grad_up[None],

time: 287 us -> 290 us (1.010)
  the two profiles are of different devices: /device:TPU:1 before, /device:TPU:0 now
where the time goes in v2:
time: 290 us; the launch traced here: 285 us
  waiting for transfers between devices  84.6 us (29%)
  starting transfers between devices  71.6 us (25%)
  Pallas kernels  63.5 us (22%)
  matrix products  29.9 us (10%)
  local copies, waits for them, and re-layouts  20.5 us (7%)
  other arithmetic  13.6 us (5%)
    all_to_all x4, waiting for transfers between devices, exchanged(): box = lax.all_to_all(box, SP, split_axis=0, concat_axis=0, tiled=True)  50 us
    dot_general x5, matrix products, dot(): return lax.dot_general(a, b, dims, preferred_element_type=F32)  29.9 us
    ppermute x18, starting transfers between devices, shifted(): return lax.ppermute(x, axis, [(i, (i + by) % count) for i in range(count)])  26.7 us
    all_to_all x4, starting transfers between devices, exchanged(): box = lax.all_to_all(box, SP, split_axis=0, concat_axis=0, tiled=True)  26.2 us
    pallas_call x2, Pallas kernels, expert_cotangents(): pl.pallas_call(expert_body, grid_spec=pltpu.PrefetchScalarGridSpec(num_sc...  25.2 us
    ppermute x8, waiting for transfers between devices, swapped(): return lax.ppermute(x, 'tp', [(i, i ^ flip) for i in range(count)])  24.2 us
    pallas_call x1, Pallas kernels, expert_forward(): vmem_call(functools.partial(expert_forward_body, experts=experts, capacit...  18.3 us
    unnamed x75, local copies, waits for them, and re-layouts  18.1 us
  transfers between devices with their start and end apart: 31, of which 13 were waited for; matrix products, arithmetic and copies ran while one was open for 15% of the time, Pallas kernels for 21%

profile of v2, /device:TPU:0, one launch (start us, length us, event | category | flops | bytes accessed | tf_op | source)
XLA Modules:
  0.0 285.0 jit_solution(1942742061734197044)
XLA Ops:
  3.6 2.6 shard_map.180
  7.8 8.7 %all-to-all-start.1 = ((bf16[32,24,2048]{2,1,0:T(8,128)(2,1)}), bf16[32,24,2048]{2,1,0:T(8,128)(2,1)}, u32[]{:S(2)}, u32[]{:S(2)}) async-start(bf16[32,24,2048]{2,1,0:T(8,128)(2,1)} %bitcast.77), calls=%async_computation.1 | async-start | bytes 6291456 | tf_op jit(solution)/shard_map/all_to_all | solution.py:610
  20.3 38.2 %all-to-all-done.1 = bf16[32,24,2048]{2,1,0:T(8,128)(2,1)} async-done(((bf16[32,24,2048]{2,1,0:T(8,128)(2,1)}), bf16[32,24,2048]{2,1,0:T(8,128)(2,1)}, u32[]{:S(2)}, u32[]{:S(2)}) %all-to-all-start.1) | async-done | bytes 3145760 | tf_op jit(solution)/shard_map/all_to_all | solution.py:610
  58.5 5.3 %all-to-all-start = ((bf16[32,16,2048]{2,1,0:T(8,128)(2,1)}), bf16[32,16,2048]{2,1,0:T(8,128)(2,1)}, u32[]{:S(2)}, u32[]{:S(2)}) async-start(bf16[32,16,2048]{2,1,0:T(8,128)(2,1)} %bitcast.86), calls=%async_computation | async-start | bytes 4194304 | tf_op jit(solution)/shard_map/all_to_all | solution.py:610
  63.9 18.3 %shard_map.179 = (bf16[1280,2048]{1,0:T(8,128)(2,1)}, bf16[1280,704]{1,0:T(8,128)(2,1)}, bf16[1280,704]{1,0:T(8,128)(2,1)}, bf16[1280,704]{1,0:T(8,128)(2,1)}) custom-call(bf16[1152,2048]{1,0:T(8,128)(2,1)} %bitcast.100, bf16[704,2048]{1,0:T(8,128)(2,1)} %bitcast.92, bf16[704,2048]{1,0:T(8,128)(2,1)} %bitcast.95), custom_call_target="tpu_custom_call" | custom-call | tf_op jit(solution)/shard_map/pallas_call | solution.py:156
  82.2 14.0 %shard_map.182 = (bf16[1280,2048]{1,0:T(8,128)(2,1)}, bf16[1280,704]{1,0:T(8,128)(2,1)}, bf16[1280,704]{1,0:T(8,128)(2,1)}, bf16[2,768,256]{2,1,0:T(8,128)(2,1)}...) custom-call(s32[1]{0:T(128)} %bitcast.5.place, ...), custom_call_target="tpu_custom_call" | custom-call | tf_op jit(solution)/shard_map/pallas_call | solution.py:209
  97.7 2.2 collective-permute-start.2
  99.9 11.2 %shard_map.183 = (bf16[1280,2048]{1,0:T(8,128)(2,1)}, bf16[1280,704]{1,0:T(8,128)(2,1)}, bf16[1280,704]{1,0:T(8,128)(2,1)}, bf16[2,512,256]{2,1,0:T(8,128)(2,1)}...) custom-call(s32[1]{0:T(128)} %bitcast.5.place, ...), custom_call_target="tpu_custom_call", output_to_operand_aliasing={{0}: (7, {}), {1}: (8, {}), {2}: (9, {})} | custom-call | tf_op jit(solution)/shard_map/pallas_call | solution.py:209
  112.4 4.5 %collective-permute-done = bf16[2,768,256]{2,1,0:T(8,128)(2,1)} collective-permute-done((bf16[2,768,256]{2,1,0:T(8,128)(2,1)}, bf16[2,768,256]{2,1,0:T(8,128)(2,1)}, u32[]{:S(2)}, u32[]{:S(2)}) %collective-permute-start) | collective-permute-done | bytes 786464 | tf_op jit(solution)/shard_map/ppermute | solution.py:229
  118.0 2.8 collective-permute-start.1
  122.3 5.8 %collective-permute-done.4 = bf16[2,512,256]{2,1,0:T(8,128)(2,1)S(1)} collective-permute-done((bf16[2,512,256]{2,1,0:T(8,128)(2,1)}, bf16[2,512,256]{2,1,0:T(8,128)(2,1)S(1)}, u32[]{:S(2)}, u32[]{:S(2)}) %collective-permute-start.4) | collective-permute-done | bytes 524320 | tf_op jit(solution)/shard_map/ppermute | solution.py:229
  129.9 2.8 collective-permute-start.5
  132.7 6.6 %collective-permute-done.1 = bf16[768,256]{1,0:T(8,128)(2,1)S(1)} collective-permute-done((bf16[768,256]{1,0:T(8,128)(2,1)S(1)}, bf16[768,256]{1,0:T(8,128)(2,1)S(1)}, u32[]{:S(2)}, u32[]{:S(2)}) %collective-permute-start.1) | collective-permute-done | bytes 393248 | tf_op jit(solution)/shard_map/ppermute | solution.py:229
  142.6 7.6 %all-to-all-start.2 = ((bf16[32,24,512]{2,1,0:T(8,128)(2,1)}), bf16[32,24,512]{2,1,0:T(8,128)(2,1)}, u32[]{:S(2)}, u32[]{:S(2)}) async-start(bf16[32,24,512]{2,1,0:T(8,128)(2,1)} %bitcast.101), calls=%async_computation.2 | async-start | bytes 1572864 | tf_op jit(solution)/shard_map/all_to_all | solution.py:610
  152.6 7.2 %collective-permute-done.7 = bf16[512,256]{1,0:T(8,128)(2,1)S(1)} collective-permute-done((bf16[512,256]{1,0:T(8,128)(2,1)S(1)}, bf16[512,256]{1,0:T(8,128)(2,1)S(1)}, u32[]{:S(2)}, u32[]{:S(2)}) %collective-permute-start.7) | collective-permute-done | bytes 262176 | tf_op jit(solution)/shard_map/ppermute | solution.py:229
  161.8 2.9 %all-to-all-done.2 = bf16[32,24,512]{2,1,0:T(8,128)(2,1)} async-done(((bf16[32,24,512]{2,1,0:T(8,128)(2,1)}), bf16[32,24,512]{2,1,0:T(8,128)(2,1)}, u32[]{:S(2)}, u32[]{:S(2)}) %all-to-all-start.2) | async-done | bytes 786464 | tf_op jit(solution)/shard_map/all_to_all | solution.py:610
  164.7 4.6 %all-to-all-start.3 = ((bf16[32,16,512]{2,1,0:T(8,128)(2,1)}), bf16[32,16,512]{2,1,0:T(8,128)(2,1)}, u32[]{:S(2)}, u32[]{:S(2)}) async-start(bf16[32,16,512]{2,1,0:T(8,128)(2,1)} %bitcast.102), calls=%async_computation.3 | async-start | bytes 1048576 | tf_op jit(solution)/shard_map/all_to_all | solution.py:610
  169.4 2.8 convolution_add_fusion
  172.1 8.8 %all-to-all-done.3 = bf16[32,16,512]{2,1,0:T(8,128)(2,1)} async-done(((bf16[32,16,512]{2,1,0:T(8,128)(2,1)}), bf16[32,16,512]{2,1,0:T(8,128)(2,1)}, u32[]{:S(2)}, u32[]{:S(2)}) %all-to-all-start.3) | async-done | bytes 524320 | tf_op jit(solution)/shard_map/all_to_all | solution.py:610
  183.1 3.2 %collective-permute-start.9 = (bf16[512,512]{1,0:T(8,128)(2,1)S(1)}, bf16[512,512]{1,0:T(8,128)(2,1)S(1)}, u32[]{:S(2)}, u32[]{:S(2)}) collective-permute-start(bf16[512,512]{1,0:T(8,128)(2,1)S(1)} %fusion.3.a), channel_id=1, source_target_pairs={{0,3},{1,0},{2,1},{3,2},{4,7},{5,4},{6,5},{7,6},{8,11},{9,8},{10,9... | collective-permute-start | bytes 1572872 | tf_op jit(solution)/shard_map/ppermute | solution.py:252
  199.6 3.2 %collective-permute-start.11 = (bf16[256,512]{1,0:T(8,128)(2,1)}, bf16[256,512]{1,0:T(8,128)(2,1)}, u32[]{:S(2)}, u32[]{:S(2)}) collective-permute-start(bf16[256,512]{1,0:T(8,128)(2,1)} %slice.81), channel_id=1, source_target_pairs={{0,3},{1,0},{2,1},{3,2},{4,7},{5,4},{6,5},{7,6},{8,11},{9,8},{10,9... | collective-permute-start | bytes 786440 | tf_op jit(solution)/shard_map/ppermute | solution.py:252
  209.6 4.5 %collective-permute-done.16.refs_1_ = f32[264,128]{1,0:T(8,128)S(1)} collective-permute-done((f32[264,128]{1,0:T(8,128)}, f32[264,128]{1,0:T(8,128)S(1)}, u32[]{:S(2)}, u32[]{:S(2)}) %collective-permute-start.16) | collective-permute-done | bytes 135200 | tf_op jit(solution)/shard_map/ppermute | solution.py:252
  217.9 2.3 shard_map.187
  224.5 2.0 shard_map.189
  227.6 8.1 %fusion.1 = bf16[1,2048,704]{1,2,0:T(8,128)(2,1)} fusion(bf16[1280,2048]{1,0:T(8,128)(2,1)} %get-tuple-element.59, bf16[1280,704]{1,0:T(8,128)(2,1)S(1)} %copy-done.32), kind=kOutput, calls=%fused_computation.4 | convolution fusion | flops 3692429312 | bytes 9928704 | tf_op jit(solution)/shard_map/dot_general | solution.py:24
  237.5 7.7 %all-to-all-start.4 = ((bf16[32,64,256]{2,1,0:T(8,128)(2,1)}), bf16[32,64,256]{2,1,0:T(8,128)(2,1)}, u32[]{:S(2)}, u32[]{:S(2)}) async-start(bf16[32,64,256]{2,1,0:T(8,128)(2,1)} %bitcast.37), calls=%async_computation.4 | async-start | bytes 2097152 | tf_op jit(solution)/shard_map/all_to_all | solution.py:671
  247.8 2.7 collective-permute-start.21
  252.0 8.8 %fusion = bf16[1,2048,704]{1,2,0:T(8,128)(2,1)} fusion(bf16[1280,2048]{1,0:T(8,128)(2,1)} %get-tuple-element.59, bf16[1280,704]{1,0:T(8,128)(2,1)} %get-tuple-element.68), kind=kOutput, calls=%fused_computation.3 | convolution fusion | flops 3692429312 | bytes 9928704 | tf_op jit(solution)/shard_map/dot_general | solution.py:24
  265.0 2.7 collective-permute-start.24
  269.5 8.3 %fusion.2 = bf16[1,704,2048]{2,1,0:T(8,128)(2,1)} fusion(bf16[1280,704]{1,0:T(8,128)(2,1)S(1)} %copy-done.36, bf16[1280,2048]{1,0:T(8,128)(2,1)} %get-tuple-element.71), kind=kOutput, calls=%fused_computation.5 | convolution fusion | flops 3692429312 | bytes 9928704 | tf_op jit(solution)/shard_map/dot_general | solution.py:24
  277.7 2.0 shard_map.190
  279.8 2.9 %shard_map.193 = (bf16[512,128]{1,0:T(8,128)(2,1)}, bf16[512,128]{1,0:T(8,128)(2,1)}, bf16[512,256]{1,0:T(8,128)(2,1)}, f32[512,128]{1,0:T(8,128)}) custom-call(bf16[512,128]{1,0:T(8,128)(2,1)S(1)} %bitcast.81, bf16[512,128]{1,0:T(8,128)(2,1)S(1)} %bitcast.85, bf16[512,256]{1,0:T(8,128)(2,1)S(1)} %bitcast.76, f32[512,128]{1,0:T(8,128)S(1)} %get-tuple-element.82.cumulative, ...), custom_call_target="tpu_custom_call" | custom-call | tf_op jit(solution)/shard_map/pallas_call | solution.py:469
  (139 shorter events, 68.3 us)
Async XLA Ops:
  7.8 50.7 %all-to-all-start.1 = ((bf16[32,24,2048]{2,1,0:T(8,128)(2,1)}), bf16[32,24,2048]{2,1,0:T(8,128)(2,1)}, u32[]{:S(2)}, u32[]{:S(2)}) async-start(bf16[32,24,2048]{2,1,0:T(8,128)(2,1)} %bitcast.77), calls=%async_computation.1 | async-start | bytes 6291456 | tf_op jit(solution)/shard_map/all_to_all | solution.py:610
  58.5 41.4 %all-to-all-start = ((bf16[32,16,2048]{2,1,0:T(8,128)(2,1)}), bf16[32,16,2048]{2,1,0:T(8,128)(2,1)}, u32[]{:S(2)}, u32[]{:S(2)}) async-start(bf16[32,16,2048]{2,1,0:T(8,128)(2,1)} %bitcast.86), calls=%async_computation | async-start | bytes 4194304 | tf_op jit(solution)/shard_map/all_to_all | solution.py:610
  96.2 20.7 %collective-permute-start = (bf16[2,768,256]{2,1,0:T(8,128)(2,1)}, bf16[2,768,256]{2,1,0:T(8,128)(2,1)}, u32[]{:S(2)}, u32[]{:S(2)}) collective-permute-start(bf16[2,768,256]{2,1,0:T(8,128)(2,1)} %get-tuple-element.74), channel_id=1, source_target_pairs={{0,1},{1,0},{2,3},{3,2},{4,5},{5,4},{6,7},{7,6},{8,9},{9,8},{10,11... | collective-permute-start | bytes 2359304 | tf_op jit(solution)/shard_map/ppermute | solution.py:229
  97.7 23.2 %collective-permute-start.2 = (bf16[2,768,256]{2,1,0:T(8,128)(2,1)}, bf16[2,768,256]{2,1,0:T(8,128)(2,1)}, u32[]{:S(2)}, u32[]{:S(2)}) collective-permute-start(bf16[2,768,256]{2,1,0:T(8,128)(2,1)} %get-tuple-element.76), channel_id=1, source_target_pairs={{0,3},{1,2},{2,1},{3,0},{4,7},{5,6},{6,5},{7,4},{8,11},{9,10},{10,... | collective-permute-start | bytes 2359304 | tf_op jit(solution)/shard_map/ppermute | solution.py:229
  111.1 17.0 %collective-permute-start.4 = (bf16[2,512,256]{2,1,0:T(8,128)(2,1)}, bf16[2,512,256]{2,1,0:T(8,128)(2,1)S(1)}, u32[]{:S(2)}, u32[]{:S(2)}) collective-permute-start(bf16[2,512,256]{2,1,0:T(8,128)(2,1)} %get-tuple-element.79), channel_id=1, source_target_pairs={{0,1},{1,0},{2,3},{3,2},{4,5},{5,4},{6,7},{7,6},{8,9},{9,8},{10,11... | collective-permute-start | bytes 1572872 | tf_op jit(solution)/shard_map/ppermute | solution.py:229
  111.7 38.5 %collective-permute-start.6 = (bf16[2,512,256]{2,1,0:T(8,128)(2,1)}, bf16[2,512,256]{2,1,0:T(8,128)(2,1)}, u32[]{:S(2)}, u32[]{:S(2)}) collective-permute-start(bf16[2,512,256]{2,1,0:T(8,128)(2,1)} %get-tuple-element.81), channel_id=1, source_target_pairs={{0,3},{1,2},{2,1},{3,0},{4,7},{5,6},{6,5},{7,4},{8,11},{9,10},{10,... | collective-permute-start | bytes 1572872 | tf_op jit(solution)/shard_map/ppermute | solution.py:229
  118.0 21.3 %collective-permute-start.1 = (bf16[768,256]{1,0:T(8,128)(2,1)S(1)}, bf16[768,256]{1,0:T(8,128)(2,1)S(1)}, u32[]{:S(2)}, u32[]{:S(2)}) collective-permute-start(bf16[768,256]{1,0:T(8,128)(2,1)S(1)} %fusion.8), channel_id=1, source_target_pairs={{0,3},{1,2},{2,1},{3,0},{4,7},{5,6},{6,5},{7,4},{8,11},{9,10},{10,... | collective-permute-start | bytes 1179656 | tf_op jit(solution)/shard_map/ppermute | solution.py:229
  122.0 18.5 %collective-permute-start.3 = (bf16[768,256]{1,0:T(8,128)(2,1)S(1)}, bf16[768,256]{1,0:T(8,128)(2,1)S(1)}, u32[]{:S(2)}, u32[]{:S(2)}) collective-permute-start(bf16[768,256]{1,0:T(8,128)(2,1)S(1)} %fusion.9), channel_id=1, source_target_pairs={{0,1},{1,0},{2,3},{3,2},{4,5},{5,4},{6,7},{7,6},{8,9},{9,8},{10,11... | collective-permute-start | bytes 1179656 | tf_op jit(solution)/shard_map/ppermute | solution.py:229
  129.9 21.5 %collective-permute-start.5 = (bf16[512,256]{1,0:T(8,128)(2,1)}, bf16[512,256]{1,0:T(8,128)(2,1)}, u32[]{:S(2)}, u32[]{:S(2)}) collective-permute-start(bf16[512,256]{1,0:T(8,128)(2,1)} %fusion.10), channel_id=1, source_target_pairs={{0,3},{1,2},{2,1},{3,0},{4,7},{5,6},{6,5},{7,4},{8,11},{9,10},{10,... | collective-permute-start | bytes 786440 | tf_op jit(solution)/shard_map/ppermute | solution.py:229
  142.6 22.1 %all-to-all-start.2 = ((bf16[32,24,512]{2,1,0:T(8,128)(2,1)}), bf16[32,24,512]{2,1,0:T(8,128)(2,1)}, u32[]{:S(2)}, u32[]{:S(2)}) async-start(bf16[32,24,512]{2,1,0:T(8,128)(2,1)} %bitcast.101), calls=%async_computation.2 | async-start | bytes 1572864 | tf_op jit(solution)/shard_map/all_to_all | solution.py:610
  151.3 8.5 %collective-permute-start.7 = (bf16[512,256]{1,0:T(8,128)(2,1)S(1)}, bf16[512,256]{1,0:T(8,128)(2,1)S(1)}, u32[]{:S(2)}, u32[]{:S(2)}) collective-permute-start(bf16[512,256]{1,0:T(8,128)(2,1)S(1)} %fusion.11), channel_id=1, source_target_pairs={{0,1},{1,0},{2,3},{3,2},{4,5},{5,4},{6,7},{7,6},{8,9},{9,8},{10,11... | collective-permute-start | bytes 786440 | tf_op jit(solution)/shard_map/ppermute | solution.py:229
  164.7 16.2 %all-to-all-start.3 = ((bf16[32,16,512]{2,1,0:T(8,128)(2,1)}), bf16[32,16,512]{2,1,0:T(8,128)(2,1)}, u32[]{:S(2)}, u32[]{:S(2)}) async-start(bf16[32,16,512]{2,1,0:T(8,128)(2,1)} %bitcast.102), calls=%async_computation.3 | async-start | bytes 1048576 | tf_op jit(solution)/shard_map/all_to_all | solution.py:610
  172.1 42.6 %copy-start.4 = (bf16[512,1,128]{2,0,1:T(8,128)(2,1)S(1)}, bf16[512,1,128]{2,0,1:T(8,128)(2,1)}, u32[]{:S(2)}) copy-start(bf16[512,1,128]{2,0,1:T(8,128)(2,1)} %param.20) | copy-start | bytes 393220
  182.9 15.2 %collective-permute-start.8 = (bf16[512,512]{1,0:T(8,128)(2,1)S(1)}, bf16[512,512]{1,0:T(8,128)(2,1)S(1)}, u32[]{:S(2)}, u32[]{:S(2)}) collective-permute-start(bf16[512,512]{1,0:T(8,128)(2,1)S(1)} %fusion.3.a), channel_id=1, source_target_pairs={{0,1},{1,2},{2,3},{3,0},{4,5},{5,6},{6,7},{7,4},{8,9},{9,10},{10,1... | collective-permute-start | bytes 1572872 | tf_op jit(solution)/shard_map/ppermute | solution.py:252
  183.1 15.8 %collective-permute-start.9 = (bf16[512,512]{1,0:T(8,128)(2,1)S(1)}, bf16[512,512]{1,0:T(8,128)(2,1)S(1)}, u32[]{:S(2)}, u32[]{:S(2)}) collective-permute-start(bf16[512,512]{1,0:T(8,128)(2,1)S(1)} %fusion.3.a), channel_id=1, source_target_pairs={{0,3},{1,0},{2,1},{3,2},{4,7},{5,4},{6,5},{7,6},{8,11},{9,8},{10,9... | collective-permute-start | bytes 1572872 | tf_op jit(solution)/shard_map/ppermute | solution.py:252
  188.9 1.5 collective-permute-start.12
  192.3 10.5 %collective-permute-start.13 = (f32[264,128]{1,0:T(8,128)S(1)}, f32[264,128]{1,0:T(8,128)}, u32[]{:S(2)}, u32[]{:S(2)}) collective-permute-start(f32[264,128]{1,0:T(8,128)S(1)} %get-tuple-element.86.refs_0_), channel_id=1, source_target_pairs={{0,8},{8,16},{16,24},{24,0},{1,9},{9,17},{17,25},{25,1},{2,10},{10... | collective-permute-start | bytes 405512 | tf_op jit(solution)/shard_map/ppermute | solution.py:252
  192.9 9.9 %collective-permute-start.14 = (f32[264,128]{1,0:T(8,128)S(1)}, f32[264,128]{1,0:T(8,128)}, u32[]{:S(2)}, u32[]{:S(2)}) collective-permute-start(f32[264,128]{1,0:T(8,128)S(1)} %get-tuple-element.86.refs_0_), channel_id=1, source_target_pairs={{0,16},{8,24},{16,0},{24,8},{1,17},{9,25},{17,1},{25,9},{2,18},{10... | collective-permute-start | bytes 405512 | tf_op jit(solution)/shard_map/ppermute | solution.py:252
  194.7 8.2 %collective-permute-start.15 = (f32[264,128]{1,0:T(8,128)S(1)}, f32[264,128]{1,0:T(8,128)}, u32[]{:S(2)}, u32[]{:S(2)}) collective-permute-start(f32[264,128]{1,0:T(8,128)S(1)} %get-tuple-element.86.refs_0_), channel_id=1, source_target_pairs={{0,24},{8,0},{16,8},{24,16},{1,25},{9,1},{17,9},{25,17},{2,26},{10... | collective-permute-start | bytes 405512 | tf_op jit(solution)/shard_map/ppermute | solution.py:252
  198.9 22.4 %collective-permute-start.10 = (bf16[256,512]{1,0:T(8,128)(2,1)}, bf16[256,512]{1,0:T(8,128)(2,1)}, u32[]{:S(2)}, u32[]{:S(2)}) collective-permute-start(bf16[256,512]{1,0:T(8,128)(2,1)} %slice.80), channel_id=1, source_target_pairs={{0,1},{1,2},{2,3},{3,0},{4,5},{5,6},{6,7},{7,4},{8,9},{9,10},{10,1... | collective-permute-start | bytes 786440 | tf_op jit(solution)/shard_map/ppermute | solution.py:252
  199.6 22.7 %collective-permute-start.11 = (bf16[256,512]{1,0:T(8,128)(2,1)}, bf16[256,512]{1,0:T(8,128)(2,1)}, u32[]{:S(2)}, u32[]{:S(2)}) collective-permute-start(bf16[256,512]{1,0:T(8,128)(2,1)} %slice.81), channel_id=1, source_target_pairs={{0,3},{1,0},{2,1},{3,2},{4,7},{5,4},{6,5},{7,6},{8,11},{9,8},{10,9... | collective-permute-start | bytes 786440 | tf_op jit(solution)/shard_map/ppermute | solution.py:252
  205.3 8.9 %collective-permute-start.16 = (f32[264,128]{1,0:T(8,128)}, f32[264,128]{1,0:T(8,128)S(1)}, u32[]{:S(2)}, u32[]{:S(2)}) collective-permute-start(f32[264,128]{1,0:T(8,128)} %get-tuple-element.87.refs_0_), channel_id=1, source_target_pairs={{0,32},{32,64},{64,96},{96,0},{1,33},{33,65},{65,97},{97,1},{2,34}... | collective-permute-start | bytes 405512 | tf_op jit(solution)/shard_map/ppermute | solution.py:252
  205.9 8.3 %collective-permute-start.17 = (f32[264,128]{1,0:T(8,128)}, f32[264,128]{1,0:T(8,128)}, u32[]{:S(2)}, u32[]{:S(2)}) collective-permute-start(f32[264,128]{1,0:T(8,128)} %get-tuple-element.87.refs_0_), channel_id=1, source_target_pairs={{0,64},{32,96},{64,0},{96,32},{1,65},{33,97},{65,1},{97,33},{2,66}... | collective-permute-start | bytes 405512 | tf_op jit(solution)/shard_map/ppermute | solution.py:252
  207.8 6.9 %collective-permute-start.18 = (f32[264,128]{1,0:T(8,128)}, f32[264,128]{1,0:T(8,128)}, u32[]{:S(2)}, u32[]{:S(2)}) collective-permute-start(f32[264,128]{1,0:T(8,128)} %get-tuple-element.87.refs_0_), channel_id=1, source_target_pairs={{0,96},{32,0},{64,32},{96,64},{1,97},{33,1},{65,33},{97,65},{2,98}... | collective-permute-start | bytes 405512 | tf_op jit(solution)/shard_map/ppermute | solution.py:252
  227.6 17.5 %collective-permute-start.19 = (bf16[256,128]{1,0:T(8,128)(2,1)S(1)}, bf16[256,128]{1,0:T(8,128)(2,1)}, u32[]{:S(2)}, u32[]{:S(2)}) collective-permute-start(bf16[256,128]{1,0:T(8,128)(2,1)S(1)} %get-tuple-element.100.refs_0_), channel_id=1, source_target_pairs={{0,4},{4,0},{1,5},{5,1},{2,6},{6,2},{3,7},{7,3},{8,12},{12,8},{9,1... | collective-permute-start | bytes 196616 | tf_op jit(solution)/shard_map/ppermute | solution.py:252
  237.5 45.3 %all-to-all-start.4 = ((bf16[32,64,256]{2,1,0:T(8,128)(2,1)}), bf16[32,64,256]{2,1,0:T(8,128)(2,1)}, u32[]{:S(2)}, u32[]{:S(2)}) async-start(bf16[32,64,256]{2,1,0:T(8,128)(2,1)} %bitcast.37), calls=%async_computation.4 | async-start | bytes 2097152 | tf_op jit(solution)/shard_map/all_to_all | solution.py:671
  246.0 15.8 %collective-permute-start.20 = (bf16[256,128]{1,0:T(8,128)(2,1)S(1)}, bf16[256,128]{1,0:T(8,128)(2,1)S(1)}, u32[]{:S(2)}, u32[]{:S(2)}) collective-permute-start(bf16[256,128]{1,0:T(8,128)(2,1)S(1)} %get-tuple-element.101.refs_0_), channel_id=1, source_target_pairs={{0,8},{8,16},{16,24},{24,0},{1,9},{9,17},{17,25},{25,1},{2,10},{10... | collective-permute-start | bytes 196616 | tf_op jit(solution)/shard_map/ppermute | solution.py:252
  247.8 15.7 %collective-permute-start.21 = (bf16[256,128]{1,0:T(8,128)(2,1)S(1)}, bf16[256,128]{1,0:T(8,128)(2,1)S(1)}, u32[]{:S(2)}, u32[]{:S(2)}) collective-permute-start(bf16[256,128]{1,0:T(8,128)(2,1)S(1)} %get-tuple-element.101.refs_0_), channel_id=1, source_target_pairs={{0,16},{8,24},{16,0},{24,8},{1,17},{9,25},{17,1},{25,9},{2,18},{10... | collective-permute-start | bytes 196616 | tf_op jit(solution)/shard_map/ppermute | solution.py:252
  250.5 13.0 %collective-permute-start.22 = (bf16[256,128]{1,0:T(8,128)(2,1)S(1)}, bf16[256,128]{1,0:T(8,128)(2,1)S(1)}, u32[]{:S(2)}, u32[]{:S(2)}) collective-permute-start(bf16[256,128]{1,0:T(8,128)(2,1)S(1)} %get-tuple-element.101.refs_0_), channel_id=1, source_target_pairs={{0,24},{8,0},{16,8},{24,16},{1,25},{9,1},{17,9},{25,17},{2,26},{10... | collective-permute-start | bytes 196616 | tf_op jit(solution)/shard_map/ppermute | solution.py:252
  263.6 16.2 %collective-permute-start.23 = (bf16[256,128]{1,0:T(8,128)(2,1)S(1)}, bf16[256,128]{1,0:T(8,128)(2,1)S(1)}, u32[]{:S(2)}, u32[]{:S(2)}) collective-permute-start(bf16[256,128]{1,0:T(8,128)(2,1)S(1)} %get-tuple-element.102.refs_0_), channel_id=1, source_target_pairs={{0,32},{32,64},{64,96},{96,0},{1,33},{33,65},{65,97},{97,1},{2,34}... | collective-permute-start | bytes 196616 | tf_op jit(solution)/shard_map/ppermute | solution.py:252
  265.0 14.7 %collective-permute-start.24 = (bf16[256,128]{1,0:T(8,128)(2,1)S(1)}, bf16[256,128]{1,0:T(8,128)(2,1)S(1)}, u32[]{:S(2)}, u32[]{:S(2)}) collective-permute-start(bf16[256,128]{1,0:T(8,128)(2,1)S(1)} %get-tuple-element.102.refs_0_), channel_id=1, source_target_pairs={{0,64},{32,96},{64,0},{96,32},{1,65},{33,97},{65,1},{97,33},{2,66}... | collective-permute-start | bytes 196616 | tf_op jit(solution)/shard_map/ppermute | solution.py:252
  267.8 12.0 %collective-permute-start.25 = (bf16[256,128]{1,0:T(8,128)(2,1)S(1)}, bf16[256,128]{1,0:T(8,128)(2,1)S(1)}, u32[]{:S(2)}, u32[]{:S(2)}) collective-permute-start(bf16[256,128]{1,0:T(8,128)(2,1)S(1)} %get-tuple-element.102.refs_0_), channel_id=1, source_target_pairs={{0,96},{32,0},{64,32},{96,64},{1,97},{33,1},{65,33},{97,65},{2,98}... | collective-permute-start | bytes 196616 | tf_op jit(solution)/shard_map/ppermute | solution.py:252
  (36 other events, 208.8 us)

commit v3 on v2

--- a/solution.py
+++ b/solution.py
@@ -66,21 +66,17 @@
     return pl.pallas_call(kernel, out_shape=outs, compiler_params=limit(mebibytes), **options)
 
 
-def fill_outbox(d_out, weight, slot_a, slot_b, outbox, pick):
-    slots, tokens = pick.shape
+def fill_outbox(rows, weight, slot_a, slot_b, outbox):
     weights_a = jnp.concatenate(thirds(weight[0:1, :]), axis=0)
     weights_b = jnp.concatenate(thirds(weight[1:2, :]), axis=0)
-    rows = d_out[...]
     step = 256
-    for start in range(0, slots, step):
-        slot = grid_of((step, tokens), 0) + start
+    for start in range(0, outbox.shape[0], step):
+        slot = grid_of((step, rows.shape[0]), 0) + start
         one_a = jnp.where(slot == slot_a, 1.0, 0.0).astype(BF16)
         one_b = jnp.where(slot == slot_b, 1.0, 0.0).astype(BF16)
-        both = one_a + one_b
         factor = dot(one_a, weights_a, NT) + dot(one_b, weights_b, NT)
         factor = jnp.sum(factor, axis=1, keepdims=True)
-        pick[start : start + step, :] = both
-        outbox[start : start + step, :] = (dot(both, rows, NN) * factor).astype(BF16)
+        outbox[start : start + step, :] = (dot(one_a + one_b, rows, NN) * factor).astype(BF16)
 
 
 def slots_of(chosen, ranks, least, most, stride):
@@ -88,7 +84,7 @@
     return jnp.where(inside, chosen * stride + ranks - least, -1)
 
 
-def route_body(d_out, chosen, weight, outbox, pick, ranks, *, experts, most, stride):
+def route_body(place, d_out, chosen, weight, outbox, ranks, *, experts, most):
     tokens = d_out.shape[0]
     first, second = chosen[0:1, :], chosen[1:2, :]
     ids = grid_of((experts, tokens), 0)
@@ -102,15 +98,26 @@
     rank_b = jnp.sum(jnp.where(is_second, before, 0.0), axis=0, keepdims=True).astype(jnp.int32)
     ranks[0:1, :] = rank_a
     ranks[1:2, :] = rank_b
-    slot_a = slots_of(first, rank_a, 0, most, stride)
-    slot_b = slots_of(second, rank_b, 0, most, stride)
-    fill_outbox(d_out, weight, slot_a, slot_b, outbox, pick)
-
-
-def refill_body(d_out, chosen, weight, ranks, outbox, pick, *, least, most, stride):
-    slot_a = slots_of(chosen[0:1, :], ranks[0:1, :], least, most, stride)
-    slot_b = slots_of(chosen[1:2, :], ranks[1:2, :], least, most, stride)
-    fill_outbox(d_out, weight, slot_a, slot_b, outbox, pick)
+    slot_a = slots_of(first, rank_a, 0, most, most)
+    slot_b = slots_of(second, rank_b, 0, most, most)
+    width = outbox.shape[1]
+    rows = d_out[:, pl.ds(pl.multiple_of(place[0] * width, width), width)]
+    fill_outbox(rows, weight, slot_a, slot_b, outbox)
+
+
+def refill_body(d_out, chosen, weight, ranks, outbox, pick, *, least, most, tail):
+    first, second = chosen[0:1, :], chosen[1:2, :]
+    rank_a, rank_b = ranks[0:1, :], ranks[1:2, :]
+    slot_a = slots_of(first, rank_a, least, most, tail)
+    slot_b = slots_of(second, rank_b, least, most, tail)
+    fill_outbox(d_out[...], weight, slot_a, slot_b, outbox)
+    slot_a = first * (least + tail) + rank_a
+    slot_b = second * (least + tail) + rank_b
+    step = 256
+    for start in range(0, pick.shape[0], step):
+        slot = grid_of((step, pick.shape[1]), 0) + start
+        found = (slot == slot_a) | (slot == slot_b)
+        pick[start : start + step, :] = jnp.where(found, 1.0, 0.0).astype(BF16)
 
 
 def slot_order(group, capacity, cut, tail):
@@ -163,10 +170,35 @@
     )(inputs, gate_w, up_w)
 
 
-def expert_body(place, routed, active, slope, down_w, gate_w, up_w, *refs):
-    routed_out, d_gate, d_up, keep_a, send_a, keep_b, send_b = refs[-7:]
-    routed_out[...] = routed[...]
-    d_hidden = dot(routed[...], down_w[...], NT)
+def expert_body(place, *refs, tiles):
+    routed, (active, slope, down_w, gate_w, up_w) = refs[:tiles], refs[tiles : tiles + 5]
+    routed_out, d_gate, d_up, keep_a, send_a, keep_b, send_b = refs[-11:-4]
+    down_v, gate_v, up_v, loaded = refs[-4:]
+    copies = [
+        pltpu.make_async_copy(source, target, loaded.at[i])
+        for i, (source, target) in enumerate(((down_w, down_v), (gate_w, gate_v), (up_w, up_v)))
+    ]
+
+    @pl.when(pl.program_id(0) == 0)
+    def _():
+        for copy in copies:
+            copy.start()
+        copies[0].wait()
+
+    d_hidden = 0.0
+    for k, tile in enumerate(routed):
+        wide = tile.shape[1]
+        cols = slice(None)
+        if tiles > 1:
+            cols = pl.ds(pl.multiple_of(((place[0] + tiles - k) & (tiles - 1)) * wide, wide), wide)
+        routed_out[:, cols] = tile[...]
+        d_hidden = d_hidden + dot(tile[...], down_v[:, cols], NT)
+
+    @pl.when(pl.program_id(0) == 0)
+    def _():
+        copies[1].wait()
+        copies[2].wait()
+
     to_gate = (d_hidden * slope[...].astype(F32)).astype(BF16)
     to_up = (d_hidden * active[...].astype(F32)).astype(BF16)
     d_gate[...] = to_gate
@@ -181,33 +213,29 @@
     for k, (home_a, home_b) in enumerate(homes):
         start = pl.multiple_of((place[0] ^ k) * (2 * half), 2 * half)
         cols = pl.ds(start, 2 * half)
-        term = dot(to_gate, gate_w[:, cols], NN) + dot(to_up, up_w[:, cols], NN)
+        term = dot(to_gate, gate_v[:, cols], NN) + dot(to_up, up_v[:, cols], NN)
         term = term.astype(BF16)
         home_a[0][home_a[1]] = term[:, :half]
         home_b[0][home_b[1]] = term[:, half:]
 
 
 def expert_cotangents(place, routed, active, slope, down_w, gate_w, up_w, first_row, earlier):
-    rows, width = routed.shape
-    units = down_w.shape[0]
+    rows, wide = routed[0].shape
+    tiles = len(routed)
+    units, width = down_w.shape
     step = 256
     half = width // 8
     skipped = first_row // step
     by_row = lambda i, *_: (i, 0)
     later_row = lambda i, *_: (i + skipped, 0)
-    whole = lambda i, *_: (0, 0)
-    in_specs = [
-        pl.BlockSpec((step, width), by_row),
+    in_specs = [pl.BlockSpec((step, wide), by_row)] * tiles + [
         pl.BlockSpec((step, units), later_row),
         pl.BlockSpec((step, units), later_row),
-        pl.BlockSpec((units, width), whole),
-        pl.BlockSpec((units, width), whole),
-        pl.BlockSpec((units, width), whole),
     ]
-    in_specs += [pl.BlockSpec(memory_space=pl.ANY)] * len(earlier)
+    in_specs += [pl.BlockSpec(memory_space=pl.ANY)] * (3 + len(earlier))
     pair = pl.BlockSpec((2, step, half), lambda i, *_: (0, i, 0))
     return pl.pallas_call(
-        expert_body,
+        functools.partial(expert_body, tiles=tiles),
         grid_spec=pltpu.PrefetchScalarGridSpec(
             num_scalar_prefetch=1,
             grid=(rows // step,),
@@ -215,13 +243,37 @@
             out_specs=[pl.BlockSpec((step, width), later_row)]
             + [pl.BlockSpec((step, units), later_row)] * 2
             + [pair] * 4,
+            scratch_shapes=[pltpu.VMEM((units, width), BF16)] * 3
+            + [pltpu.SemaphoreType.DMA((3,))],
         ),
         out_shape=[jax.ShapeDtypeStruct((active.shape[0], width), BF16)]
         + [jax.ShapeDtypeStruct(active.shape, BF16)] * 2
         + [jax.ShapeDtypeStruct((2, rows, half), BF16)] * 4,
-        input_output_aliases={7 + i: i for i in range(len(earlier))},
+        input_output_aliases={6 + tiles + i: i for i in range(len(earlier))},
         compiler_params=limit(56),
-    )(place, routed, active, slope, down_w, gate_w, up_w, *earlier)
+    )(place, *routed, active, slope, down_w, gate_w, up_w, *earlier)
+
+
+def weight_grads_body(d_gate, d_up, rows_in, for_gate, for_up):
+    rows = rows_in[...]
+    for_gate[...] = dot(d_gate[...], rows, TN).astype(BF16)
+    for_up[...] = dot(d_up[...], rows, TN).astype(BF16)
+
+
+def weight_grads(d_gate, d_up, rows_in):
+    rows, width = rows_in.shape
+    units = d_gate.shape[1]
+    step = 512
+    whole = pl.BlockSpec((rows, units), lambda i: (0, 0))
+    by_col = lambda i: (0, i)
+    return pl.pallas_call(
+        weight_grads_body,
+        grid=(width // step,),
+        in_specs=[whole, whole, pl.BlockSpec((rows, step), by_col)],
+        out_specs=[pl.BlockSpec((units, step), by_col)] * 2,
+        out_shape=[jax.ShapeDtypeStruct((units, width), BF16)] * 2,
+        compiler_params=limit(48),
+    )(d_gate, d_up, rows_in)
 
 
 def swapped(x, flip):
@@ -234,6 +286,27 @@
     for term in terms[1:]:
         total = total + term.astype(F32)
     return total.astype(BF16)
+
+
+def final_sum_body(keep_a, got_a, last_a, keep_b, got_b, last_b, out):
+    half = keep_a.shape[2]
+    for start, keep, got, last in ((0, keep_a, got_a, last_a), (half, keep_b, got_b, last_b)):
+        total = keep[0].astype(F32) + got[0].astype(F32) + last[...].astype(F32)
+        out[:, start : start + half] = total.astype(BF16)
+
+
+def final_sum(keep_a, got_a, last_a, keep_b, got_b, last_b):
+    _, rows, half = keep_a.shape
+    first = pl.BlockSpec((1, rows, half), lambda i: (0, 0, 0))
+    whole = pl.BlockSpec((rows, half), lambda i: (0, 0))
+    return pl.pallas_call(
+        final_sum_body,
+        grid=(1,),
+        in_specs=[first, first, whole] * 2,
+        out_specs=pl.BlockSpec((rows, 2 * half), lambda i: (0, 0)),
+        out_shape=jax.ShapeDtypeStruct((rows, 2 * half), BF16),
+        compiler_params=limit(12),
+    )(keep_a, got_a, last_a, keep_b, got_b, last_b)
 
 
 def summed_over_tp(keep_a, send_a, keep_b, send_b):
@@ -242,9 +315,7 @@
     last_a, last_b = plus(keep_a[1], got_a[1]), plus(keep_b[1], got_b[1])
     last_a = swapped(last_a, 3)
     last_b = swapped(last_b, 1)
-    return jnp.concatenate(
-        [plus(keep_a[0], got_a[0], last_a), plus(keep_b[0], got_b[0], last_b)], axis=1
-    )
+    return final_sum(keep_a, got_a, last_a, keep_b, got_b, last_b)
 
 
 def shifted(x, axis, by):
@@ -599,36 +670,42 @@
     tok_rows, model_width = d_out.shape
     experts = lax.axis_size(SP)
     capacity = expert_inputs.shape[1] // experts
-    cut = capacity * 2 // 3 // PAD * PAD
+    cut = PAD * 2
     tail = -(-(capacity - cut) // PAD) * PAD
+    slots = experts * (cut + tail)
     quarter = model_width // lax.axis_size("tp")
     place = lax.axis_index("tp").reshape(1)
     chosen, weight = route_expert.T, route_weight.T
 
-    def exchanged(box, stride):
-        box = box.reshape(experts, stride, box.shape[1])
+    def exchanged(box):
+        rows, width = box.shape
+        box = box.reshape(experts, rows // experts, width)
         box = lax.all_to_all(box, SP, split_axis=0, concat_axis=0, tiled=True)
-        return box.reshape(experts * stride, box.shape[2])
-
-    outbox_a, pick_a, ranks = vmem_call(
-        functools.partial(route_body, experts=experts, most=cut, stride=cut),
+        return box.reshape(rows, width)
+
+    outbox_q, ranks = vmem_call(
+        functools.partial(route_body, experts=experts, most=cut),
         [
-            jax.ShapeDtypeStruct((experts * cut, model_width), BF16),
-            jax.ShapeDtypeStruct((experts * cut, tok_rows), BF16),
+            jax.ShapeDtypeStruct((experts * cut, quarter), BF16),
             jax.ShapeDtypeStruct((2, tok_rows), jnp.int32),
         ],
         mebibytes=20,
-    )(d_out, chosen, weight)
-    routed_a = exchanged(outbox_a, cut)
-    outbox_b, pick_b = vmem_call(
-        functools.partial(refill_body, least=cut, most=capacity, stride=tail),
+        in_specs=[SMEM] + [VMEM] * 3,
+    )(place, d_out, chosen, weight)
+    tile = exchanged(outbox_q)
+    routed_q = [tile]
+    for k in range(1, lax.axis_size("tp")):
+        routed_q.append(shifted(tile, "tp", k))
+
+    outbox_d, pick = vmem_call(
+        functools.partial(refill_body, least=cut, most=capacity, tail=tail),
         [
             jax.ShapeDtypeStruct((experts * tail, model_width), BF16),
-            jax.ShapeDtypeStruct((experts * tail, tok_rows), BF16),
+            jax.ShapeDtypeStruct((slots, tok_rows), BF16),
         ],
         mebibytes=20,
     )(d_out, chosen, weight, ranks)
-    routed_b = exchanged(outbox_b, tail)
+    routed_d = exchanged(outbox_d)
 
     gate_w, up_w, down_w = w_gate[0].T, w_up[0].T, w_down[0]
     rows_in, active, slope, hidden = expert_forward(
@@ -643,21 +720,25 @@
 
     weights = (active, slope, down_w, gate_w, up_w)
     *whole, keep_a, send_a, keep_b, send_b = expert_cotangents(
-        place, routed_a, *weights, 0, ()
-    )
-    parts_a = (keep_a, send_a, keep_b, send_b)
-    routed, d_gate, d_up, *parts_b = expert_cotangents(
-        place, routed_b, *weights, experts * cut, whole
-    )
-    returned_a = exchanged(summed_over_tp(*parts_a), cut)
-    returned_b = exchanged(summed_over_tp(*parts_b), tail)
-    grad_gate = dot(d_gate, rows_in, TN).astype(BF16).T
-    grad_up = dot(d_up, rows_in, TN).astype(BF16).T
+        place, routed_q, *weights, 0, ()
+    )
+    parts_q = (keep_a, send_a, keep_b, send_b)
+    routed, d_gate, d_up, *parts_d = expert_cotangents(
+        place, (routed_d,), *weights, experts * cut, whole
+    )
+    summed = jnp.concatenate(
+        [
+            summed_over_tp(*parts_q).reshape(experts, cut, quarter),
+            summed_over_tp(*parts_d).reshape(experts, tail, quarter),
+        ],
+        axis=1,
+    )
+    returned = exchanged(summed.reshape(slots, quarter))
+    grad_gate, grad_up = weight_grads(d_gate, d_up, rows_in)
     grad_down = dot(hidden, routed, TN).astype(BF16)
 
     own_cols = lax.dynamic_slice_in_dim(d_out, place[0] * quarter, quarter, 1)
-    picked = own_cols.astype(F32) + dot(pick_a, returned_a, TN)
-    picked = picked + dot(pick_b, returned_b, TN)
+    picked = own_cols.astype(F32) + dot(pick, returned, TN)
     tiles = gathered_ring(picked.astype(BF16))
 
     d_mixed, back, own_term = cotangents(place, tiles, w_out, query, cumulative, ends)
@@ -671,8 +752,8 @@
     proj = lax.all_to_all(proj, SP, 0, 0, tiled=True)
     grad_proj = jnp.sum(proj.astype(F32), axis=0)
     return (
-        grad_gate[None],
-        grad_up[None],
+        grad_gate.T[None],
+        grad_up.T[None],
         grad_down[None],
         grad_proj,
         grad_q[:, None],

time: 290 us -> 281 us (0.969)
  matrix products: 29.9 us -> 11.4 us
  Pallas kernels: 63.5 us -> 73.6 us
  other arithmetic: 13.6 us -> 4.48 us
  waiting for transfers between devices: 84.6 us -> 92.6 us
    all_to_all x4 -> x3, waiting for transfers between devices: 50 us -> 28.7 us  [exchanged(): box = lax.all_to_all(box, SP, split_axis=0, concat_axis=0, tiled=True)]
    dot_general x5 -> x2, matrix products: 29.9 us -> 11.4 us  [dot(): return lax.dot_general(a, b, dims, preferred_element_type=F32)]
    ppermute x18 -> x21, waiting for transfers between devices: 10.5 us -> 27.9 us  [shifted(): return lax.ppermute(x, axis, [(i, (i + by) % count) for i in range(count)])]
    pallas_call x4 -> x7, Pallas kernels: 29.5 us -> 41.6 us  [the longest x2 26.2 us: expert_cotangents(): pl.pallas_call(functools.partial(expert_body, tiles=tiles), grid_spec=plt...]
    ppermute x8, waiting for transfers between devices: 24.2 us -> 35.9 us  [swapped(): return lax.ppermute(x, 'tp', [(i, i ^ flip) for i in range(count)])]
    convert_element_type x8 -> x4, other arithmetic: 9.79 us -> 1.32 us  [plus(): return total.astype(BF16)]
    ppermute x18 -> x21, starting transfers between devices: 26.7 us -> 34.5 us  [shifted(): return lax.ppermute(x, axis, [(i, (i + by) % count) for i in range(count)])]
    all_to_all x4 -> x3, starting transfers between devices: 26.2 us -> 22.3 us  [exchanged(): box = lax.all_to_all(box, SP, split_axis=0, concat_axis=0, tiled=True)]
  transfers between devices with their start and end apart: 31 -> 33, of which waited for: 13 -> 11; matrix products, arithmetic and copies ran while one was open for 15% -> 5% of each run, Pallas kernels for 21% -> 21%
where the time goes in v3:
time: 281 us; the launch traced here: 276 us
  waiting for transfers between devices  92.6 us (33%)
  Pallas kernels  73.6 us (26%)
  starting transfers between devices  72.4 us (26%)
  local copies, waits for them, and re-layouts  19.8 us (7%)
  matrix products  11.4 us (4%)
  other arithmetic  4.48 us (2%)
    ppermute x8, waiting for transfers between devices, swapped(): return lax.ppermute(x, 'tp', [(i, i ^ flip) for i in range(count)])  35.9 us
    ppermute x21, starting transfers between devices, shifted(): return lax.ppermute(x, axis, [(i, (i + by) % count) for i in range(count)])  34.5 us
    all_to_all x3, waiting for transfers between devices, exchanged(): box = lax.all_to_all(box, SP, split_axis=0, concat_axis=0, tiled=True)  28.7 us
    ppermute x21, waiting for transfers between devices, shifted(): return lax.ppermute(x, axis, [(i, (i + by) % count) for i in range(count)])  27.9 us
    pallas_call x2, Pallas kernels, expert_cotangents(): pl.pallas_call(functools.partial(expert_body, tiles=tiles), grid_spec=plt...  26.2 us
    all_to_all x3, starting transfers between devices, exchanged(): box = lax.all_to_all(box, SP, split_axis=0, concat_axis=0, tiled=True)  22.3 us
    pallas_call x1, Pallas kernels, expert_forward(): vmem_call(functools.partial(expert_forward_body, experts=experts, capacit...  18.3 us
    unnamed x93, local copies, waits for them, and re-layouts  17.4 us
  transfers between devices with their start and end apart: 33, of which 11 were waited for; matrix products, arithmetic and copies ran while one was open for 5% of the time, Pallas kernels for 21%

profile of v3, /device:TPU:0, one launch (start us, length us, event | category | flops | bytes accessed | tf_op | source)
XLA Modules:
  0.0 275.5 jit_solution(9412255402363455000)
XLA Ops:
  5.5 8.4 %all-to-all-start.1 = ((bf16[32,16,512]{2,1,0:T(8,128)(2,1)}), bf16[32,16,512]{2,1,0:T(8,128)(2,1)S(1)}, u32[]{:S(2)}, u32[]{:S(2)}) async-start(bf16[32,16,512]{2,1,0:T(8,128)(2,1)} %bitcast.11), calls=%async_computation.1 | async-start | bytes 1048576 | tf_op jit(solution)/shard_map/all_to_all | solution.py:683
  14.0 2.5 shard_map.180
  19.3 6.3 %all-to-all-done.1 = bf16[32,16,512]{2,1,0:T(8,128)(2,1)S(1)} async-done(((bf16[32,16,512]{2,1,0:T(8,128)(2,1)}), bf16[32,16,512]{2,1,0:T(8,128)(2,1)S(1)}, u32[]{:S(2)}, u32[]{:S(2)}) %all-to-all-start.1) | async-done | bytes 524320 | tf_op jit(solution)/shard_map/all_to_all | solution.py:683
  25.6 4.8 %all-to-all-start = ((bf16[32,24,2048]{2,1,0:T(8,128)(2,1)}), bf16[32,24,2048]{2,1,0:T(8,128)(2,1)}, u32[]{:S(2)}, u32[]{:S(2)}) async-start(bf16[32,24,2048]{2,1,0:T(8,128)(2,1)} %bitcast.56), calls=%async_computation | async-start | bytes 6291456 | tf_op jit(solution)/shard_map/all_to_all | solution.py:683
  32.0 2.7 collective-permute-start.1
  36.4 18.3 %shard_map.181 = (bf16[1280,2048]{1,0:T(8,128)(2,1)}, bf16[1280,704]{1,0:T(8,128)(2,1)}, bf16[1280,704]{1,0:T(8,128)(2,1)}, bf16[1280,704]{1,0:T(8,128)(2,1)}) custom-call(bf16[1152,2048]{1,0:T(8,128)(2,1)} %bitcast.80, bf16[704,2048]{1,0:T(8,128)(2,1)} %bitcast.72, bf16[704,2048]{1,0:T(8,128)(2,1)} %bitcast.75), custom_call_target="tpu_custom_call" | custom-call | tf_op jit(solution)/shard_map/pallas_call | solution.py:163
  54.7 3.1 %collective-permute-done.1.refs_2_ = bf16[512,512]{1,0:T(8,128)(2,1)S(1)} collective-permute-done((bf16[512,512]{1,0:T(8,128)(2,1)S(1)}, bf16[512,512]{1,0:T(8,128)(2,1)S(1)}, u32[]{:S(2)}, u32[]{:S(2)}) %collective-permute-start.1) | collective-permute-done | bytes 524320 | tf_op jit(solution)/shard_map/ppermute | solution.py:323
  58.8 11.7 %shard_map.182 = (bf16[1280,2048]{1,0:T(8,128)(2,1)}, bf16[1280,704]{1,0:T(8,128)(2,1)}, bf16[1280,704]{1,0:T(8,128)(2,1)}, bf16[2,512,256]{2,1,0:T(8,128)(2,1)}...) custom-call(s32[1]{0:T(128)} %bitcast.place, ...), custom_call_target="tpu_custom_call" | custom-call | tf_op jit(solution)/shard_map/pallas_call | solution.py:237
  72.4 14.5 %shard_map.183 = (bf16[1280,2048]{1,0:T(8,128)(2,1)}, bf16[1280,704]{1,0:T(8,128)(2,1)}, bf16[1280,704]{1,0:T(8,128)(2,1)}, bf16[2,768,256]{2,1,0:T(8,128)(2,1)}...) custom-call(s32[1]{0:T(128)} %bitcast.place, ...), custom_call_target="tpu_custom_call", output_to_operand_aliasing={{0}: (7, {}), {1}: (8, {}), {2}: (9, {})} | custom-call | tf_op jit(solution)/shard_map/pallas_call | solution.py:237
  86.9 2.9 %collective-permute-start.9 = (bf16[2,768,256]{2,1,0:T(8,128)(2,1)}, bf16[2,768,256]{2,1,0:T(8,128)(2,1)S(1)}, u32[]{:S(2)}, u32[]{:S(2)}) collective-permute-start(bf16[2,768,256]{2,1,0:T(8,128)(2,1)} %get-tuple-element.83), channel_id=1, source_target_pairs={{0,3},{1,2},{2,1},{3,0},{4,7},{5,6},{6,5},{7,4},{8,11},{9,10},{10,... | collective-permute-start | bytes 2359304 | tf_op jit(solution)/shard_map/ppermute | solution.py:281
  92.2 24.9 %collective-permute-done.5.got_b = bf16[2,512,256]{2,1,0:T(8,128)(2,1)S(1)} collective-permute-done((bf16[2,512,256]{2,1,0:T(8,128)(2,1)S(1)}, bf16[2,512,256]{2,1,0:T(8,128)(2,1)S(1)}, u32[]{:S(2)}, u32[]{:S(2)}) %collective-permute-start.5) | collective-permute-done | bytes 524320 | tf_op jit(solution)/shard_map/ppermute | solution.py:281
  120.6 2.9 %collective-permute-start.8 = (bf16[768,256]{1,0:T(8,128)(2,1)S(1)}, bf16[768,256]{1,0:T(8,128)(2,1)S(1)}, u32[]{:S(2)}, u32[]{:S(2)}) collective-permute-start(bf16[768,256]{1,0:T(8,128)(2,1)S(1)} %fusion.2), channel_id=1, source_target_pairs={{0,3},{1,2},{2,1},{3,0},{4,7},{5,6},{6,5},{7,4},{8,11},{9,10},{10,... | collective-permute-start | bytes 1179656 | tf_op jit(solution)/shard_map/ppermute | solution.py:281
  124.0 2.4 collective-permute-done.6.last_b
  126.4 8.7 %collective-permute-done.4.last_a = bf16[512,256]{1,0:T(8,128)(2,1)S(1)} collective-permute-done((bf16[512,256]{1,0:T(8,128)(2,1)S(1)}, bf16[512,256]{1,0:T(8,128)(2,1)S(1)}, u32[]{:S(2)}, u32[]{:S(2)}) %collective-permute-start.4) | collective-permute-done | bytes 262176 | tf_op jit(solution)/shard_map/ppermute | solution.py:281
  136.8 9.0 %all-to-all-start.2 = ((bf16[32,40,512]{2,1,0:T(8,128)(2,1)}), bf16[32,40,512]{2,1,0:T(8,128)(2,1)}, u32[]{:S(2)}, u32[]{:S(2)}) async-start(bf16[32,40,512]{2,1,0:T(8,128)(2,1)} %pad_maximum_fusion), calls=%async_computation.2 | async-start | bytes 2621440 | tf_op jit(solution)/shard_map/all_to_all | solution.py:683
  145.8 20.5 %all-to-all-done.2 = bf16[32,40,512]{2,1,0:T(8,128)(2,1)} async-done(((bf16[32,40,512]{2,1,0:T(8,128)(2,1)}), bf16[32,40,512]{2,1,0:T(8,128)(2,1)}, u32[]{:S(2)}, u32[]{:S(2)}) %all-to-all-start.2) | async-done | bytes 1310752 | tf_op jit(solution)/shard_map/all_to_all | solution.py:683
  166.4 2.6 fusion.1.a
  169.1 3.2 %collective-permute-start.12 = (bf16[512,512]{1,0:T(8,128)(2,1)S(1)}, bf16[512,512]{1,0:T(8,128)(2,1)S(1)}, u32[]{:S(2)}, u32[]{:S(2)}) collective-permute-start(bf16[512,512]{1,0:T(8,128)(2,1)S(1)} %fusion.1.a), channel_id=1, source_target_pairs={{0,3},{1,0},{2,1},{3,2},{4,7},{5,4},{6,5},{7,6},{8,11},{9,8},{10,9... | collective-permute-start | bytes 1572872 | tf_op jit(solution)/shard_map/ppermute | solution.py:323
  174.5 8.7 %collective-permute-done.11.b = bf16[512,512]{1,0:T(8,128)(2,1)S(1)} collective-permute-done((bf16[512,512]{1,0:T(8,128)(2,1)S(1)}, bf16[512,512]{1,0:T(8,128)(2,1)S(1)}, u32[]{:S(2)}, u32[]{:S(2)}) %collective-permute-start.11) | collective-permute-done | bytes 524320 | tf_op jit(solution)/shard_map/ppermute | solution.py:323
  184.6 3.2 %collective-permute-start.14 = (bf16[256,512]{1,0:T(8,128)(2,1)}, bf16[256,512]{1,0:T(8,128)(2,1)}, u32[]{:S(2)}, u32[]{:S(2)}) collective-permute-start(bf16[256,512]{1,0:T(8,128)(2,1)} %slice.45), channel_id=1, source_target_pairs={{0,3},{1,0},{2,1},{3,2},{4,7},{5,4},{6,5},{7,6},{8,11},{9,8},{10,9... | collective-permute-start | bytes 786440 | tf_op jit(solution)/shard_map/ppermute | solution.py:323
  191.7 2.1 collective-permute-start.18
  193.8 4.6 %collective-permute-done.16.refs_1_ = f32[264,128]{1,0:T(8,128)S(1)} collective-permute-done((f32[264,128]{1,0:T(8,128)S(1)}, f32[264,128]{1,0:T(8,128)S(1)}, u32[]{:S(2)}, u32[]{:S(2)}) %collective-permute-start.16) | collective-permute-done | bytes 135200 | tf_op jit(solution)/shard_map/ppermute | solution.py:323
  201.6 2.5 collective-permute-start.21
  207.1 2.6 shard_map.192
  215.1 2.1 shard_map.190
  220.1 4.7 %all-to-all-start.3 = ((bf16[32,64,256]{2,1,0:T(8,128)(2,1)}), bf16[32,64,256]{2,1,0:T(8,128)(2,1)}, u32[]{:S(2)}, u32[]{:S(2)}) async-start(bf16[32,64,256]{2,1,0:T(8,128)(2,1)} %bitcast.34), calls=%async_computation.3 | async-start | bytes 2097152 | tf_op jit(solution)/shard_map/all_to_all | solution.py:752
  227.3 2.7 collective-permute-start.24
  231.5 9.9 %collective-permute-done.23.refs_1_ = bf16[256,128]{1,0:T(8,128)(2,1)S(1)} collective-permute-done((bf16[256,128]{1,0:T(8,128)(2,1)S(1)}, bf16[256,128]{1,0:T(8,128)(2,1)S(1)}, u32[]{:S(2)}, u32[]{:S(2)}) %collective-permute-start.23) | collective-permute-done | bytes 65568 | tf_op jit(solution)/shard_map/ppermute | solution.py:323
  244.6 2.8 %collective-permute-start.27 = (bf16[256,128]{1,0:T(8,128)(2,1)S(1)}, bf16[256,128]{1,0:T(8,128)(2,1)S(1)}, u32[]{:S(2)}, u32[]{:S(2)}) collective-permute-start(bf16[256,128]{1,0:T(8,128)(2,1)S(1)} %get-tuple-element.104.refs_0_), channel_id=1, source_target_pairs={{0,64},{32,96},{64,0},{96,32},{1,65},{33,97},{65,1},{97,33},{2,66}... | collective-permute-start | bytes 196616 | tf_op jit(solution)/shard_map/ppermute | solution.py:323
  249.0 8.8 %fusion = bf16[1,704,2048]{2,1,0:T(8,128)(2,1)} fusion(bf16[1280,704]{1,0:T(8,128)(2,1)} %get-tuple-element.73, bf16[1280,2048]{1,0:T(8,128)(2,1)} %get-tuple-element.74), kind=kOutput, calls=%fused_computation.1 | convolution fusion | flops 3692429312 | bytes 9928704 | tf_op jit(solution)/shard_map/dot_general | solution.py:24
  257.8 10.5 %shard_map.184 = (bf16[704,2048]{1,0:T(8,128)(2,1)}, bf16[704,2048]{1,0:T(8,128)(2,1)}) custom-call(bf16[1280,704]{1,0:T(8,128)(2,1)S(1)} %copy-done.2, bf16[1280,704]{1,0:T(8,128)(2,1)S(1)} %copy-done.3, bf16[1280,2048]{1,0:T(8,128)(2,1)} %get-tuple-element.70.rows_in), custom_call_target="tpu_custom_call" | custom-call | tf_op jit(solution)/shard_map/pallas_call | solution.py:269
  270.4 2.9 %shard_map.196 = (bf16[512,128]{1,0:T(8,128)(2,1)}, bf16[512,128]{1,0:T(8,128)(2,1)}, bf16[512,256]{1,0:T(8,128)(2,1)}, f32[512,128]{1,0:T(8,128)}) custom-call(bf16[512,128]{1,0:T(8,128)(2,1)S(1)} %bitcast.61, bf16[512,128]{1,0:T(8,128)(2,1)S(1)} %bitcast.65, bf16[512,256]{1,0:T(8,128)(2,1)S(1)} %bitcast.55, f32[512,128]{1,0:T(8,128)S(1)} %get-tuple-element.84.cumulative, ...), custom_call_target="tpu_custom_call" | custom-call | tf_op jit(solution)/shard_map/pallas_call | solution.py:540
  (156 shorter events, 56.5 us)
Async XLA Ops:
  5.5 20.0 %all-to-all-start.1 = ((bf16[32,16,512]{2,1,0:T(8,128)(2,1)}), bf16[32,16,512]{2,1,0:T(8,128)(2,1)S(1)}, u32[]{:S(2)}, u32[]{:S(2)}) async-start(bf16[32,16,512]{2,1,0:T(8,128)(2,1)} %bitcast.11), calls=%async_computation.1 | async-start | bytes 1048576 | tf_op jit(solution)/shard_map/all_to_all | solution.py:683
  25.6 46.8 %all-to-all-start = ((bf16[32,24,2048]{2,1,0:T(8,128)(2,1)}), bf16[32,24,2048]{2,1,0:T(8,128)(2,1)}, u32[]{:S(2)}, u32[]{:S(2)}) async-start(bf16[32,24,2048]{2,1,0:T(8,128)(2,1)} %bitcast.56), calls=%async_computation | async-start | bytes 6291456 | tf_op jit(solution)/shard_map/all_to_all | solution.py:683
  30.4 24.3 %collective-permute-start = (bf16[512,512]{1,0:T(8,128)(2,1)S(1)}, bf16[512,512]{1,0:T(8,128)(2,1)S(1)}, u32[]{:S(2)}, u32[]{:S(2)}) collective-permute-start(bf16[512,512]{1,0:T(8,128)(2,1)S(1)} %bitcast.81), channel_id=1, source_target_pairs={{0,1},{1,2},{2,3},{3,0},{4,5},{5,6},{6,7},{7,4},{8,9},{9,10},{10,1... | collective-permute-start | bytes 1572872 | tf_op jit(solution)/shard_map/ppermute | solution.py:323
  32.0 25.9 %collective-permute-start.1 = (bf16[512,512]{1,0:T(8,128)(2,1)S(1)}, bf16[512,512]{1,0:T(8,128)(2,1)S(1)}, u32[]{:S(2)}, u32[]{:S(2)}) collective-permute-start(bf16[512,512]{1,0:T(8,128)(2,1)S(1)} %bitcast.82), channel_id=1, source_target_pairs={{0,2},{1,3},{2,0},{3,1},{4,6},{5,7},{6,4},{7,5},{8,10},{9,11},{10,... | collective-permute-start | bytes 1572872 | tf_op jit(solution)/shard_map/ppermute | solution.py:323
  34.7 23.1 %collective-permute-start.2 = (bf16[512,512]{1,0:T(8,128)(2,1)S(1)}, bf16[512,512]{1,0:T(8,128)(2,1)S(1)}, u32[]{:S(2)}, u32[]{:S(2)}) collective-permute-start(bf16[512,512]{1,0:T(8,128)(2,1)S(1)} %bitcast.83), channel_id=1, source_target_pairs={{0,3},{1,0},{2,1},{3,2},{4,7},{5,4},{6,5},{7,6},{8,11},{9,8},{10,9... | collective-permute-start | bytes 1572872 | tf_op jit(solution)/shard_map/ppermute | solution.py:323
  86.9 30.7 %collective-permute-start.9 = (bf16[2,768,256]{2,1,0:T(8,128)(2,1)}, bf16[2,768,256]{2,1,0:T(8,128)(2,1)S(1)}, u32[]{:S(2)}, u32[]{:S(2)}) collective-permute-start(bf16[2,768,256]{2,1,0:T(8,128)(2,1)} %get-tuple-element.83), channel_id=1, source_target_pairs={{0,3},{1,2},{2,1},{3,0},{4,7},{5,6},{6,5},{7,4},{8,11},{9,10},{10,... | collective-permute-start | bytes 2359304 | tf_op jit(solution)/shard_map/ppermute | solution.py:281
  89.8 27.3 %collective-permute-start.5 = (bf16[2,512,256]{2,1,0:T(8,128)(2,1)S(1)}, bf16[2,512,256]{2,1,0:T(8,128)(2,1)S(1)}, u32[]{:S(2)}, u32[]{:S(2)}) collective-permute-start(bf16[2,512,256]{2,1,0:T(8,128)(2,1)S(1)} %copy-done.45), channel_id=1, source_target_pairs={{0,3},{1,2},{2,1},{3,0},{4,7},{5,6},{6,5},{7,4},{8,11},{9,10},{10,... | collective-permute-start | bytes 1572872 | tf_op jit(solution)/shard_map/ppermute | solution.py:281
  90.2 30.2 %collective-permute-start.7 = (bf16[2,768,256]{2,1,0:T(8,128)(2,1)}, bf16[2,768,256]{2,1,0:T(8,128)(2,1)S(1)}, u32[]{:S(2)}, u32[]{:S(2)}) collective-permute-start(bf16[2,768,256]{2,1,0:T(8,128)(2,1)} %get-tuple-element.81), channel_id=1, source_target_pairs={{0,1},{1,0},{2,3},{3,2},{4,5},{5,4},{6,7},{7,6},{8,9},{9,8},{10,11... | collective-permute-start | bytes 2359304 | tf_op jit(solution)/shard_map/ppermute | solution.py:281
  90.5 32.9 %collective-permute-start.3 = (bf16[2,512,256]{2,1,0:T(8,128)(2,1)S(1)}, bf16[2,512,256]{2,1,0:T(8,128)(2,1)S(1)}, u32[]{:S(2)}, u32[]{:S(2)}) collective-permute-start(bf16[2,512,256]{2,1,0:T(8,128)(2,1)S(1)} %copy-done.44), channel_id=1, source_target_pairs={{0,1},{1,0},{2,3},{3,2},{4,5},{5,4},{6,7},{7,6},{8,9},{9,8},{10,11... | collective-permute-start | bytes 1572872 | tf_op jit(solution)/shard_map/ppermute | solution.py:281
  117.2 9.3 %collective-permute-start.6 = (bf16[512,256]{1,0:T(8,128)(2,1)S(1)}, bf16[512,256]{1,0:T(8,128)(2,1)S(1)}, u32[]{:S(2)}, u32[]{:S(2)}) collective-permute-start(bf16[512,256]{1,0:T(8,128)(2,1)S(1)} %fusion.5), channel_id=1, source_target_pairs={{0,1},{1,0},{2,3},{3,2},{4,5},{5,4},{6,7},{7,6},{8,9},{9,8},{10,11... | collective-permute-start | bytes 786440 | tf_op jit(solution)/shard_map/ppermute | solution.py:281
  118.7 16.7 %collective-permute-start.10 = (bf16[768,256]{1,0:T(8,128)(2,1)S(1)}, bf16[768,256]{1,0:T(8,128)(2,1)S(1)}, u32[]{:S(2)}, u32[]{:S(2)}) collective-permute-start(bf16[768,256]{1,0:T(8,128)(2,1)S(1)} %fusion.3), channel_id=1, source_target_pairs={{0,1},{1,0},{2,3},{3,2},{4,5},{5,4},{6,7},{7,6},{8,9},{9,8},{10,11... | collective-permute-start | bytes 1179656 | tf_op jit(solution)/shard_map/ppermute | solution.py:281
  120.6 14.7 %collective-permute-start.8 = (bf16[768,256]{1,0:T(8,128)(2,1)S(1)}, bf16[768,256]{1,0:T(8,128)(2,1)S(1)}, u32[]{:S(2)}, u32[]{:S(2)}) collective-permute-start(bf16[768,256]{1,0:T(8,128)(2,1)S(1)} %fusion.2), channel_id=1, source_target_pairs={{0,3},{1,2},{2,1},{3,0},{4,7},{5,6},{6,5},{7,4},{8,11},{9,10},{10,... | collective-permute-start | bytes 1179656 | tf_op jit(solution)/shard_map/ppermute | solution.py:281
  123.5 11.6 %collective-permute-start.4 = (bf16[512,256]{1,0:T(8,128)(2,1)S(1)}, bf16[512,256]{1,0:T(8,128)(2,1)S(1)}, u32[]{:S(2)}, u32[]{:S(2)}) collective-permute-start(bf16[512,256]{1,0:T(8,128)(2,1)S(1)} %fusion.4), channel_id=1, source_target_pairs={{0,3},{1,2},{2,1},{3,0},{4,7},{5,6},{6,5},{7,4},{8,11},{9,10},{10,... | collective-permute-start | bytes 786440 | tf_op jit(solution)/shard_map/ppermute | solution.py:281
  136.8 29.6 %all-to-all-start.2 = ((bf16[32,40,512]{2,1,0:T(8,128)(2,1)}), bf16[32,40,512]{2,1,0:T(8,128)(2,1)}, u32[]{:S(2)}, u32[]{:S(2)}) async-start(bf16[32,40,512]{2,1,0:T(8,128)(2,1)} %pad_maximum_fusion), calls=%async_computation.2 | async-start | bytes 2621440 | tf_op jit(solution)/shard_map/all_to_all | solution.py:683
  169.1 14.1 %collective-permute-start.11 = (bf16[512,512]{1,0:T(8,128)(2,1)S(1)}, bf16[512,512]{1,0:T(8,128)(2,1)S(1)}, u32[]{:S(2)}, u32[]{:S(2)}) collective-permute-start(bf16[512,512]{1,0:T(8,128)(2,1)S(1)} %fusion.1.a), channel_id=1, source_target_pairs={{0,1},{1,2},{2,3},{3,0},{4,5},{5,6},{6,7},{7,4},{8,9},{9,10},{10,1... | collective-permute-start | bytes 1572872 | tf_op jit(solution)/shard_map/ppermute | solution.py:323
  169.1 14.8 %collective-permute-start.12 = (bf16[512,512]{1,0:T(8,128)(2,1)S(1)}, bf16[512,512]{1,0:T(8,128)(2,1)S(1)}, u32[]{:S(2)}, u32[]{:S(2)}) collective-permute-start(bf16[512,512]{1,0:T(8,128)(2,1)S(1)} %fusion.1.a), channel_id=1, source_target_pairs={{0,3},{1,0},{2,1},{3,2},{4,7},{5,4},{6,5},{7,6},{8,11},{9,8},{10,9... | collective-permute-start | bytes 1572872 | tf_op jit(solution)/shard_map/ppermute | solution.py:323
  174.5 13.4 %collective-permute-start.15 = (f32[264,128]{1,0:T(8,128)S(1)}, f32[264,128]{1,0:T(8,128)S(1)}, u32[]{:S(2)}, u32[]{:S(2)}) collective-permute-start(f32[264,128]{1,0:T(8,128)S(1)} %get-tuple-element.87.refs_0_), channel_id=1, source_target_pairs={{0,4},{4,0},{1,5},{5,1},{2,6},{6,2},{3,7},{7,3},{8,12},{12,8},{9,1... | collective-permute-start | bytes 405512 | tf_op jit(solution)/shard_map/ppermute | solution.py:323
  183.9 20.3 %collective-permute-start.13 = (bf16[256,512]{1,0:T(8,128)(2,1)}, bf16[256,512]{1,0:T(8,128)(2,1)S(1)}, u32[]{:S(2)}, u32[]{:S(2)}) collective-permute-start(bf16[256,512]{1,0:T(8,128)(2,1)} %slice.44), channel_id=1, source_target_pairs={{0,1},{1,2},{2,3},{3,0},{4,5},{5,6},{6,7},{7,4},{8,9},{9,10},{10,1... | collective-permute-start | bytes 786440 | tf_op jit(solution)/shard_map/ppermute | solution.py:323
  184.6 19.5 %collective-permute-start.14 = (bf16[256,512]{1,0:T(8,128)(2,1)}, bf16[256,512]{1,0:T(8,128)(2,1)}, u32[]{:S(2)}, u32[]{:S(2)}) collective-permute-start(bf16[256,512]{1,0:T(8,128)(2,1)} %slice.45), channel_id=1, source_target_pairs={{0,3},{1,0},{2,1},{3,2},{4,7},{5,4},{6,5},{7,6},{8,11},{9,8},{10,9... | collective-permute-start | bytes 786440 | tf_op jit(solution)/shard_map/ppermute | solution.py:323
  189.2 9.3 %collective-permute-start.16 = (f32[264,128]{1,0:T(8,128)S(1)}, f32[264,128]{1,0:T(8,128)S(1)}, u32[]{:S(2)}, u32[]{:S(2)}) collective-permute-start(f32[264,128]{1,0:T(8,128)S(1)} %get-tuple-element.88.refs_0_), channel_id=1, source_target_pairs={{0,8},{8,16},{16,24},{24,0},{1,9},{9,17},{17,25},{25,1},{2,10},{10... | collective-permute-start | bytes 405512 | tf_op jit(solution)/shard_map/ppermute | solution.py:323
  190.6 7.9 %collective-permute-start.17 = (f32[264,128]{1,0:T(8,128)S(1)}, f32[264,128]{1,0:T(8,128)S(1)}, u32[]{:S(2)}, u32[]{:S(2)}) collective-permute-start(f32[264,128]{1,0:T(8,128)S(1)} %get-tuple-element.88.refs_0_), channel_id=1, source_target_pairs={{0,16},{8,24},{16,0},{24,8},{1,17},{9,25},{17,1},{25,9},{2,18},{10... | collective-permute-start | bytes 405512 | tf_op jit(solution)/shard_map/ppermute | solution.py:323
  198.6 12.1 %collective-permute-start.19 = (f32[264,128]{1,0:T(8,128)S(1)}, f32[264,128]{1,0:T(8,128)}, u32[]{:S(2)}, u32[]{:S(2)}) collective-permute-start(f32[264,128]{1,0:T(8,128)S(1)} %get-tuple-element.89.refs_0_), channel_id=1, source_target_pairs={{0,32},{32,64},{64,96},{96,0},{1,33},{33,65},{65,97},{97,1},{2,34}... | collective-permute-start | bytes 405512 | tf_op jit(solution)/shard_map/ppermute | solution.py:323
  200.2 10.4 %collective-permute-start.20 = (f32[264,128]{1,0:T(8,128)S(1)}, f32[264,128]{1,0:T(8,128)}, u32[]{:S(2)}, u32[]{:S(2)}) collective-permute-start(f32[264,128]{1,0:T(8,128)S(1)} %get-tuple-element.89.refs_0_), channel_id=1, source_target_pairs={{0,64},{32,96},{64,0},{96,32},{1,65},{33,97},{65,1},{97,33},{2,66}... | collective-permute-start | bytes 405512 | tf_op jit(solution)/shard_map/ppermute | solution.py:323
  201.6 9.1 %collective-permute-start.21 = (f32[264,128]{1,0:T(8,128)S(1)}, f32[264,128]{1,0:T(8,128)}, u32[]{:S(2)}, u32[]{:S(2)}) collective-permute-start(f32[264,128]{1,0:T(8,128)S(1)} %get-tuple-element.89.refs_0_), channel_id=1, source_target_pairs={{0,96},{32,0},{64,32},{96,64},{1,97},{33,1},{65,33},{97,65},{2,98}... | collective-permute-start | bytes 405512 | tf_op jit(solution)/shard_map/ppermute | solution.py:323
  210.7 14.1 %collective-permute-start.22 = (bf16[256,128]{1,0:T(8,128)(2,1)}, bf16[256,128]{1,0:T(8,128)(2,1)}, u32[]{:S(2)}, u32[]{:S(2)}) collective-permute-start(bf16[256,128]{1,0:T(8,128)(2,1)} %get-tuple-element.102.refs_0_), channel_id=1, source_target_pairs={{0,4},{4,0},{1,5},{5,1},{2,6},{6,2},{3,7},{7,3},{8,12},{12,8},{9,1... | collective-permute-start | bytes 196616 | tf_op jit(solution)/shard_map/ppermute | solution.py:323
  220.1 53.2 %all-to-all-start.3 = ((bf16[32,64,256]{2,1,0:T(8,128)(2,1)}), bf16[32,64,256]{2,1,0:T(8,128)(2,1)}, u32[]{:S(2)}, u32[]{:S(2)}) async-start(bf16[32,64,256]{2,1,0:T(8,128)(2,1)} %bitcast.34), calls=%async_computation.3 | async-start | bytes 2097152 | tf_op jit(solution)/shard_map/all_to_all | solution.py:752
  225.7 15.8 %collective-permute-start.23 = (bf16[256,128]{1,0:T(8,128)(2,1)S(1)}, bf16[256,128]{1,0:T(8,128)(2,1)S(1)}, u32[]{:S(2)}, u32[]{:S(2)}) collective-permute-start(bf16[256,128]{1,0:T(8,128)(2,1)S(1)} %get-tuple-element.103.refs_0_), channel_id=1, source_target_pairs={{0,8},{8,16},{16,24},{24,0},{1,9},{9,17},{17,25},{25,1},{2,10},{10... | collective-permute-start | bytes 196616 | tf_op jit(solution)/shard_map/ppermute | solution.py:323
  227.3 15.6 %collective-permute-start.24 = (bf16[256,128]{1,0:T(8,128)(2,1)S(1)}, bf16[256,128]{1,0:T(8,128)(2,1)S(1)}, u32[]{:S(2)}, u32[]{:S(2)}) collective-permute-start(bf16[256,128]{1,0:T(8,128)(2,1)S(1)} %get-tuple-element.103.refs_0_), channel_id=1, source_target_pairs={{0,16},{8,24},{16,0},{24,8},{1,17},{9,25},{17,1},{25,9},{2,18},{10... | collective-permute-start | bytes 196616 | tf_op jit(solution)/shard_map/ppermute | solution.py:323
  230.0 12.9 %collective-permute-start.25 = (bf16[256,128]{1,0:T(8,128)(2,1)S(1)}, bf16[256,128]{1,0:T(8,128)(2,1)S(1)}, u32[]{:S(2)}, u32[]{:S(2)}) collective-permute-start(bf16[256,128]{1,0:T(8,128)(2,1)S(1)} %get-tuple-element.103.refs_0_), channel_id=1, source_target_pairs={{0,24},{8,0},{16,8},{24,16},{1,25},{9,1},{17,9},{25,17},{2,26},{10... | collective-permute-start | bytes 196616 | tf_op jit(solution)/shard_map/ppermute | solution.py:323
  243.1 27.3 %collective-permute-start.26 = (bf16[256,128]{1,0:T(8,128)(2,1)S(1)}, bf16[256,128]{1,0:T(8,128)(2,1)S(1)}, u32[]{:S(2)}, u32[]{:S(2)}) collective-permute-start(bf16[256,128]{1,0:T(8,128)(2,1)S(1)} %get-tuple-element.104.refs_0_), channel_id=1, source_target_pairs={{0,32},{32,64},{64,96},{96,0},{1,33},{33,65},{65,97},{97,1},{2,34}... | collective-permute-start | bytes 196616 | tf_op jit(solution)/shard_map/ppermute | solution.py:323
  244.6 25.8 %collective-permute-start.27 = (bf16[256,128]{1,0:T(8,128)(2,1)S(1)}, bf16[256,128]{1,0:T(8,128)(2,1)S(1)}, u32[]{:S(2)}, u32[]{:S(2)}) collective-permute-start(bf16[256,128]{1,0:T(8,128)(2,1)S(1)} %get-tuple-element.104.refs_0_), channel_id=1, source_target_pairs={{0,64},{32,96},{64,0},{96,32},{1,65},{33,97},{65,1},{97,33},{2,66}... | collective-permute-start | bytes 196616 | tf_op jit(solution)/shard_map/ppermute | solution.py:323
  247.4 23.0 %collective-permute-start.28 = (bf16[256,128]{1,0:T(8,128)(2,1)S(1)}, bf16[256,128]{1,0:T(8,128)(2,1)S(1)}, u32[]{:S(2)}, u32[]{:S(2)}) collective-permute-start(bf16[256,128]{1,0:T(8,128)(2,1)S(1)} %get-tuple-element.104.refs_0_), channel_id=1, source_target_pairs={{0,96},{32,0},{64,32},{96,64},{1,97},{33,1},{65,33},{97,65},{2,98}... | collective-permute-start | bytes 196616 | tf_op jit(solution)/shard_map/ppermute | solution.py:323
  (47 other events, 391.3 us)

commit v4 on v3

--- a/solution.py
+++ b/solution.py
@@ -133,46 +133,50 @@
     return placed(group * cut, cut, cut, 0), placed(group * tail, tail, capacity - cut, cut)
 
 
-def expert_forward_body(
-    inputs, gate_w, up_w, rows_in, active, slope, hidden, *, experts, capacity, cut, tail
-):
-    group = 8
-    orders = slot_order(group, capacity, cut, tail)
-    for step in range(experts // group):
-        block = inputs[step * group * capacity : (step + 1) * group * capacity, :]
-        for order, start in zip(orders, (step * group * cut, experts * cut + step * group * tail)):
-            rows_in[start : start + order.shape[0], :] = dot(order, block, NN).astype(BF16)
+def expert_forward_body(inputs, gate_w, up_w, *outs, orders):
+    order = jnp.concatenate(slot_order(*orders), axis=0)
+    moved = dot(order, inputs[...], NN).astype(BF16)
+    split = outs[0].shape[0]
+    rows_q, rows_d = outs[0:2]
+    rows_q[...] = moved[:split]
+    rows_d[...] = moved[split:]
     units = gate_w.shape[0]
-    step = rows_in.shape[0] // 2
     for first in range(0, units, 256):
         cols = slice(first, min(first + 256, units))
-        for start in range(0, rows_in.shape[0], step):
-            rows = slice(start, start + step)
-            gate = dot(rows_in[rows, :], gate_w[cols, :], NT)
-            up = dot(rows_in[rows, :], up_w[cols, :], NT)
-            sigmoid = 1.0 / (1.0 + jnp.exp(-gate))
-            silu = gate * sigmoid
-            hidden[rows, cols] = (silu * up).astype(BF16)
-            active[rows, cols] = silu.astype(BF16)
-            slope[rows, cols] = (up * sigmoid * (1.0 + gate * (1.0 - sigmoid))).astype(BF16)
+        gate = dot(moved, gate_w[cols, :], NT)
+        up = dot(moved, up_w[cols, :], NT)
+        sigmoid = 1.0 / (1.0 + jnp.exp(-gate))
+        silu = gate * sigmoid
+        slope = up * sigmoid * (1.0 + gate * (1.0 - sigmoid))
+        for i, value in enumerate((silu, slope, silu * up)):
+            value = value.astype(BF16)
+            outs[2 + 2 * i][:, cols] = value[:split]
+            outs[3 + 2 * i][:, cols] = value[split:]
 
 
 def expert_forward(inputs, gate_w, up_w, experts, capacity, cut, tail):
-    slots = experts * (cut + tail)
-    units = gate_w.shape[0]
-    return vmem_call(
-        functools.partial(
-            expert_forward_body, experts=experts, capacity=capacity, cut=cut, tail=tail
-        ),
-        [jax.ShapeDtypeStruct((slots, inputs.shape[1]), BF16)]
-        + [jax.ShapeDtypeStruct((slots, units), BF16)] * 3,
-        mebibytes=56,
+    group = 8
+    width, units = inputs.shape[1], gate_w.shape[0]
+    sizes = (group * cut, group * tail)
+    by_row = lambda i: (i, 0)
+    whole = pl.BlockSpec((units, width), lambda i: (0, 0))
+    widths = [width] * 2 + [units] * 6
+    return pl.pallas_call(
+        functools.partial(expert_forward_body, orders=(group, capacity, cut, tail)),
+        grid=(experts // group,),
+        in_specs=[pl.BlockSpec((group * capacity, width), by_row), whole, whole],
+        out_specs=[pl.BlockSpec((sizes[i % 2], w), by_row) for i, w in enumerate(widths)],
+        out_shape=[
+            jax.ShapeDtypeStruct((experts // group * sizes[i % 2], w), BF16)
+            for i, w in enumerate(widths)
+        ],
+        compiler_params=limit(56),
     )(inputs, gate_w, up_w)
 
 
 def expert_body(place, *refs, tiles):
     routed, (active, slope, down_w, gate_w, up_w) = refs[:tiles], refs[tiles : tiles + 5]
-    routed_out, d_gate, d_up, keep_a, send_a, keep_b, send_b = refs[-11:-4]
+    *routed_out, d_gate, d_up, keep_a, send_a, keep_b, send_b = refs[tiles + 5 : -4]
     down_v, gate_v, up_v, loaded = refs[-4:]
     copies = [
         pltpu.make_async_copy(source, target, loaded.at[i])
@@ -191,7 +195,7 @@
         cols = slice(None)
         if tiles > 1:
             cols = pl.ds(pl.multiple_of(((place[0] + tiles - k) & (tiles - 1)) * wide, wide), wide)
-        routed_out[:, cols] = tile[...]
+            routed_out[0][:, cols] = tile[...]
         d_hidden = d_hidden + dot(tile[...], down_v[:, cols], NT)
 
     @pl.when(pl.program_id(0) == 0)
@@ -219,61 +223,56 @@
         home_b[0][home_b[1]] = term[:, half:]
 
 
-def expert_cotangents(place, routed, active, slope, down_w, gate_w, up_w, first_row, earlier):
+def expert_cotangents(place, routed, active, slope, down_w, gate_w, up_w):
     rows, wide = routed[0].shape
     tiles = len(routed)
     units, width = down_w.shape
     step = 256
     half = width // 8
-    skipped = first_row // step
     by_row = lambda i, *_: (i, 0)
-    later_row = lambda i, *_: (i + skipped, 0)
-    in_specs = [pl.BlockSpec((step, wide), by_row)] * tiles + [
-        pl.BlockSpec((step, units), later_row),
-        pl.BlockSpec((step, units), later_row),
-    ]
-    in_specs += [pl.BlockSpec(memory_space=pl.ANY)] * (3 + len(earlier))
     pair = pl.BlockSpec((2, step, half), lambda i, *_: (0, i, 0))
+    rebuilt = [width] if tiles > 1 else []
     return pl.pallas_call(
         functools.partial(expert_body, tiles=tiles),
         grid_spec=pltpu.PrefetchScalarGridSpec(
             num_scalar_prefetch=1,
             grid=(rows // step,),
-            in_specs=in_specs,
-            out_specs=[pl.BlockSpec((step, width), later_row)]
-            + [pl.BlockSpec((step, units), later_row)] * 2
+            in_specs=[pl.BlockSpec((step, wide), by_row)] * tiles
+            + [pl.BlockSpec((step, units), by_row)] * 2
+            + [pl.BlockSpec(memory_space=pl.ANY)] * 3,
+            out_specs=[pl.BlockSpec((step, w), by_row) for w in rebuilt + [units] * 2]
             + [pair] * 4,
             scratch_shapes=[pltpu.VMEM((units, width), BF16)] * 3
             + [pltpu.SemaphoreType.DMA((3,))],
         ),
-        out_shape=[jax.ShapeDtypeStruct((active.shape[0], width), BF16)]
-        + [jax.ShapeDtypeStruct(active.shape, BF16)] * 2
+        out_shape=[jax.ShapeDtypeStruct((rows, w), BF16) for w in rebuilt + [units] * 2]
         + [jax.ShapeDtypeStruct((2, rows, half), BF16)] * 4,
-        input_output_aliases={6 + tiles + i: i for i in range(len(earlier))},
         compiler_params=limit(56),
-    )(place, *routed, active, slope, down_w, gate_w, up_w, *earlier)
-
-
-def weight_grads_body(d_gate, d_up, rows_in, for_gate, for_up):
-    rows = rows_in[...]
-    for_gate[...] = dot(d_gate[...], rows, TN).astype(BF16)
-    for_up[...] = dot(d_up[...], rows, TN).astype(BF16)
-
-
-def weight_grads(d_gate, d_up, rows_in):
-    rows, width = rows_in.shape
-    units = d_gate.shape[1]
+    )(place, *routed, active, slope, down_w, gate_w, up_w)
+
+
+def weight_grads_body(*refs):
+    *parts, rows_q, rows_d = refs[: len(refs) - (len(refs) - 2) // 3]
+    for i, out in enumerate(refs[len(refs) - len(parts) // 2 :]):
+        total = dot(parts[2 * i][...], rows_q[...], TN)
+        out[...] = (total + dot(parts[2 * i + 1][...], rows_d[...], TN)).astype(BF16)
+
+
+def weight_grads(pairs, rows):
+    width = rows[0].shape[1]
+    units = pairs[0][0].shape[1]
     step = 512
-    whole = pl.BlockSpec((rows, units), lambda i: (0, 0))
+    parts = [part for pair in pairs for part in pair]
     by_col = lambda i: (0, i)
     return pl.pallas_call(
         weight_grads_body,
         grid=(width // step,),
-        in_specs=[whole, whole, pl.BlockSpec((rows, step), by_col)],
-        out_specs=[pl.BlockSpec((units, step), by_col)] * 2,
-        out_shape=[jax.ShapeDtypeStruct((units, width), BF16)] * 2,
-        compiler_params=limit(48),
-    )(d_gate, d_up, rows_in)
+        in_specs=[pl.BlockSpec(part.shape, lambda i: (0, 0)) for part in parts]
+        + [pl.BlockSpec((part.shape[0], step), by_col) for part in rows],
+        out_specs=[pl.BlockSpec((units, step), by_col)] * len(pairs),
+        out_shape=[jax.ShapeDtypeStruct((units, width), BF16)] * len(pairs),
+        compiler_params=limit(58),
+    )(*parts, *rows)
 
 
 def swapped(x, flip):
@@ -708,7 +707,7 @@
     routed_d = exchanged(outbox_d)
 
     gate_w, up_w, down_w = w_gate[0].T, w_up[0].T, w_down[0]
-    rows_in, active, slope, hidden = expert_forward(
+    rows_q, rows_d, active_q, active_d, slope_q, slope_d, hidden_q, hidden_d = expert_forward(
         expert_inputs[0], gate_w, up_w, experts, capacity, cut, tail
     )
 
@@ -718,13 +717,12 @@
     mixed, states, scores, book = forward(query, key, value, cumulative, ends, gain, before)
     books = (*before[3], book)
 
-    weights = (active, slope, down_w, gate_w, up_w)
-    *whole, keep_a, send_a, keep_b, send_b = expert_cotangents(
-        place, routed_q, *weights, 0, ()
-    )
-    parts_q = (keep_a, send_a, keep_b, send_b)
-    routed, d_gate, d_up, *parts_d = expert_cotangents(
-        place, (routed_d,), *weights, experts * cut, whole
+    weights = (down_w, gate_w, up_w)
+    routed_q, gate_q, up_q, *parts_q = expert_cotangents(
+        place, routed_q, active_q, slope_q, *weights
+    )
+    gate_d, up_d, *parts_d = expert_cotangents(
+        place, (routed_d,), active_d, slope_d, *weights
     )
     summed = jnp.concatenate(
         [
@@ -734,8 +732,8 @@
         axis=1,
     )
     returned = exchanged(summed.reshape(slots, quarter))
-    grad_gate, grad_up = weight_grads(d_gate, d_up, rows_in)
-    grad_down = dot(hidden, routed, TN).astype(BF16)
+    grad_gate, grad_up = weight_grads(((gate_q, gate_d), (up_q, up_d)), (rows_q, rows_d))
+    (grad_down,) = weight_grads(((hidden_q, hidden_d),), (routed_q, routed_d))
 
     own_cols = lax.dynamic_slice_in_dim(d_out, place[0] * quarter, quarter, 1)
     picked = own_cols.astype(F32) + dot(pick, returned, TN)

time: 281 us -> 269 us (0.957)
  the two profiles are of different devices: /device:TPU:0 before, /device:TPU:1 now
where the time goes in v4:
time: 269 us; the launch traced here: 268 us
  waiting for transfers between devices  98.7 us (37%)
  Pallas kernels  77 us (29%)
  starting transfers between devices  66.1 us (25%)
  local copies, waits for them, and re-layouts  17.5 us (7%)
  other arithmetic  4.43 us (2%)
    all_to_all x3, waiting for transfers between devices, exchanged(): box = lax.all_to_all(box, SP, split_axis=0, concat_axis=0, tiled=True)  44.3 us
    ppermute x8, waiting for transfers between devices, swapped(): return lax.ppermute(x, 'tp', [(i, i ^ flip) for i in range(count)])  38.1 us
    ppermute x21, starting transfers between devices, shifted(): return lax.ppermute(x, axis, [(i, (i + by) % count) for i in range(count)])  30.6 us
    pallas_call x2, Pallas kernels, expert_cotangents(): pl.pallas_call(functools.partial(expert_body, tiles=tiles), grid_spec=plt...  24.9 us
    all_to_all x3, starting transfers between devices, exchanged(): box = lax.all_to_all(box, SP, split_axis=0, concat_axis=0, tiled=True)  22.3 us
    pallas_call x2, Pallas kernels, weight_grads(): pl.pallas_call(weight_grads_body, grid=(width // step,), in_specs=[pl.Blo...  19.6 us
    ppermute x21, waiting for transfers between devices, shifted(): return lax.ppermute(x, axis, [(i, (i + by) % count) for i in range(count)])  16.3 us
    pallas_call x1, Pallas kernels, expert_forward(): pl.pallas_call(functools.partial(expert_forward_body, orders=(group, capa...  16.3 us
  transfers between devices with their start and end apart: 33, of which 15 were waited for; matrix products, arithmetic and copies ran while one was open for 1% of the time, Pallas kernels for 27%

profile of v4, /device:TPU:1, one launch (start us, length us, event | category | flops | bytes accessed | tf_op | source)
XLA Modules:
  0.0 267.6 jit_solution(2290388279898617258)
XLA Ops:
  5.5 9.6 %all-to-all-start = ((bf16[32,16,512]{2,1,0:T(8,128)(2,1)}), bf16[32,16,512]{2,1,0:T(8,128)(2,1)S(1)}, u32[]{:S(2)}, u32[]{:S(2)}) async-start(bf16[32,16,512]{2,1,0:T(8,128)(2,1)} %bitcast.3), calls=%async_computation | async-start | bytes 1048576 | tf_op jit(solution)/shard_map/all_to_all | solution.py:682
  15.2 2.5 shard_map.182
  20.4 6.1 %all-to-all-done = bf16[32,16,512]{2,1,0:T(8,128)(2,1)S(1)} async-done(((bf16[32,16,512]{2,1,0:T(8,128)(2,1)}), bf16[32,16,512]{2,1,0:T(8,128)(2,1)S(1)}, u32[]{:S(2)}, u32[]{:S(2)}) %all-to-all-start) | async-done | bytes 524320 | tf_op jit(solution)/shard_map/all_to_all | solution.py:682
  26.6 4.8 %all-to-all-start.1 = ((bf16[32,24,2048]{2,1,0:T(8,128)(2,1)}), bf16[32,24,2048]{2,1,0:T(8,128)(2,1)}, u32[]{:S(2)}, u32[]{:S(2)}) async-start(bf16[32,24,2048]{2,1,0:T(8,128)(2,1)} %bitcast.53), calls=%async_computation.1 | async-start | bytes 6291456 | tf_op jit(solution)/shard_map/all_to_all | solution.py:682
  32.7 2.5 collective-permute-start.1
  36.3 16.3 %shard_map.180 = (bf16[512,2048]{1,0:T(8,128)(2,1)}, bf16[768,2048]{1,0:T(8,128)(2,1)}, bf16[512,704]{1,0:T(8,128)(2,1)}, bf16[768,704]{1,0:T(8,128)(2,1)}, bf16...) custom-call(bf16[1152,2048]{1,0:T(8,128)(2,1)} %bitcast.77, ...), custom_call_target="tpu_custom_call" | custom-call | tf_op jit(solution)/shard_map/pallas_call | solution.py:164
  52.6 18.7 %all-to-all-done.1 = bf16[32,24,2048]{2,1,0:T(8,128)(2,1)} async-done(((bf16[32,24,2048]{2,1,0:T(8,128)(2,1)}), bf16[32,24,2048]{2,1,0:T(8,128)(2,1)}, u32[]{:S(2)}, u32[]{:S(2)}) %all-to-all-start.1) | async-done | bytes 3145760 | tf_op jit(solution)/shard_map/all_to_all | solution.py:682
  71.3 13.8 %shard_map.183 = (bf16[768,704]{1,0:T(8,128)(2,1)}, bf16[768,704]{1,0:T(8,128)(2,1)}, bf16[2,768,256]{2,1,0:T(8,128)(2,1)}, bf16[2,768,256]{2,1,0:T(8,128)(2,1)}...) custom-call(s32[1]{0:T(128)} %bitcast.place, bf16[768,2048]{1,0:T(8,128)(2,1)} %bitcast.12.refs_0_.refs_3_, ...), custom_call_target="tpu_custom_call" | custom-call | tf_op jit(solution)/shard_map/pallas_call | solution.py:235
  85.1 2.8 %collective-permute-start.9 = (bf16[2,768,256]{2,1,0:T(8,128)(2,1)}, bf16[2,768,256]{2,1,0:T(8,128)(2,1)S(1)}, u32[]{:S(2)}, u32[]{:S(2)}) collective-permute-start(bf16[2,768,256]{2,1,0:T(8,128)(2,1)} %get-tuple-element.89), channel_id=1, source_target_pairs={{0,3},{1,2},{2,1},{3,0},{4,7},{5,6},{6,5},{7,4},{8,11},{9,10},{10,... | collective-permute-start | bytes 2359304 | tf_op jit(solution)/shard_map/ppermute | solution.py:280
  88.6 11.2 %shard_map.181 = (bf16[512,2048]{1,0:T(8,128)(2,1)}, bf16[512,704]{1,0:T(8,128)(2,1)}, bf16[512,704]{1,0:T(8,128)(2,1)}, bf16[2,512,256]{2,1,0:T(8,128)(2,1)}, b...) custom-call(s32[1]{0:T(128)} %bitcast.place, bf16[512,512]{1,0:T(8,128)(2,1)} %bitcast.82, ...), custom_call_target="tpu_custom_call" | custom-call | tf_op jit(solution)/shard_map/pallas_call | solution.py:235
  101.6 9.3 %collective-permute-done.3.got_a = bf16[2,512,256]{2,1,0:T(8,128)(2,1)S(1)} collective-permute-done((bf16[2,512,256]{2,1,0:T(8,128)(2,1)}, bf16[2,512,256]{2,1,0:T(8,128)(2,1)S(1)}, u32[]{:S(2)}, u32[]{:S(2)}) %collective-permute-start.3) | collective-permute-done | bytes 524320 | tf_op jit(solution)/shard_map/ppermute | solution.py:280
  112.3 15.4 %collective-permute-done.7.got_a = bf16[2,768,256]{2,1,0:T(8,128)(2,1)S(1)} collective-permute-done((bf16[2,768,256]{2,1,0:T(8,128)(2,1)S(1)}, bf16[2,768,256]{2,1,0:T(8,128)(2,1)S(1)}, u32[]{:S(2)}, u32[]{:S(2)}) %collective-permute-start.7) | collective-permute-done | bytes 786464 | tf_op jit(solution)/shard_map/ppermute | solution.py:280
  128.3 13.5 %collective-permute-done.6.last_b = bf16[512,256]{1,0:T(8,128)(2,1)S(1)} collective-permute-done((bf16[512,256]{1,0:T(8,128)(2,1)S(1)}, bf16[512,256]{1,0:T(8,128)(2,1)S(1)}, u32[]{:S(2)}, u32[]{:S(2)}) %collective-permute-start.6) | collective-permute-done | bytes 262176 | tf_op jit(solution)/shard_map/ppermute | solution.py:280
  143.4 7.9 %all-to-all-start.2 = ((bf16[32,40,512]{2,1,0:T(8,128)(2,1)}), bf16[32,40,512]{2,1,0:T(8,128)(2,1)}, u32[]{:S(2)}, u32[]{:S(2)}) async-start(bf16[32,40,512]{2,1,0:T(8,128)(2,1)} %pad_maximum_fusion), calls=%async_computation.2 | async-start | bytes 2621440 | tf_op jit(solution)/shard_map/all_to_all | solution.py:682
  151.3 19.4 %all-to-all-done.2 = bf16[32,40,512]{2,1,0:T(8,128)(2,1)} async-done(((bf16[32,40,512]{2,1,0:T(8,128)(2,1)}), bf16[32,40,512]{2,1,0:T(8,128)(2,1)}, u32[]{:S(2)}, u32[]{:S(2)}) %all-to-all-start.2) | async-done | bytes 1310752 | tf_op jit(solution)/shard_map/all_to_all | solution.py:682
  170.8 2.6 fusion.a
  173.5 2.7 collective-permute-start.12
  178.3 2.1 collective-permute-start.15
  188.1 2.7 collective-permute-start.14
  192.2 2.1 collective-permute-start.19
  195.5 2.1 collective-permute-start.21
  197.5 3.8 %collective-permute-done.20.refs_2_ = f32[264,128]{1,0:T(8,128)S(1)} collective-permute-done((f32[264,128]{1,0:T(8,128)S(1)}, f32[264,128]{1,0:T(8,128)S(1)}, u32[]{:S(2)}, u32[]{:S(2)}) %collective-permute-start.20) | collective-permute-done | bytes 135200 | tf_op jit(solution)/shard_map/ppermute | solution.py:322
  210.3 8.0 %all-to-all-start.3 = ((bf16[32,64,256]{2,1,0:T(8,128)(2,1)}), bf16[32,64,256]{2,1,0:T(8,128)(2,1)}, u32[]{:S(2)}, u32[]{:S(2)}) async-start(bf16[32,64,256]{2,1,0:T(8,128)(2,1)} %bitcast.34), calls=%async_computation.3 | async-start | bytes 2097152 | tf_op jit(solution)/shard_map/all_to_all | solution.py:750
  219.6 2.0 shard_map.193
  224.5 2.4 collective-permute-start.24
  228.1 6.5 %collective-permute-done.23.refs_1_ = bf16[256,128]{1,0:T(8,128)(2,1)S(1)} collective-permute-done((bf16[256,128]{1,0:T(8,128)(2,1)S(1)}, bf16[256,128]{1,0:T(8,128)(2,1)S(1)}, u32[]{:S(2)}, u32[]{:S(2)}) %collective-permute-start.23) | collective-permute-done | bytes 65568 | tf_op jit(solution)/shard_map/ppermute | solution.py:322
  237.3 2.5 collective-permute-start.27
  240.9 7.8 %shard_map.185 = bf16[704,2048]{1,0:T(8,128)(2,1)} custom-call(bf16[512,704]{1,0:T(8,128)(2,1)} %get-tuple-element.78.refs_0_, bf16[768,704]{1,0:T(8,128)(2,1)} %get-tuple-element.79.refs_1_, bf16[512,2048]{1,0:T(8,128)(2,1)} %get-tuple-element.80.refs_2_, bf16[768,2048]{1,0:T(8,128)(2,1)} %bitcast.12.refs_0_.refs_3_), custom_call_target="tpu_custom_call" | custom-call | tf_op jit(solution)/shard_map/pallas_call | solution.py:267
  248.8 11.8 %shard_map.184 = (bf16[704,2048]{1,0:T(8,128)(2,1)}, bf16[704,2048]{1,0:T(8,128)(2,1)}) custom-call(bf16[512,704]{1,0:T(8,128)(2,1)} %get-tuple-element.66.refs_0_, bf16[768,704]{1,0:T(8,128)(2,1)} %get-tuple-element.71.refs_1_, bf16[512,704]{1,0:T(8,128)(2,1)} %get-tuple-element.72.refs_2_, bf16[768,704]{1,0:T(8,128)(2,1)} %get-tuple-element.73.refs_3_, ...), custom_call_target="tpu_custom_call" | custom-call | tf_op jit(solution)/shard_map/pallas_call | solution.py:267
  260.6 2.0 shard_map.194
  262.7 2.9 %shard_map.197 = (bf16[512,128]{1,0:T(8,128)(2,1)}, bf16[512,128]{1,0:T(8,128)(2,1)}, bf16[512,256]{1,0:T(8,128)(2,1)}, f32[512,128]{1,0:T(8,128)}) custom-call(bf16[512,128]{1,0:T(8,128)(2,1)S(1)} %bitcast.58, bf16[512,128]{1,0:T(8,128)(2,1)S(1)} %bitcast.62, bf16[512,256]{1,0:T(8,128)(2,1)S(1)} %bitcast.52, f32[512,128]{1,0:T(8,128)S(1)} %get-tuple-element.90.cumulative, ...), custom_call_target="tpu_custom_call" | custom-call | tf_op jit(solution)/shard_map/pallas_call | solution.py:539
  265.5 2.0 convert_reduce_fusion
  (134 shorter events, 46.8 us)
Async XLA Ops:
  5.5 21.0 %all-to-all-start = ((bf16[32,16,512]{2,1,0:T(8,128)(2,1)}), bf16[32,16,512]{2,1,0:T(8,128)(2,1)S(1)}, u32[]{:S(2)}, u32[]{:S(2)}) async-start(bf16[32,16,512]{2,1,0:T(8,128)(2,1)} %bitcast.3), calls=%async_computation | async-start | bytes 1048576 | tf_op jit(solution)/shard_map/all_to_all | solution.py:682
  26.6 44.7 %all-to-all-start.1 = ((bf16[32,24,2048]{2,1,0:T(8,128)(2,1)}), bf16[32,24,2048]{2,1,0:T(8,128)(2,1)}, u32[]{:S(2)}, u32[]{:S(2)}) async-start(bf16[32,24,2048]{2,1,0:T(8,128)(2,1)} %bitcast.53), calls=%async_computation.1 | async-start | bytes 6291456 | tf_op jit(solution)/shard_map/all_to_all | solution.py:682
  31.4 56.5 %collective-permute-start = (bf16[512,512]{1,0:T(8,128)(2,1)S(1)}, bf16[512,512]{1,0:T(8,128)(2,1)S(1)}, u32[]{:S(2)}, u32[]{:S(2)}) collective-permute-start(bf16[512,512]{1,0:T(8,128)(2,1)S(1)} %bitcast.79), channel_id=1, source_target_pairs={{0,1},{1,2},{2,3},{3,0},{4,5},{5,6},{6,7},{7,4},{8,9},{9,10},{10,1... | collective-permute-start | bytes 1572872 | tf_op jit(solution)/shard_map/ppermute | solution.py:322
  32.7 55.2 %collective-permute-start.1 = (bf16[512,512]{1,0:T(8,128)(2,1)S(1)}, bf16[512,512]{1,0:T(8,128)(2,1)}, u32[]{:S(2)}, u32[]{:S(2)}) collective-permute-start(bf16[512,512]{1,0:T(8,128)(2,1)S(1)} %bitcast.80), channel_id=1, source_target_pairs={{0,2},{1,3},{2,0},{3,1},{4,6},{5,7},{6,4},{7,5},{8,10},{9,11},{10,... | collective-permute-start | bytes 1572872 | tf_op jit(solution)/shard_map/ppermute | solution.py:322
  35.1 52.7 %collective-permute-start.2 = (bf16[512,512]{1,0:T(8,128)(2,1)S(1)}, bf16[512,512]{1,0:T(8,128)(2,1)}, u32[]{:S(2)}, u32[]{:S(2)}) collective-permute-start(bf16[512,512]{1,0:T(8,128)(2,1)S(1)} %bitcast.81), channel_id=1, source_target_pairs={{0,3},{1,0},{2,1},{3,2},{4,7},{5,4},{6,5},{7,6},{8,11},{9,8},{10,9... | collective-permute-start | bytes 1572872 | tf_op jit(solution)/shard_map/ppermute | solution.py:322
  85.1 27.1 %collective-permute-start.9 = (bf16[2,768,256]{2,1,0:T(8,128)(2,1)}, bf16[2,768,256]{2,1,0:T(8,128)(2,1)S(1)}, u32[]{:S(2)}, u32[]{:S(2)}) collective-permute-start(bf16[2,768,256]{2,1,0:T(8,128)(2,1)} %get-tuple-element.89), channel_id=1, source_target_pairs={{0,3},{1,2},{2,1},{3,0},{4,7},{5,6},{6,5},{7,4},{8,11},{9,10},{10,... | collective-permute-start | bytes 2359304 | tf_op jit(solution)/shard_map/ppermute | solution.py:280
  99.9 11.0 %collective-permute-start.3 = (bf16[2,512,256]{2,1,0:T(8,128)(2,1)}, bf16[2,512,256]{2,1,0:T(8,128)(2,1)S(1)}, u32[]{:S(2)}, u32[]{:S(2)}) collective-permute-start(bf16[2,512,256]{2,1,0:T(8,128)(2,1)} %get-tuple-element.83), channel_id=1, source_target_pairs={{0,1},{1,0},{2,3},{3,2},{4,5},{5,4},{6,7},{7,6},{8,9},{9,8},{10,11... | collective-permute-start | bytes 1572872 | tf_op jit(solution)/shard_map/ppermute | solution.py:280
  100.0 27.8 %collective-permute-start.7 = (bf16[2,768,256]{2,1,0:T(8,128)(2,1)S(1)}, bf16[2,768,256]{2,1,0:T(8,128)(2,1)S(1)}, u32[]{:S(2)}, u32[]{:S(2)}) collective-permute-start(bf16[2,768,256]{2,1,0:T(8,128)(2,1)S(1)} %copy-done.34), channel_id=1, source_target_pairs={{0,1},{1,0},{2,3},{3,2},{4,5},{5,4},{6,7},{7,6},{8,9},{9,8},{10,11... | collective-permute-start | bytes 2359304 | tf_op jit(solution)/shard_map/ppermute | solution.py:280
  101.4 26.7 %collective-permute-start.5 = (bf16[2,512,256]{2,1,0:T(8,128)(2,1)}, bf16[2,512,256]{2,1,0:T(8,128)(2,1)S(1)}, u32[]{:S(2)}, u32[]{:S(2)}) collective-permute-start(bf16[2,512,256]{2,1,0:T(8,128)(2,1)} %get-tuple-element.85), channel_id=1, source_target_pairs={{0,3},{1,2},{2,1},{3,0},{4,7},{5,6},{6,5},{7,4},{8,11},{9,10},{10,... | collective-permute-start | bytes 1572872 | tf_op jit(solution)/shard_map/ppermute | solution.py:280
  111.9 16.4 %collective-permute-start.4 = (bf16[512,256]{1,0:T(8,128)(2,1)S(1)}, bf16[512,256]{1,0:T(8,128)(2,1)S(1)}, u32[]{:S(2)}, u32[]{:S(2)}) collective-permute-start(bf16[512,256]{1,0:T(8,128)(2,1)S(1)} %fusion.3), channel_id=1, source_target_pairs={{0,3},{1,2},{2,1},{3,0},{4,7},{5,6},{6,5},{7,4},{8,11},{9,10},{10,... | collective-permute-start | bytes 786440 | tf_op jit(solution)/shard_map/ppermute | solution.py:280
  112.3 29.7 %collective-permute-start.10 = (bf16[768,256]{1,0:T(8,128)(2,1)S(1)}, bf16[768,256]{1,0:T(8,128)(2,1)S(1)}, u32[]{:S(2)}, u32[]{:S(2)}) collective-permute-start(bf16[768,256]{1,0:T(8,128)(2,1)S(1)} %fusion.2), channel_id=1, source_target_pairs={{0,1},{1,0},{2,3},{3,2},{4,5},{5,4},{6,7},{7,6},{8,9},{9,8},{10,11... | collective-permute-start | bytes 1179656 | tf_op jit(solution)/shard_map/ppermute | solution.py:280
  127.8 14.2 %collective-permute-start.8 = (bf16[768,256]{1,0:T(8,128)(2,1)S(1)}, bf16[768,256]{1,0:T(8,128)(2,1)S(1)}, u32[]{:S(2)}, u32[]{:S(2)}) collective-permute-start(bf16[768,256]{1,0:T(8,128)(2,1)S(1)} %fusion.1), channel_id=1, source_target_pairs={{0,3},{1,2},{2,1},{3,0},{4,7},{5,6},{6,5},{7,4},{8,11},{9,10},{10,... | collective-permute-start | bytes 1179656 | tf_op jit(solution)/shard_map/ppermute | solution.py:280
  128.2 13.6 %collective-permute-start.6 = (bf16[512,256]{1,0:T(8,128)(2,1)S(1)}, bf16[512,256]{1,0:T(8,128)(2,1)S(1)}, u32[]{:S(2)}, u32[]{:S(2)}) collective-permute-start(bf16[512,256]{1,0:T(8,128)(2,1)S(1)} %fusion.4), channel_id=1, source_target_pairs={{0,1},{1,0},{2,3},{3,2},{4,5},{5,4},{6,7},{7,6},{8,9},{9,8},{10,11... | collective-permute-start | bytes 786440 | tf_op jit(solution)/shard_map/ppermute | solution.py:280
  143.4 27.3 %all-to-all-start.2 = ((bf16[32,40,512]{2,1,0:T(8,128)(2,1)}), bf16[32,40,512]{2,1,0:T(8,128)(2,1)}, u32[]{:S(2)}, u32[]{:S(2)}) async-start(bf16[32,40,512]{2,1,0:T(8,128)(2,1)} %pad_maximum_fusion), calls=%async_computation.2 | async-start | bytes 2621440 | tf_op jit(solution)/shard_map/all_to_all | solution.py:682
  173.4 13.2 %collective-permute-start.11 = (bf16[512,512]{1,0:T(8,128)(2,1)S(1)}, bf16[512,512]{1,0:T(8,128)(2,1)S(1)}, u32[]{:S(2)}, u32[]{:S(2)}) collective-permute-start(bf16[512,512]{1,0:T(8,128)(2,1)S(1)} %fusion.a), channel_id=1, source_target_pairs={{0,1},{1,2},{2,3},{3,0},{4,5},{5,6},{6,7},{7,4},{8,9},{9,10},{10,1... | collective-permute-start | bytes 1572872 | tf_op jit(solution)/shard_map/ppermute | solution.py:322
  173.5 13.9 %collective-permute-start.12 = (bf16[512,512]{1,0:T(8,128)(2,1)S(1)}, bf16[512,512]{1,0:T(8,128)(2,1)S(1)}, u32[]{:S(2)}, u32[]{:S(2)}) collective-permute-start(bf16[512,512]{1,0:T(8,128)(2,1)S(1)} %fusion.a), channel_id=1, source_target_pairs={{0,3},{1,0},{2,1},{3,2},{4,7},{5,4},{6,5},{7,6},{8,11},{9,8},{10,9... | collective-permute-start | bytes 1572872 | tf_op jit(solution)/shard_map/ppermute | solution.py:322
  178.3 3.1 %collective-permute-start.15 = (f32[264,128]{1,0:T(8,128)S(1)}, f32[264,128]{1,0:T(8,128)S(1)}, u32[]{:S(2)}, u32[]{:S(2)}) collective-permute-start(f32[264,128]{1,0:T(8,128)S(1)} %get-tuple-element.93.refs_0_), channel_id=1, source_target_pairs={{0,4},{4,0},{1,5},{5,1},{2,6},{6,2},{3,7},{7,3},{8,12},{12,8},{9,1... | collective-permute-start | bytes 405512 | tf_op jit(solution)/shard_map/ppermute | solution.py:322
  182.1 8.9 %collective-permute-start.16 = (f32[264,128]{1,0:T(8,128)S(1)}, f32[264,128]{1,0:T(8,128)S(1)}, u32[]{:S(2)}, u32[]{:S(2)}) collective-permute-start(f32[264,128]{1,0:T(8,128)S(1)} %get-tuple-element.94.refs_0_), channel_id=1, source_target_pairs={{0,8},{8,16},{16,24},{24,0},{1,9},{9,17},{17,25},{25,1},{2,10},{10... | collective-permute-start | bytes 405512 | tf_op jit(solution)/shard_map/ppermute | solution.py:322
  182.1 8.9 %collective-permute-start.17 = (f32[264,128]{1,0:T(8,128)S(1)}, f32[264,128]{1,0:T(8,128)S(1)}, u32[]{:S(2)}, u32[]{:S(2)}) collective-permute-start(f32[264,128]{1,0:T(8,128)S(1)} %get-tuple-element.94.refs_0_), channel_id=1, source_target_pairs={{0,16},{8,24},{16,0},{24,8},{1,17},{9,25},{17,1},{25,9},{2,18},{10... | collective-permute-start | bytes 405512 | tf_op jit(solution)/shard_map/ppermute | solution.py:322
  183.7 7.7 %collective-permute-start.18 = (f32[264,128]{1,0:T(8,128)S(1)}, f32[264,128]{1,0:T(8,128)S(1)}, u32[]{:S(2)}, u32[]{:S(2)}) collective-permute-start(f32[264,128]{1,0:T(8,128)S(1)} %get-tuple-element.94.refs_0_), channel_id=1, source_target_pairs={{0,24},{8,0},{16,8},{24,16},{1,25},{9,1},{17,9},{25,17},{2,26},{10... | collective-permute-start | bytes 405512 | tf_op jit(solution)/shard_map/ppermute | solution.py:322
  187.4 19.2 %collective-permute-start.13 = (bf16[256,512]{1,0:T(8,128)(2,1)}, bf16[256,512]{1,0:T(8,128)(2,1)}, u32[]{:S(2)}, u32[]{:S(2)}) collective-permute-start(bf16[256,512]{1,0:T(8,128)(2,1)} %slice.44), channel_id=1, source_target_pairs={{0,1},{1,2},{2,3},{3,0},{4,5},{5,6},{6,7},{7,4},{8,9},{9,10},{10,1... | collective-permute-start | bytes 786440 | tf_op jit(solution)/shard_map/ppermute | solution.py:322
  188.1 19.4 %collective-permute-start.14 = (bf16[256,512]{1,0:T(8,128)(2,1)}, bf16[256,512]{1,0:T(8,128)(2,1)}, u32[]{:S(2)}, u32[]{:S(2)}) collective-permute-start(bf16[256,512]{1,0:T(8,128)(2,1)} %slice.45), channel_id=1, source_target_pairs={{0,3},{1,0},{2,1},{3,2},{4,7},{5,4},{6,5},{7,6},{8,11},{9,8},{10,9... | collective-permute-start | bytes 786440 | tf_op jit(solution)/shard_map/ppermute | solution.py:322
  192.2 5.4 %collective-permute-start.19 = (f32[264,128]{1,0:T(8,128)S(1)}, f32[264,128]{1,0:T(8,128)S(1)}, u32[]{:S(2)}, u32[]{:S(2)}) collective-permute-start(f32[264,128]{1,0:T(8,128)S(1)} %get-tuple-element.95.refs_0_), channel_id=1, source_target_pairs={{0,32},{32,64},{64,96},{96,0},{1,33},{33,65},{65,97},{97,1},{2,34}... | collective-permute-start | bytes 405512 | tf_op jit(solution)/shard_map/ppermute | solution.py:322
  194.2 7.1 %collective-permute-start.20 = (f32[264,128]{1,0:T(8,128)S(1)}, f32[264,128]{1,0:T(8,128)S(1)}, u32[]{:S(2)}, u32[]{:S(2)}) collective-permute-start(f32[264,128]{1,0:T(8,128)S(1)} %get-tuple-element.95.refs_0_), channel_id=1, source_target_pairs={{0,64},{32,96},{64,0},{96,32},{1,65},{33,97},{65,1},{97,33},{2,66}... | collective-permute-start | bytes 405512 | tf_op jit(solution)/shard_map/ppermute | solution.py:322
  195.5 5.9 %collective-permute-start.21 = (f32[264,128]{1,0:T(8,128)S(1)}, f32[264,128]{1,0:T(8,128)S(1)}, u32[]{:S(2)}, u32[]{:S(2)}) collective-permute-start(f32[264,128]{1,0:T(8,128)S(1)} %get-tuple-element.95.refs_0_), channel_id=1, source_target_pairs={{0,96},{32,0},{64,32},{96,64},{1,97},{33,1},{65,33},{97,65},{2,98}... | collective-permute-start | bytes 405512 | tf_op jit(solution)/shard_map/ppermute | solution.py:322
  210.3 55.2 %all-to-all-start.3 = ((bf16[32,64,256]{2,1,0:T(8,128)(2,1)}), bf16[32,64,256]{2,1,0:T(8,128)(2,1)}, u32[]{:S(2)}, u32[]{:S(2)}) async-start(bf16[32,64,256]{2,1,0:T(8,128)(2,1)} %bitcast.34), calls=%async_computation.3 | async-start | bytes 2097152 | tf_op jit(solution)/shard_map/all_to_all | solution.py:750
  223.0 11.6 %collective-permute-start.23 = (bf16[256,128]{1,0:T(8,128)(2,1)S(1)}, bf16[256,128]{1,0:T(8,128)(2,1)S(1)}, u32[]{:S(2)}, u32[]{:S(2)}) collective-permute-start(bf16[256,128]{1,0:T(8,128)(2,1)S(1)} %get-tuple-element.109.refs_0_), channel_id=1, source_target_pairs={{0,8},{8,16},{16,24},{24,0},{1,9},{9,17},{17,25},{25,1},{2,10},{10... | collective-permute-start | bytes 196616 | tf_op jit(solution)/shard_map/ppermute | solution.py:322
  224.5 11.6 %collective-permute-start.24 = (bf16[256,128]{1,0:T(8,128)(2,1)S(1)}, bf16[256,128]{1,0:T(8,128)(2,1)S(1)}, u32[]{:S(2)}, u32[]{:S(2)}) collective-permute-start(bf16[256,128]{1,0:T(8,128)(2,1)S(1)} %get-tuple-element.109.refs_0_), channel_id=1, source_target_pairs={{0,16},{8,24},{16,0},{24,8},{1,17},{9,25},{17,1},{25,9},{2,18},{10... | collective-permute-start | bytes 196616 | tf_op jit(solution)/shard_map/ppermute | solution.py:322
  226.9 9.2 %collective-permute-start.25 = (bf16[256,128]{1,0:T(8,128)(2,1)S(1)}, bf16[256,128]{1,0:T(8,128)(2,1)S(1)}, u32[]{:S(2)}, u32[]{:S(2)}) collective-permute-start(bf16[256,128]{1,0:T(8,128)(2,1)S(1)} %get-tuple-element.109.refs_0_), channel_id=1, source_target_pairs={{0,24},{8,0},{16,8},{24,16},{1,25},{9,1},{17,9},{25,17},{2,26},{10... | collective-permute-start | bytes 196616 | tf_op jit(solution)/shard_map/ppermute | solution.py:322
  236.2 26.4 %collective-permute-start.26 = (bf16[256,128]{1,0:T(8,128)(2,1)S(1)}, bf16[256,128]{1,0:T(8,128)(2,1)S(1)}, u32[]{:S(2)}, u32[]{:S(2)}) collective-permute-start(bf16[256,128]{1,0:T(8,128)(2,1)S(1)} %get-tuple-element.110.refs_0_), channel_id=1, source_target_pairs={{0,32},{32,64},{64,96},{96,0},{1,33},{33,65},{65,97},{97,1},{2,34}... | collective-permute-start | bytes 196616 | tf_op jit(solution)/shard_map/ppermute | solution.py:322
  237.3 25.3 %collective-permute-start.27 = (bf16[256,128]{1,0:T(8,128)(2,1)S(1)}, bf16[256,128]{1,0:T(8,128)(2,1)S(1)}, u32[]{:S(2)}, u32[]{:S(2)}) collective-permute-start(bf16[256,128]{1,0:T(8,128)(2,1)S(1)} %get-tuple-element.110.refs_0_), channel_id=1, source_target_pairs={{0,64},{32,96},{64,0},{96,32},{1,65},{33,97},{65,1},{97,33},{2,66}... | collective-permute-start | bytes 196616 | tf_op jit(solution)/shard_map/ppermute | solution.py:322
  239.8 22.8 %collective-permute-start.28 = (bf16[256,128]{1,0:T(8,128)(2,1)S(1)}, bf16[256,128]{1,0:T(8,128)(2,1)S(1)}, u32[]{:S(2)}, u32[]{:S(2)}) collective-permute-start(bf16[256,128]{1,0:T(8,128)(2,1)S(1)} %get-tuple-element.110.refs_0_), channel_id=1, source_target_pairs={{0,96},{32,0},{64,32},{96,64},{1,97},{33,1},{65,33},{97,65},{2,98}... | collective-permute-start | bytes 196616 | tf_op jit(solution)/shard_map/ppermute | solution.py:322
  (36 other events, 343.1 us)

commit v5 on v4

--- a/solution.py
+++ b/solution.py
@@ -12,6 +12,7 @@
 BLK = 64
 PAD = 8
 SP = ("sp_0", "sp_1", "sp_2")
+TP = "tp"
 F32 = jnp.float32
 BF16 = jnp.bfloat16
 
@@ -84,8 +85,11 @@
     return jnp.where(inside, chosen * stride + ranks - least, -1)
 
 
-def route_body(place, d_out, chosen, weight, outbox, ranks, *, experts, most):
-    tokens = d_out.shape[0]
+def route_body(place, d_out, chosen, weight, outbox, ranks, rows, loaded, *, experts, most):
+    tokens, width = rows.shape
+    start = pl.multiple_of(place[0] * width, width)
+    copy = pltpu.make_async_copy(d_out.at[:, pl.ds(start, width)], rows, loaded)
+    copy.start()
     first, second = chosen[0:1, :], chosen[1:2, :]
     ids = grid_of((experts, tokens), 0)
     is_first, is_second = ids == first, ids == second
@@ -100,9 +104,8 @@
     ranks[1:2, :] = rank_b
     slot_a = slots_of(first, rank_a, 0, most, most)
     slot_b = slots_of(second, rank_b, 0, most, most)
-    width = outbox.shape[1]
-    rows = d_out[:, pl.ds(pl.multiple_of(place[0] * width, width), width)]
-    fill_outbox(rows, weight, slot_a, slot_b, outbox)
+    copy.wait()
+    fill_outbox(rows[...], weight, slot_a, slot_b, outbox)
 
 
 def refill_body(d_out, chosen, weight, ranks, outbox, pick, *, least, most, tail):
@@ -276,8 +279,8 @@
 
 
 def swapped(x, flip):
-    count = lax.axis_size("tp")
-    return lax.ppermute(x, "tp", [(i, i ^ flip) for i in range(count)])
+    count = lax.axis_size(TP)
+    return lax.ppermute(x, TP, [(i, i ^ flip) for i in range(count)])
 
 
 def plus(*terms):
@@ -324,10 +327,10 @@
 
 def gathered_ring(x):
     half = x.shape[0] // 2
-    below = shifted(x, "tp", 1)
-    above = shifted(x, "tp", -1)
+    below = shifted(x, TP, 1)
+    above = shifted(x, TP, -1)
     across = jnp.concatenate(
-        [shifted(below[:half], "tp", 1), shifted(above[half:], "tp", -1)], axis=0
+        [shifted(below[:half], TP, 1), shifted(above[half:], TP, -1)], axis=0
     )
     return x, below, above, across
 
@@ -672,8 +675,8 @@
     cut = PAD * 2
     tail = -(-(capacity - cut) // PAD) * PAD
     slots = experts * (cut + tail)
-    quarter = model_width // lax.axis_size("tp")
-    place = lax.axis_index("tp").reshape(1)
+    quarter = model_width // lax.axis_size(TP)
+    place = lax.axis_index(TP).reshape(1)
     chosen, weight = route_expert.T, route_weight.T
 
     def exchanged(box):
@@ -688,13 +691,14 @@
             jax.ShapeDtypeStruct((experts * cut, quarter), BF16),
             jax.ShapeDtypeStruct((2, tok_rows), jnp.int32),
         ],
-        mebibytes=20,
-        in_specs=[SMEM] + [VMEM] * 3,
+        mebibytes=58,
+        in_specs=[SMEM, pl.BlockSpec(memory_space=pltpu.HBM)] + [VMEM] * 2,
+        scratch_shapes=[pltpu.VMEM((tok_rows, quarter), BF16), pltpu.SemaphoreType.DMA(())],
     )(place, d_out, chosen, weight)
     tile = exchanged(outbox_q)
     routed_q = [tile]
-    for k in range(1, lax.axis_size("tp")):
-        routed_q.append(shifted(tile, "tp", k))
+    for k in range(1, lax.axis_size(TP)):
+        routed_q.append(shifted(tile, TP, k))
 
     outbox_d, pick = vmem_call(
         functools.partial(refill_body, least=cut, most=capacity, tail=tail),
@@ -762,7 +766,7 @@
 
 
 def solution(mesh):
-    finer = Mesh(mesh.devices.reshape(4, 4, 2, mesh.shape["tp"]), ("sp_0", "sp_1", "sp_2", "tp"))
+    finer = Mesh(mesh.devices.reshape(4, 4, 2, mesh.shape[TP]), (*SP, TP))
     return jax.shard_map(
         local,
         mesh=finer,
@@ -771,24 +775,24 @@
             P(SP, None),
             P(SP, None),
             P(SP, None, None),
-            P(SP, None, "tp"),
-            P(SP, None, "tp"),
-            P(SP, "tp", None),
-            P(None, "tp"),
-            P(SP, "tp", None),
-            P(SP, "tp", None),
-            P(SP, "tp", None),
-            P(SP, "tp", None),
+            P(SP, None, TP),
+            P(SP, None, TP),
+            P(SP, TP, None),
+            P(None, TP),
+            P(SP, TP, None),
+            P(SP, TP, None),
+            P(SP, TP, None),
+            P(SP, TP, None),
         ),
         out_specs=(
-            P(SP, None, "tp"),
-            P(SP, None, "tp"),
-            P(SP, "tp", None),
-            P(SP, "tp"),
-            P(SP, "tp", None),
-            P(SP, "tp", None),
-            P(SP, "tp", None),
-            P(SP, "tp", None),
+            P(SP, None, TP),
+            P(SP, None, TP),
+            P(SP, TP, None),
+            P(SP, TP),
+            P(SP, TP, None),
+            P(SP, TP, None),
+            P(SP, TP, None),
+            P(SP, TP, None),
         ),
         check_vma=False,
     )

time: 269 us -> 267 us (level)
    unnamed x71 -> x67, local copies, waits for them, and re-layouts: 15.1 us -> 12.8 us
where the time goes in v5:
time: 267 us; the launch traced here: 266 us
  waiting for transfers between devices  98.1 us (37%)
  Pallas kernels  78.6 us (29%)
  starting transfers between devices  66.1 us (25%)
  local copies, waits for them, and re-layouts  15.2 us (6%)
  other arithmetic  4.43 us (2%)
    all_to_all x3, waiting for transfers between devices, exchanged(): box = lax.all_to_all(box, SP, split_axis=0, concat_axis=0, tiled=True)  43.6 us
    ppermute x8, waiting for transfers between devices, swapped(): return lax.ppermute(x, TP, [(i, i ^ flip) for i in range(count)])  38.2 us
    ppermute x21, starting transfers between devices, shifted(): return lax.ppermute(x, axis, [(i, (i + by) % count) for i in range(count)])  30.6 us
    pallas_call x2, Pallas kernels, expert_cotangents(): pl.pallas_call(functools.partial(expert_body, tiles=tiles), grid_spec=plt...  24.9 us
    all_to_all x3, starting transfers between devices, exchanged(): box = lax.all_to_all(box, SP, split_axis=0, concat_axis=0, tiled=True)  22.3 us
    pallas_call x2, Pallas kernels, weight_grads(): pl.pallas_call(weight_grads_body, grid=(width // step,), in_specs=[pl.Blo...  19.6 us
    pallas_call x1, Pallas kernels, expert_forward(): pl.pallas_call(functools.partial(expert_forward_body, orders=(group, capa...  16.3 us
    ppermute x21, waiting for transfers between devices, shifted(): return lax.ppermute(x, axis, [(i, (i + by) % count) for i in range(count)])  16.3 us
  transfers between devices with their start and end apart: 33, of which 15 were waited for; matrix products, arithmetic and copies ran while one was open for 1% of the time, Pallas kernels for 27%

profile of v5, /device:TPU:1, one launch (start us, length us, event | category | flops | bytes accessed | tf_op | source)
XLA Modules:
  0.0 266.2 jit_solution(10959789969764727108)
XLA Ops:
  0.7 3.5 %shard_map.179 = (bf16[512,512]{1,0:T(8,128)(2,1)}, s32[2,512]{1,0:T(2,128)}) custom-call(s32[1]{0:T(128)} %bitcast.place, bf16[512,2048]{1,0:T(8,128)(2,1)} %d_out.3, s32[2,512]{1,0:T(2,128)} %bitcast.65, f32[2,512]{1,0:T(2,128)} %bitcast.67), custom_call_target="tpu_custom_call" | custom-call | tf_op jit(solution)/shard_map/pallas_call | solution.py:688
  4.2 9.6 %all-to-all-start = ((bf16[32,16,512]{2,1,0:T(8,128)(2,1)}), bf16[32,16,512]{2,1,0:T(8,128)(2,1)S(1)}, u32[]{:S(2)}, u32[]{:S(2)}) async-start(bf16[32,16,512]{2,1,0:T(8,128)(2,1)} %bitcast.83), calls=%async_computation | async-start | bytes 1048576 | tf_op jit(solution)/shard_map/all_to_all | solution.py:685
  14.5 2.5 shard_map.182
  19.8 5.4 %all-to-all-done = bf16[32,16,512]{2,1,0:T(8,128)(2,1)S(1)} async-done(((bf16[32,16,512]{2,1,0:T(8,128)(2,1)}), bf16[32,16,512]{2,1,0:T(8,128)(2,1)S(1)}, u32[]{:S(2)}, u32[]{:S(2)}) %all-to-all-start) | async-done | bytes 524320 | tf_op jit(solution)/shard_map/all_to_all | solution.py:685
  25.3 4.8 %all-to-all-start.1 = ((bf16[32,24,2048]{2,1,0:T(8,128)(2,1)}), bf16[32,24,2048]{2,1,0:T(8,128)(2,1)}, u32[]{:S(2)}, u32[]{:S(2)}) async-start(bf16[32,24,2048]{2,1,0:T(8,128)(2,1)} %bitcast.53), calls=%async_computation.1 | async-start | bytes 6291456 | tf_op jit(solution)/shard_map/all_to_all | solution.py:685
  31.4 2.5 collective-permute-start.1
  35.0 16.3 %shard_map.180 = (bf16[512,2048]{1,0:T(8,128)(2,1)}, bf16[768,2048]{1,0:T(8,128)(2,1)}, bf16[512,704]{1,0:T(8,128)(2,1)}, bf16[768,704]{1,0:T(8,128)(2,1)}, bf16...) custom-call(bf16[1152,2048]{1,0:T(8,128)(2,1)} %bitcast.77, ...), custom_call_target="tpu_custom_call" | custom-call | tf_op jit(solution)/shard_map/pallas_call | solution.py:167
  51.3 18.7 %all-to-all-done.1 = bf16[32,24,2048]{2,1,0:T(8,128)(2,1)} async-done(((bf16[32,24,2048]{2,1,0:T(8,128)(2,1)}), bf16[32,24,2048]{2,1,0:T(8,128)(2,1)}, u32[]{:S(2)}, u32[]{:S(2)}) %all-to-all-start.1) | async-done | bytes 3145760 | tf_op jit(solution)/shard_map/all_to_all | solution.py:685
  70.0 13.7 %shard_map.183 = (bf16[768,704]{1,0:T(8,128)(2,1)}, bf16[768,704]{1,0:T(8,128)(2,1)}, bf16[2,768,256]{2,1,0:T(8,128)(2,1)}, bf16[2,768,256]{2,1,0:T(8,128)(2,1)}...) custom-call(s32[1]{0:T(128)} %bitcast.place, bf16[768,2048]{1,0:T(8,128)(2,1)} %bitcast.12.refs_0_.refs_3_, ...), custom_call_target="tpu_custom_call" | custom-call | tf_op jit(solution)/shard_map/pallas_call | solution.py:238
  83.7 2.8 %collective-permute-start.9 = (bf16[2,768,256]{2,1,0:T(8,128)(2,1)}, bf16[2,768,256]{2,1,0:T(8,128)(2,1)S(1)}, u32[]{:S(2)}, u32[]{:S(2)}) collective-permute-start(bf16[2,768,256]{2,1,0:T(8,128)(2,1)} %get-tuple-element.89), channel_id=1, source_target_pairs={{0,3},{1,2},{2,1},{3,0},{4,7},{5,6},{6,5},{7,4},{8,11},{9,10},{10,... | collective-permute-start | bytes 2359304 | tf_op jit(solution)/shard_map/ppermute | solution.py:283
  87.3 11.2 %shard_map.181 = (bf16[512,2048]{1,0:T(8,128)(2,1)}, bf16[512,704]{1,0:T(8,128)(2,1)}, bf16[512,704]{1,0:T(8,128)(2,1)}, bf16[2,512,256]{2,1,0:T(8,128)(2,1)}, b...) custom-call(s32[1]{0:T(128)} %bitcast.place, bf16[512,512]{1,0:T(8,128)(2,1)} %bitcast.82, ...), custom_call_target="tpu_custom_call" | custom-call | tf_op jit(solution)/shard_map/pallas_call | solution.py:238
  100.2 9.3 %collective-permute-done.3.got_a = bf16[2,512,256]{2,1,0:T(8,128)(2,1)S(1)} collective-permute-done((bf16[2,512,256]{2,1,0:T(8,128)(2,1)}, bf16[2,512,256]{2,1,0:T(8,128)(2,1)S(1)}, u32[]{:S(2)}, u32[]{:S(2)}) %collective-permute-start.3) | collective-permute-done | bytes 524320 | tf_op jit(solution)/shard_map/ppermute | solution.py:283
  111.0 15.4 %collective-permute-done.7.got_a = bf16[2,768,256]{2,1,0:T(8,128)(2,1)S(1)} collective-permute-done((bf16[2,768,256]{2,1,0:T(8,128)(2,1)S(1)}, bf16[2,768,256]{2,1,0:T(8,128)(2,1)S(1)}, u32[]{:S(2)}, u32[]{:S(2)}) %collective-permute-start.7) | collective-permute-done | bytes 786464 | tf_op jit(solution)/shard_map/ppermute | solution.py:283
  126.9 13.5 %collective-permute-done.6.last_b = bf16[512,256]{1,0:T(8,128)(2,1)S(1)} collective-permute-done((bf16[512,256]{1,0:T(8,128)(2,1)S(1)}, bf16[512,256]{1,0:T(8,128)(2,1)S(1)}, u32[]{:S(2)}, u32[]{:S(2)}) %collective-permute-start.6) | collective-permute-done | bytes 262176 | tf_op jit(solution)/shard_map/ppermute | solution.py:283
  142.1 7.9 %all-to-all-start.2 = ((bf16[32,40,512]{2,1,0:T(8,128)(2,1)}), bf16[32,40,512]{2,1,0:T(8,128)(2,1)}, u32[]{:S(2)}, u32[]{:S(2)}) async-start(bf16[32,40,512]{2,1,0:T(8,128)(2,1)} %pad_maximum_fusion), calls=%async_computation.2 | async-start | bytes 2621440 | tf_op jit(solution)/shard_map/all_to_all | solution.py:685
  150.0 19.4 %all-to-all-done.2 = bf16[32,40,512]{2,1,0:T(8,128)(2,1)} async-done(((bf16[32,40,512]{2,1,0:T(8,128)(2,1)}), bf16[32,40,512]{2,1,0:T(8,128)(2,1)}, u32[]{:S(2)}, u32[]{:S(2)}) %all-to-all-start.2) | async-done | bytes 1310752 | tf_op jit(solution)/shard_map/all_to_all | solution.py:685
  169.4 2.6 fusion.a
  172.2 2.7 %collective-permute-start.12 = (bf16[512,512]{1,0:T(8,128)(2,1)S(1)}, bf16[512,512]{1,0:T(8,128)(2,1)S(1)}, u32[]{:S(2)}, u32[]{:S(2)}) collective-permute-start(bf16[512,512]{1,0:T(8,128)(2,1)S(1)} %fusion.a), channel_id=1, source_target_pairs={{0,3},{1,0},{2,1},{3,2},{4,7},{5,4},{6,5},{7,6},{8,11},{9,8},{10,9... | collective-permute-start | bytes 1572872 | tf_op jit(solution)/shard_map/ppermute | solution.py:325
  177.0 2.1 collective-permute-start.15
  186.8 2.7 %collective-permute-start.14 = (bf16[256,512]{1,0:T(8,128)(2,1)}, bf16[256,512]{1,0:T(8,128)(2,1)}, u32[]{:S(2)}, u32[]{:S(2)}) collective-permute-start(bf16[256,512]{1,0:T(8,128)(2,1)} %slice.45), channel_id=1, source_target_pairs={{0,3},{1,0},{2,1},{3,2},{4,7},{5,4},{6,5},{7,6},{8,11},{9,8},{10,9... | collective-permute-start | bytes 786440 | tf_op jit(solution)/shard_map/ppermute | solution.py:325
  190.8 2.1 collective-permute-start.19
  194.1 2.1 collective-permute-start.21
  196.2 3.8 %collective-permute-done.20.refs_2_ = f32[264,128]{1,0:T(8,128)S(1)} collective-permute-done((f32[264,128]{1,0:T(8,128)S(1)}, f32[264,128]{1,0:T(8,128)S(1)}, u32[]{:S(2)}, u32[]{:S(2)}) %collective-permute-start.20) | collective-permute-done | bytes 135200 | tf_op jit(solution)/shard_map/ppermute | solution.py:325
  209.0 8.0 %all-to-all-start.3 = ((bf16[32,64,256]{2,1,0:T(8,128)(2,1)}), bf16[32,64,256]{2,1,0:T(8,128)(2,1)}, u32[]{:S(2)}, u32[]{:S(2)}) async-start(bf16[32,64,256]{2,1,0:T(8,128)(2,1)} %bitcast.34), calls=%async_computation.3 | async-start | bytes 2097152 | tf_op jit(solution)/shard_map/all_to_all | solution.py:754
  218.2 2.0 shard_map.193
  223.1 2.4 collective-permute-start.24
  226.7 6.5 %collective-permute-done.23.refs_1_ = bf16[256,128]{1,0:T(8,128)(2,1)S(1)} collective-permute-done((bf16[256,128]{1,0:T(8,128)(2,1)S(1)}, bf16[256,128]{1,0:T(8,128)(2,1)S(1)}, u32[]{:S(2)}, u32[]{:S(2)}) %collective-permute-start.23) | collective-permute-done | bytes 65568 | tf_op jit(solution)/shard_map/ppermute | solution.py:325
  236.0 2.5 collective-permute-start.27
  239.6 7.8 %shard_map.185 = bf16[704,2048]{1,0:T(8,128)(2,1)} custom-call(bf16[512,704]{1,0:T(8,128)(2,1)} %get-tuple-element.78.refs_0_, bf16[768,704]{1,0:T(8,128)(2,1)} %get-tuple-element.79.refs_1_, bf16[512,2048]{1,0:T(8,128)(2,1)} %get-tuple-element.80.refs_2_, bf16[768,2048]{1,0:T(8,128)(2,1)} %bitcast.12.refs_0_.refs_3_), custom_call_target="tpu_custom_call" | custom-call | tf_op jit(solution)/shard_map/pallas_call | solution.py:270
  247.5 11.8 %shard_map.184 = (bf16[704,2048]{1,0:T(8,128)(2,1)}, bf16[704,2048]{1,0:T(8,128)(2,1)}) custom-call(bf16[512,704]{1,0:T(8,128)(2,1)} %get-tuple-element.66.refs_0_, bf16[768,704]{1,0:T(8,128)(2,1)} %get-tuple-element.71.refs_1_, bf16[512,704]{1,0:T(8,128)(2,1)} %get-tuple-element.72.refs_2_, bf16[768,704]{1,0:T(8,128)(2,1)} %get-tuple-element.73.refs_3_, ...), custom_call_target="tpu_custom_call" | custom-call | tf_op jit(solution)/shard_map/pallas_call | solution.py:270
  259.2 2.0 shard_map.194
  261.3 2.9 %shard_map.197 = (bf16[512,128]{1,0:T(8,128)(2,1)}, bf16[512,128]{1,0:T(8,128)(2,1)}, bf16[512,256]{1,0:T(8,128)(2,1)}, f32[512,128]{1,0:T(8,128)}) custom-call(bf16[512,128]{1,0:T(8,128)(2,1)S(1)} %bitcast.58, bf16[512,128]{1,0:T(8,128)(2,1)S(1)} %bitcast.62, bf16[512,256]{1,0:T(8,128)(2,1)S(1)} %bitcast.52, f32[512,128]{1,0:T(8,128)S(1)} %get-tuple-element.90.cumulative, ...), custom_call_target="tpu_custom_call" | custom-call | tf_op jit(solution)/shard_map/pallas_call | solution.py:542
  (130 shorter events, 44.6 us)
Async XLA Ops:
  4.2 21.0 %all-to-all-start = ((bf16[32,16,512]{2,1,0:T(8,128)(2,1)}), bf16[32,16,512]{2,1,0:T(8,128)(2,1)S(1)}, u32[]{:S(2)}, u32[]{:S(2)}) async-start(bf16[32,16,512]{2,1,0:T(8,128)(2,1)} %bitcast.83), calls=%async_computation | async-start | bytes 1048576 | tf_op jit(solution)/shard_map/all_to_all | solution.py:685
  25.3 44.7 %all-to-all-start.1 = ((bf16[32,24,2048]{2,1,0:T(8,128)(2,1)}), bf16[32,24,2048]{2,1,0:T(8,128)(2,1)}, u32[]{:S(2)}, u32[]{:S(2)}) async-start(bf16[32,24,2048]{2,1,0:T(8,128)(2,1)} %bitcast.53), calls=%async_computation.1 | async-start | bytes 6291456 | tf_op jit(solution)/shard_map/all_to_all | solution.py:685
  30.1 56.4 %collective-permute-start = (bf16[512,512]{1,0:T(8,128)(2,1)S(1)}, bf16[512,512]{1,0:T(8,128)(2,1)S(1)}, u32[]{:S(2)}, u32[]{:S(2)}) collective-permute-start(bf16[512,512]{1,0:T(8,128)(2,1)S(1)} %bitcast.79), channel_id=1, source_target_pairs={{0,1},{1,2},{2,3},{3,0},{4,5},{5,6},{6,7},{7,4},{8,9},{9,10},{10,1... | collective-permute-start | bytes 1572872 | tf_op jit(solution)/shard_map/ppermute | solution.py:325
  31.4 55.2 %collective-permute-start.1 = (bf16[512,512]{1,0:T(8,128)(2,1)S(1)}, bf16[512,512]{1,0:T(8,128)(2,1)}, u32[]{:S(2)}, u32[]{:S(2)}) collective-permute-start(bf16[512,512]{1,0:T(8,128)(2,1)S(1)} %bitcast.80), channel_id=1, source_target_pairs={{0,2},{1,3},{2,0},{3,1},{4,6},{5,7},{6,4},{7,5},{8,10},{9,11},{10,... | collective-permute-start | bytes 1572872 | tf_op jit(solution)/shard_map/ppermute | solution.py:325
  33.8 52.7 %collective-permute-start.2 = (bf16[512,512]{1,0:T(8,128)(2,1)S(1)}, bf16[512,512]{1,0:T(8,128)(2,1)}, u32[]{:S(2)}, u32[]{:S(2)}) collective-permute-start(bf16[512,512]{1,0:T(8,128)(2,1)S(1)} %bitcast.81), channel_id=1, source_target_pairs={{0,3},{1,0},{2,1},{3,2},{4,7},{5,4},{6,5},{7,6},{8,11},{9,8},{10,9... | collective-permute-start | bytes 1572872 | tf_op jit(solution)/shard_map/ppermute | solution.py:325
  83.7 27.1 %collective-permute-start.9 = (bf16[2,768,256]{2,1,0:T(8,128)(2,1)}, bf16[2,768,256]{2,1,0:T(8,128)(2,1)S(1)}, u32[]{:S(2)}, u32[]{:S(2)}) collective-permute-start(bf16[2,768,256]{2,1,0:T(8,128)(2,1)} %get-tuple-element.89), channel_id=1, source_target_pairs={{0,3},{1,2},{2,1},{3,0},{4,7},{5,6},{6,5},{7,4},{8,11},{9,10},{10,... | collective-permute-start | bytes 2359304 | tf_op jit(solution)/shard_map/ppermute | solution.py:283
  98.5 11.0 %collective-permute-start.3 = (bf16[2,512,256]{2,1,0:T(8,128)(2,1)}, bf16[2,512,256]{2,1,0:T(8,128)(2,1)S(1)}, u32[]{:S(2)}, u32[]{:S(2)}) collective-permute-start(bf16[2,512,256]{2,1,0:T(8,128)(2,1)} %get-tuple-element.83), channel_id=1, source_target_pairs={{0,1},{1,0},{2,3},{3,2},{4,5},{5,4},{6,7},{7,6},{8,9},{9,8},{10,11... | collective-permute-start | bytes 1572872 | tf_op jit(solution)/shard_map/ppermute | solution.py:283
  98.6 27.8 %collective-permute-start.7 = (bf16[2,768,256]{2,1,0:T(8,128)(2,1)S(1)}, bf16[2,768,256]{2,1,0:T(8,128)(2,1)S(1)}, u32[]{:S(2)}, u32[]{:S(2)}) collective-permute-start(bf16[2,768,256]{2,1,0:T(8,128)(2,1)S(1)} %copy-done.32), channel_id=1, source_target_pairs={{0,1},{1,0},{2,3},{3,2},{4,5},{5,4},{6,7},{7,6},{8,9},{9,8},{10,11... | collective-permute-start | bytes 2359304 | tf_op jit(solution)/shard_map/ppermute | solution.py:283
  100.1 26.7 %collective-permute-start.5 = (bf16[2,512,256]{2,1,0:T(8,128)(2,1)}, bf16[2,512,256]{2,1,0:T(8,128)(2,1)S(1)}, u32[]{:S(2)}, u32[]{:S(2)}) collective-permute-start(bf16[2,512,256]{2,1,0:T(8,128)(2,1)} %get-tuple-element.85), channel_id=1, source_target_pairs={{0,3},{1,2},{2,1},{3,0},{4,7},{5,6},{6,5},{7,4},{8,11},{9,10},{10,... | collective-permute-start | bytes 1572872 | tf_op jit(solution)/shard_map/ppermute | solution.py:283
  110.5 16.4 %collective-permute-start.4 = (bf16[512,256]{1,0:T(8,128)(2,1)S(1)}, bf16[512,256]{1,0:T(8,128)(2,1)S(1)}, u32[]{:S(2)}, u32[]{:S(2)}) collective-permute-start(bf16[512,256]{1,0:T(8,128)(2,1)S(1)} %fusion.3), channel_id=1, source_target_pairs={{0,3},{1,2},{2,1},{3,0},{4,7},{5,6},{6,5},{7,4},{8,11},{9,10},{10,... | collective-permute-start | bytes 786440 | tf_op jit(solution)/shard_map/ppermute | solution.py:283
  110.9 29.7 %collective-permute-start.10 = (bf16[768,256]{1,0:T(8,128)(2,1)S(1)}, bf16[768,256]{1,0:T(8,128)(2,1)S(1)}, u32[]{:S(2)}, u32[]{:S(2)}) collective-permute-start(bf16[768,256]{1,0:T(8,128)(2,1)S(1)} %fusion.2), channel_id=1, source_target_pairs={{0,1},{1,0},{2,3},{3,2},{4,5},{5,4},{6,7},{7,6},{8,9},{9,8},{10,11... | collective-permute-start | bytes 1179656 | tf_op jit(solution)/shard_map/ppermute | solution.py:283
  126.5 14.2 %collective-permute-start.8 = (bf16[768,256]{1,0:T(8,128)(2,1)S(1)}, bf16[768,256]{1,0:T(8,128)(2,1)S(1)}, u32[]{:S(2)}, u32[]{:S(2)}) collective-permute-start(bf16[768,256]{1,0:T(8,128)(2,1)S(1)} %fusion.1), channel_id=1, source_target_pairs={{0,3},{1,2},{2,1},{3,0},{4,7},{5,6},{6,5},{7,4},{8,11},{9,10},{10,... | collective-permute-start | bytes 1179656 | tf_op jit(solution)/shard_map/ppermute | solution.py:283
  126.8 13.6 %collective-permute-start.6 = (bf16[512,256]{1,0:T(8,128)(2,1)S(1)}, bf16[512,256]{1,0:T(8,128)(2,1)S(1)}, u32[]{:S(2)}, u32[]{:S(2)}) collective-permute-start(bf16[512,256]{1,0:T(8,128)(2,1)S(1)} %fusion.4), channel_id=1, source_target_pairs={{0,1},{1,0},{2,3},{3,2},{4,5},{5,4},{6,7},{7,6},{8,9},{9,8},{10,11... | collective-permute-start | bytes 786440 | tf_op jit(solution)/shard_map/ppermute | solution.py:283
  142.1 27.3 %all-to-all-start.2 = ((bf16[32,40,512]{2,1,0:T(8,128)(2,1)}), bf16[32,40,512]{2,1,0:T(8,128)(2,1)}, u32[]{:S(2)}, u32[]{:S(2)}) async-start(bf16[32,40,512]{2,1,0:T(8,128)(2,1)} %pad_maximum_fusion), calls=%async_computation.2 | async-start | bytes 2621440 | tf_op jit(solution)/shard_map/all_to_all | solution.py:685
  172.1 13.2 %collective-permute-start.11 = (bf16[512,512]{1,0:T(8,128)(2,1)S(1)}, bf16[512,512]{1,0:T(8,128)(2,1)S(1)}, u32[]{:S(2)}, u32[]{:S(2)}) collective-permute-start(bf16[512,512]{1,0:T(8,128)(2,1)S(1)} %fusion.a), channel_id=1, source_target_pairs={{0,1},{1,2},{2,3},{3,0},{4,5},{5,6},{6,7},{7,4},{8,9},{9,10},{10,1... | collective-permute-start | bytes 1572872 | tf_op jit(solution)/shard_map/ppermute | solution.py:325
  172.2 13.9 %collective-permute-start.12 = (bf16[512,512]{1,0:T(8,128)(2,1)S(1)}, bf16[512,512]{1,0:T(8,128)(2,1)S(1)}, u32[]{:S(2)}, u32[]{:S(2)}) collective-permute-start(bf16[512,512]{1,0:T(8,128)(2,1)S(1)} %fusion.a), channel_id=1, source_target_pairs={{0,3},{1,0},{2,1},{3,2},{4,7},{5,4},{6,5},{7,6},{8,11},{9,8},{10,9... | collective-permute-start | bytes 1572872 | tf_op jit(solution)/shard_map/ppermute | solution.py:325
  177.0 3.1 %collective-permute-start.15 = (f32[264,128]{1,0:T(8,128)S(1)}, f32[264,128]{1,0:T(8,128)S(1)}, u32[]{:S(2)}, u32[]{:S(2)}) collective-permute-start(f32[264,128]{1,0:T(8,128)S(1)} %get-tuple-element.93.refs_0_), channel_id=1, source_target_pairs={{0,4},{4,0},{1,5},{5,1},{2,6},{6,2},{3,7},{7,3},{8,12},{12,8},{9,1... | collective-permute-start | bytes 405512 | tf_op jit(solution)/shard_map/ppermute | solution.py:325
  180.8 8.9 %collective-permute-start.16 = (f32[264,128]{1,0:T(8,128)S(1)}, f32[264,128]{1,0:T(8,128)S(1)}, u32[]{:S(2)}, u32[]{:S(2)}) collective-permute-start(f32[264,128]{1,0:T(8,128)S(1)} %get-tuple-element.94.refs_0_), channel_id=1, source_target_pairs={{0,8},{8,16},{16,24},{24,0},{1,9},{9,17},{17,25},{25,1},{2,10},{10... | collective-permute-start | bytes 405512 | tf_op jit(solution)/shard_map/ppermute | solution.py:325
  180.8 8.9 %collective-permute-start.17 = (f32[264,128]{1,0:T(8,128)S(1)}, f32[264,128]{1,0:T(8,128)S(1)}, u32[]{:S(2)}, u32[]{:S(2)}) collective-permute-start(f32[264,128]{1,0:T(8,128)S(1)} %get-tuple-element.94.refs_0_), channel_id=1, source_target_pairs={{0,16},{8,24},{16,0},{24,8},{1,17},{9,25},{17,1},{25,9},{2,18},{10... | collective-permute-start | bytes 405512 | tf_op jit(solution)/shard_map/ppermute | solution.py:325
  182.3 7.7 %collective-permute-start.18 = (f32[264,128]{1,0:T(8,128)S(1)}, f32[264,128]{1,0:T(8,128)S(1)}, u32[]{:S(2)}, u32[]{:S(2)}) collective-permute-start(f32[264,128]{1,0:T(8,128)S(1)} %get-tuple-element.94.refs_0_), channel_id=1, source_target_pairs={{0,24},{8,0},{16,8},{24,16},{1,25},{9,1},{17,9},{25,17},{2,26},{10... | collective-permute-start | bytes 405512 | tf_op jit(solution)/shard_map/ppermute | solution.py:325
  186.1 19.2 %collective-permute-start.13 = (bf16[256,512]{1,0:T(8,128)(2,1)}, bf16[256,512]{1,0:T(8,128)(2,1)}, u32[]{:S(2)}, u32[]{:S(2)}) collective-permute-start(bf16[256,512]{1,0:T(8,128)(2,1)} %slice.44), channel_id=1, source_target_pairs={{0,1},{1,2},{2,3},{3,0},{4,5},{5,6},{6,7},{7,4},{8,9},{9,10},{10,1... | collective-permute-start | bytes 786440 | tf_op jit(solution)/shard_map/ppermute | solution.py:325
  186.8 19.4 %collective-permute-start.14 = (bf16[256,512]{1,0:T(8,128)(2,1)}, bf16[256,512]{1,0:T(8,128)(2,1)}, u32[]{:S(2)}, u32[]{:S(2)}) collective-permute-start(bf16[256,512]{1,0:T(8,128)(2,1)} %slice.45), channel_id=1, source_target_pairs={{0,3},{1,0},{2,1},{3,2},{4,7},{5,4},{6,5},{7,6},{8,11},{9,8},{10,9... | collective-permute-start | bytes 786440 | tf_op jit(solution)/shard_map/ppermute | solution.py:325
  190.8 5.4 %collective-permute-start.19 = (f32[264,128]{1,0:T(8,128)S(1)}, f32[264,128]{1,0:T(8,128)S(1)}, u32[]{:S(2)}, u32[]{:S(2)}) collective-permute-start(f32[264,128]{1,0:T(8,128)S(1)} %get-tuple-element.95.refs_0_), channel_id=1, source_target_pairs={{0,32},{32,64},{64,96},{96,0},{1,33},{33,65},{65,97},{97,1},{2,34}... | collective-permute-start | bytes 405512 | tf_op jit(solution)/shard_map/ppermute | solution.py:325
  192.9 7.1 %collective-permute-start.20 = (f32[264,128]{1,0:T(8,128)S(1)}, f32[264,128]{1,0:T(8,128)S(1)}, u32[]{:S(2)}, u32[]{:S(2)}) collective-permute-start(f32[264,128]{1,0:T(8,128)S(1)} %get-tuple-element.95.refs_0_), channel_id=1, source_target_pairs={{0,64},{32,96},{64,0},{96,32},{1,65},{33,97},{65,1},{97,33},{2,66}... | collective-permute-start | bytes 405512 | tf_op jit(solution)/shard_map/ppermute | solution.py:325
  194.1 5.9 %collective-permute-start.21 = (f32[264,128]{1,0:T(8,128)S(1)}, f32[264,128]{1,0:T(8,128)S(1)}, u32[]{:S(2)}, u32[]{:S(2)}) collective-permute-start(f32[264,128]{1,0:T(8,128)S(1)} %get-tuple-element.95.refs_0_), channel_id=1, source_target_pairs={{0,96},{32,0},{64,32},{96,64},{1,97},{33,1},{65,33},{97,65},{2,98}... | collective-permute-start | bytes 405512 | tf_op jit(solution)/shard_map/ppermute | solution.py:325
  209.0 55.2 %all-to-all-start.3 = ((bf16[32,64,256]{2,1,0:T(8,128)(2,1)}), bf16[32,64,256]{2,1,0:T(8,128)(2,1)}, u32[]{:S(2)}, u32[]{:S(2)}) async-start(bf16[32,64,256]{2,1,0:T(8,128)(2,1)} %bitcast.34), calls=%async_computation.3 | async-start | bytes 2097152 | tf_op jit(solution)/shard_map/all_to_all | solution.py:754
  221.7 11.6 %collective-permute-start.23 = (bf16[256,128]{1,0:T(8,128)(2,1)S(1)}, bf16[256,128]{1,0:T(8,128)(2,1)S(1)}, u32[]{:S(2)}, u32[]{:S(2)}) collective-permute-start(bf16[256,128]{1,0:T(8,128)(2,1)S(1)} %get-tuple-element.109.refs_0_), channel_id=1, source_target_pairs={{0,8},{8,16},{16,24},{24,0},{1,9},{9,17},{17,25},{25,1},{2,10},{10... | collective-permute-start | bytes 196616 | tf_op jit(solution)/shard_map/ppermute | solution.py:325
  223.1 11.6 %collective-permute-start.24 = (bf16[256,128]{1,0:T(8,128)(2,1)S(1)}, bf16[256,128]{1,0:T(8,128)(2,1)S(1)}, u32[]{:S(2)}, u32[]{:S(2)}) collective-permute-start(bf16[256,128]{1,0:T(8,128)(2,1)S(1)} %get-tuple-element.109.refs_0_), channel_id=1, source_target_pairs={{0,16},{8,24},{16,0},{24,8},{1,17},{9,25},{17,1},{25,9},{2,18},{10... | collective-permute-start | bytes 196616 | tf_op jit(solution)/shard_map/ppermute | solution.py:325
  225.5 9.2 %collective-permute-start.25 = (bf16[256,128]{1,0:T(8,128)(2,1)S(1)}, bf16[256,128]{1,0:T(8,128)(2,1)S(1)}, u32[]{:S(2)}, u32[]{:S(2)}) collective-permute-start(bf16[256,128]{1,0:T(8,128)(2,1)S(1)} %get-tuple-element.109.refs_0_), channel_id=1, source_target_pairs={{0,24},{8,0},{16,8},{24,16},{1,25},{9,1},{17,9},{25,17},{2,26},{10... | collective-permute-start | bytes 196616 | tf_op jit(solution)/shard_map/ppermute | solution.py:325
  234.8 26.4 %collective-permute-start.26 = (bf16[256,128]{1,0:T(8,128)(2,1)S(1)}, bf16[256,128]{1,0:T(8,128)(2,1)S(1)}, u32[]{:S(2)}, u32[]{:S(2)}) collective-permute-start(bf16[256,128]{1,0:T(8,128)(2,1)S(1)} %get-tuple-element.110.refs_0_), channel_id=1, source_target_pairs={{0,32},{32,64},{64,96},{96,0},{1,33},{33,65},{65,97},{97,1},{2,34}... | collective-permute-start | bytes 196616 | tf_op jit(solution)/shard_map/ppermute | solution.py:325
  236.0 25.3 %collective-permute-start.27 = (bf16[256,128]{1,0:T(8,128)(2,1)S(1)}, bf16[256,128]{1,0:T(8,128)(2,1)S(1)}, u32[]{:S(2)}, u32[]{:S(2)}) collective-permute-start(bf16[256,128]{1,0:T(8,128)(2,1)S(1)} %get-tuple-element.110.refs_0_), channel_id=1, source_target_pairs={{0,64},{32,96},{64,0},{96,32},{1,65},{33,97},{65,1},{97,33},{2,66}... | collective-permute-start | bytes 196616 | tf_op jit(solution)/shard_map/ppermute | solution.py:325
  238.5 22.8 %collective-permute-start.28 = (bf16[256,128]{1,0:T(8,128)(2,1)S(1)}, bf16[256,128]{1,0:T(8,128)(2,1)S(1)}, u32[]{:S(2)}, u32[]{:S(2)}) collective-permute-start(bf16[256,128]{1,0:T(8,128)(2,1)S(1)} %get-tuple-element.110.refs_0_), channel_id=1, source_target_pairs={{0,96},{32,0},{64,32},{96,64},{1,97},{33,1},{65,33},{97,65},{2,98}... | collective-permute-start | bytes 196616 | tf_op jit(solution)/shard_map/ppermute | solution.py:325
  (34 other events, 339.9 us)

commit v6 on v5

--- a/solution.py
+++ b/solution.py
@@ -179,19 +179,7 @@
 
 def expert_body(place, *refs, tiles):
     routed, (active, slope, down_w, gate_w, up_w) = refs[:tiles], refs[tiles : tiles + 5]
-    *routed_out, d_gate, d_up, keep_a, send_a, keep_b, send_b = refs[tiles + 5 : -4]
-    down_v, gate_v, up_v, loaded = refs[-4:]
-    copies = [
-        pltpu.make_async_copy(source, target, loaded.at[i])
-        for i, (source, target) in enumerate(((down_w, down_v), (gate_w, gate_v), (up_w, up_v)))
-    ]
-
-    @pl.when(pl.program_id(0) == 0)
-    def _():
-        for copy in copies:
-            copy.start()
-        copies[0].wait()
-
+    *routed_out, d_gate, d_up, keep_a, send_a, keep_b, send_b = refs[tiles + 5 :]
     d_hidden = 0.0
     for k, tile in enumerate(routed):
         wide = tile.shape[1]
@@ -199,12 +187,7 @@
         if tiles > 1:
             cols = pl.ds(pl.multiple_of(((place[0] + tiles - k) & (tiles - 1)) * wide, wide), wide)
             routed_out[0][:, cols] = tile[...]
-        d_hidden = d_hidden + dot(tile[...], down_v[:, cols], NT)
-
-    @pl.when(pl.program_id(0) == 0)
-    def _():
-        copies[1].wait()
-        copies[2].wait()
+        d_hidden = d_hidden + dot(tile[...], down_w[:, cols], NT)
 
     to_gate = (d_hidden * slope[...].astype(F32)).astype(BF16)
     to_up = (d_hidden * active[...].astype(F32)).astype(BF16)
@@ -220,7 +203,7 @@
     for k, (home_a, home_b) in enumerate(homes):
         start = pl.multiple_of((place[0] ^ k) * (2 * half), 2 * half)
         cols = pl.ds(start, 2 * half)
-        term = dot(to_gate, gate_v[:, cols], NN) + dot(to_up, up_v[:, cols], NN)
+        term = dot(to_gate, gate_w[:, cols], NN) + dot(to_up, up_w[:, cols], NN)
         term = term.astype(BF16)
         home_a[0][home_a[1]] = term[:, :half]
         home_b[0][home_b[1]] = term[:, half:]
@@ -242,15 +225,13 @@
             grid=(rows // step,),
             in_specs=[pl.BlockSpec((step, wide), by_row)] * tiles
             + [pl.BlockSpec((step, units), by_row)] * 2
-            + [pl.BlockSpec(memory_space=pl.ANY)] * 3,
+            + [VMEM] * 3,
             out_specs=[pl.BlockSpec((step, w), by_row) for w in rebuilt + [units] * 2]
             + [pair] * 4,
-            scratch_shapes=[pltpu.VMEM((units, width), BF16)] * 3
-            + [pltpu.SemaphoreType.DMA((3,))],
         ),
         out_shape=[jax.ShapeDtypeStruct((rows, w), BF16) for w in rebuilt + [units] * 2]
         + [jax.ShapeDtypeStruct((2, rows, half), BF16)] * 4,
-        compiler_params=limit(56),
+        compiler_params=limit(53),
     )(place, *routed, active, slope, down_w, gate_w, up_w)
 
 

time: 267 us -> 266 us (level)
    unnamed x67 -> x61, local copies, waits for them, and re-layouts: 12.8 us -> 12.1 us
where the time goes in v6:
time: 266 us; the launch traced here: 265 us
  waiting for transfers between devices  99 us (37%)
  Pallas kernels  78.4 us (29%)
  starting transfers between devices  65.9 us (25%)
  local copies, waits for them, and re-layouts  14.5 us (5%)
  other arithmetic  3.51 us (1%)
    all_to_all x3, waiting for transfers between devices, exchanged(): box = lax.all_to_all(box, SP, split_axis=0, concat_axis=0, tiled=True)  43.6 us
    ppermute x8, waiting for transfers between devices, swapped(): return lax.ppermute(x, TP, [(i, i ^ flip) for i in range(count)])  39.1 us
    ppermute x21, starting transfers between devices, shifted(): return lax.ppermute(x, axis, [(i, (i + by) % count) for i in range(count)])  30.6 us
    pallas_call x2, Pallas kernels, expert_cotangents(): pl.pallas_call(functools.partial(expert_body, tiles=tiles), grid_spec=plt...  24.7 us
    all_to_all x3, starting transfers between devices, exchanged(): box = lax.all_to_all(box, SP, split_axis=0, concat_axis=0, tiled=True)  22.3 us
    pallas_call x2, Pallas kernels, weight_grads(): pl.pallas_call(weight_grads_body, grid=(width // step,), in_specs=[pl.Blo...  19.6 us
    ppermute x21, waiting for transfers between devices, shifted(): return lax.ppermute(x, axis, [(i, (i + by) % count) for i in range(count)])  16.3 us
    pallas_call x1, Pallas kernels, expert_forward(): pl.pallas_call(functools.partial(expert_forward_body, orders=(group, capa...  16.3 us
  transfers between devices with their start and end apart: 33, of which 15 were waited for; matrix products, arithmetic and copies ran while one was open for 1% of the time, Pallas kernels for 27%

profile of v6, /device:TPU:1, one launch (start us, length us, event | category | flops | bytes accessed | tf_op | source)
XLA Modules:
  0.0 265.0 jit_solution(13144164106385453105)
XLA Ops:
  0.7 3.5 %shard_map.179 = (bf16[512,512]{1,0:T(8,128)(2,1)}, s32[2,512]{1,0:T(2,128)}) custom-call(s32[1]{0:T(128)} %bitcast.place, bf16[512,2048]{1,0:T(8,128)(2,1)} %d_out.3, s32[2,512]{1,0:T(2,128)} %bitcast.65, f32[2,512]{1,0:T(2,128)} %bitcast.67), custom_call_target="tpu_custom_call" | custom-call | tf_op jit(solution)/shard_map/pallas_call | solution.py:669
  4.2 9.6 %all-to-all-start = ((bf16[32,16,512]{2,1,0:T(8,128)(2,1)}), bf16[32,16,512]{2,1,0:T(8,128)(2,1)S(1)}, u32[]{:S(2)}, u32[]{:S(2)}) async-start(bf16[32,16,512]{2,1,0:T(8,128)(2,1)} %bitcast.83), calls=%async_computation | async-start | bytes 1048576 | tf_op jit(solution)/shard_map/all_to_all | solution.py:666
  14.5 2.5 shard_map.182
  19.8 5.4 %all-to-all-done = bf16[32,16,512]{2,1,0:T(8,128)(2,1)S(1)} async-done(((bf16[32,16,512]{2,1,0:T(8,128)(2,1)}), bf16[32,16,512]{2,1,0:T(8,128)(2,1)S(1)}, u32[]{:S(2)}, u32[]{:S(2)}) %all-to-all-start) | async-done | bytes 524320 | tf_op jit(solution)/shard_map/all_to_all | solution.py:666
  25.3 4.8 %all-to-all-start.1 = ((bf16[32,24,2048]{2,1,0:T(8,128)(2,1)}), bf16[32,24,2048]{2,1,0:T(8,128)(2,1)}, u32[]{:S(2)}, u32[]{:S(2)}) async-start(bf16[32,24,2048]{2,1,0:T(8,128)(2,1)} %bitcast.53), calls=%async_computation.1 | async-start | bytes 6291456 | tf_op jit(solution)/shard_map/all_to_all | solution.py:666
  31.4 2.5 collective-permute-start.1
  35.0 16.3 %shard_map.180 = (bf16[512,2048]{1,0:T(8,128)(2,1)}, bf16[768,2048]{1,0:T(8,128)(2,1)}, bf16[512,704]{1,0:T(8,128)(2,1)}, bf16[768,704]{1,0:T(8,128)(2,1)}, bf16...) custom-call(bf16[1152,2048]{1,0:T(8,128)(2,1)} %bitcast.77, ...), custom_call_target="tpu_custom_call" | custom-call | tf_op jit(solution)/shard_map/pallas_call | solution.py:167
  51.3 18.7 %all-to-all-done.1 = bf16[32,24,2048]{2,1,0:T(8,128)(2,1)} async-done(((bf16[32,24,2048]{2,1,0:T(8,128)(2,1)}), bf16[32,24,2048]{2,1,0:T(8,128)(2,1)}, u32[]{:S(2)}, u32[]{:S(2)}) %all-to-all-start.1) | async-done | bytes 3145760 | tf_op jit(solution)/shard_map/all_to_all | solution.py:666
  70.0 13.4 %shard_map.183 = (bf16[768,704]{1,0:T(8,128)(2,1)}, bf16[768,704]{1,0:T(8,128)(2,1)}, bf16[2,768,256]{2,1,0:T(8,128)(2,1)S(1)}, bf16[2,768,256]{2,1,0:T(8,128)(2...) custom-call(s32[1]{0:T(128)} %bitcast.place, bf16[768,2048]{1,0:T(8,128)(2,1)} %bitcast.12.refs_0_.refs_3_, ...), custom_call_target="tpu_custom_call" | custom-call | tf_op jit(solution)/shard_map/pallas_call | solution.py:221
  83.4 2.5 collective-permute-start.9
  86.0 11.3 %shard_map.181 = (bf16[512,2048]{1,0:T(8,128)(2,1)}, bf16[512,704]{1,0:T(8,128)(2,1)}, bf16[512,704]{1,0:T(8,128)(2,1)}, bf16[2,512,256]{2,1,0:T(8,128)(2,1)S(1)...) custom-call(s32[1]{0:T(128)} %bitcast.place, ...), custom_call_target="tpu_custom_call" | custom-call | tf_op jit(solution)/shard_map/pallas_call | solution.py:221
  99.0 9.3 %collective-permute-done.3.got_a = bf16[2,512,256]{2,1,0:T(8,128)(2,1)S(1)} collective-permute-done((bf16[2,512,256]{2,1,0:T(8,128)(2,1)}, bf16[2,512,256]{2,1,0:T(8,128)(2,1)S(1)}, u32[]{:S(2)}, u32[]{:S(2)}) %collective-permute-start.3) | collective-permute-done | bytes 524320 | tf_op jit(solution)/shard_map/ppermute | solution.py:264
  108.9 16.3 %collective-permute-done.7.got_a = bf16[2,768,256]{2,1,0:T(8,128)(2,1)S(1)} collective-permute-done((bf16[2,768,256]{2,1,0:T(8,128)(2,1)S(1)}, bf16[2,768,256]{2,1,0:T(8,128)(2,1)S(1)}, u32[]{:S(2)}, u32[]{:S(2)}) %collective-permute-start.7) | collective-permute-done | bytes 786464 | tf_op jit(solution)/shard_map/ppermute | solution.py:264
  125.7 13.5 %collective-permute-done.6.last_b = bf16[512,256]{1,0:T(8,128)(2,1)S(1)} collective-permute-done((bf16[512,256]{1,0:T(8,128)(2,1)S(1)}, bf16[512,256]{1,0:T(8,128)(2,1)S(1)}, u32[]{:S(2)}, u32[]{:S(2)}) %collective-permute-start.6) | collective-permute-done | bytes 262176 | tf_op jit(solution)/shard_map/ppermute | solution.py:264
  140.9 7.9 %all-to-all-start.2 = ((bf16[32,40,512]{2,1,0:T(8,128)(2,1)}), bf16[32,40,512]{2,1,0:T(8,128)(2,1)}, u32[]{:S(2)}, u32[]{:S(2)}) async-start(bf16[32,40,512]{2,1,0:T(8,128)(2,1)} %pad_maximum_fusion), calls=%async_computation.2 | async-start | bytes 2621440 | tf_op jit(solution)/shard_map/all_to_all | solution.py:666
  148.8 19.4 %all-to-all-done.2 = bf16[32,40,512]{2,1,0:T(8,128)(2,1)} async-done(((bf16[32,40,512]{2,1,0:T(8,128)(2,1)}), bf16[32,40,512]{2,1,0:T(8,128)(2,1)}, u32[]{:S(2)}, u32[]{:S(2)}) %all-to-all-start.2) | async-done | bytes 1310752 | tf_op jit(solution)/shard_map/all_to_all | solution.py:666
  168.2 2.6 fusion.a
  171.0 2.7 %collective-permute-start.12 = (bf16[512,512]{1,0:T(8,128)(2,1)S(1)}, bf16[512,512]{1,0:T(8,128)(2,1)S(1)}, u32[]{:S(2)}, u32[]{:S(2)}) collective-permute-start(bf16[512,512]{1,0:T(8,128)(2,1)S(1)} %fusion.a), channel_id=1, source_target_pairs={{0,3},{1,0},{2,1},{3,2},{4,7},{5,4},{6,5},{7,6},{8,11},{9,8},{10,9... | collective-permute-start | bytes 1572872 | tf_op jit(solution)/shard_map/ppermute | solution.py:306
  175.7 2.1 collective-permute-start.15
  185.6 2.7 %collective-permute-start.14 = (bf16[256,512]{1,0:T(8,128)(2,1)}, bf16[256,512]{1,0:T(8,128)(2,1)}, u32[]{:S(2)}, u32[]{:S(2)}) collective-permute-start(bf16[256,512]{1,0:T(8,128)(2,1)} %slice.45), channel_id=1, source_target_pairs={{0,3},{1,0},{2,1},{3,2},{4,7},{5,4},{6,5},{7,6},{8,11},{9,8},{10,9... | collective-permute-start | bytes 786440 | tf_op jit(solution)/shard_map/ppermute | solution.py:306
  189.6 2.1 collective-permute-start.19
  192.9 2.1 collective-permute-start.21
  195.0 3.8 %collective-permute-done.20.refs_2_ = f32[264,128]{1,0:T(8,128)S(1)} collective-permute-done((f32[264,128]{1,0:T(8,128)S(1)}, f32[264,128]{1,0:T(8,128)S(1)}, u32[]{:S(2)}, u32[]{:S(2)}) %collective-permute-start.20) | collective-permute-done | bytes 135200 | tf_op jit(solution)/shard_map/ppermute | solution.py:306
  207.8 8.0 %all-to-all-start.3 = ((bf16[32,64,256]{2,1,0:T(8,128)(2,1)}), bf16[32,64,256]{2,1,0:T(8,128)(2,1)}, u32[]{:S(2)}, u32[]{:S(2)}) async-start(bf16[32,64,256]{2,1,0:T(8,128)(2,1)} %bitcast.34), calls=%async_computation.3 | async-start | bytes 2097152 | tf_op jit(solution)/shard_map/all_to_all | solution.py:735
  217.1 2.0 shard_map.193
  221.9 2.4 collective-permute-start.24
  225.5 6.5 %collective-permute-done.23.refs_1_ = bf16[256,128]{1,0:T(8,128)(2,1)S(1)} collective-permute-done((bf16[256,128]{1,0:T(8,128)(2,1)S(1)}, bf16[256,128]{1,0:T(8,128)(2,1)S(1)}, u32[]{:S(2)}, u32[]{:S(2)}) %collective-permute-start.23) | collective-permute-done | bytes 65568 | tf_op jit(solution)/shard_map/ppermute | solution.py:306
  234.8 2.5 collective-permute-start.27
  238.4 7.8 %shard_map.185 = bf16[704,2048]{1,0:T(8,128)(2,1)} custom-call(bf16[512,704]{1,0:T(8,128)(2,1)} %get-tuple-element.78.refs_0_, bf16[768,704]{1,0:T(8,128)(2,1)} %get-tuple-element.79.refs_1_, bf16[512,2048]{1,0:T(8,128)(2,1)} %get-tuple-element.80.refs_2_, bf16[768,2048]{1,0:T(8,128)(2,1)} %bitcast.12.refs_0_.refs_3_), custom_call_target="tpu_custom_call" | custom-call | tf_op jit(solution)/shard_map/pallas_call | solution.py:251
  246.3 11.8 %shard_map.184 = (bf16[704,2048]{1,0:T(8,128)(2,1)}, bf16[704,2048]{1,0:T(8,128)(2,1)}) custom-call(bf16[512,704]{1,0:T(8,128)(2,1)} %get-tuple-element.66.refs_0_, bf16[768,704]{1,0:T(8,128)(2,1)} %get-tuple-element.71.refs_1_, bf16[512,704]{1,0:T(8,128)(2,1)} %get-tuple-element.72.refs_2_, bf16[768,704]{1,0:T(8,128)(2,1)} %get-tuple-element.73.refs_3_, ...), custom_call_target="tpu_custom_call" | custom-call | tf_op jit(solution)/shard_map/pallas_call | solution.py:251
  258.1 2.0 shard_map.194
  260.2 2.9 %shard_map.197 = (bf16[512,128]{1,0:T(8,128)(2,1)}, bf16[512,128]{1,0:T(8,128)(2,1)}, bf16[512,256]{1,0:T(8,128)(2,1)}, f32[512,128]{1,0:T(8,128)}) custom-call(bf16[512,128]{1,0:T(8,128)(2,1)S(1)} %bitcast.58, bf16[512,128]{1,0:T(8,128)(2,1)S(1)} %bitcast.62, bf16[512,256]{1,0:T(8,128)(2,1)S(1)} %bitcast.52, f32[512,128]{1,0:T(8,128)S(1)} %get-tuple-element.90.cumulative, ...), custom_call_target="tpu_custom_call" | custom-call | tf_op jit(solution)/shard_map/pallas_call | solution.py:523
  (124 shorter events, 42.9 us)
Async XLA Ops:
  4.2 21.0 %all-to-all-start = ((bf16[32,16,512]{2,1,0:T(8,128)(2,1)}), bf16[32,16,512]{2,1,0:T(8,128)(2,1)S(1)}, u32[]{:S(2)}, u32[]{:S(2)}) async-start(bf16[32,16,512]{2,1,0:T(8,128)(2,1)} %bitcast.83), calls=%async_computation | async-start | bytes 1048576 | tf_op jit(solution)/shard_map/all_to_all | solution.py:666
  25.3 44.7 %all-to-all-start.1 = ((bf16[32,24,2048]{2,1,0:T(8,128)(2,1)}), bf16[32,24,2048]{2,1,0:T(8,128)(2,1)}, u32[]{:S(2)}, u32[]{:S(2)}) async-start(bf16[32,24,2048]{2,1,0:T(8,128)(2,1)} %bitcast.53), calls=%async_computation.1 | async-start | bytes 6291456 | tf_op jit(solution)/shard_map/all_to_all | solution.py:666
  30.1 55.9 %collective-permute-start = (bf16[512,512]{1,0:T(8,128)(2,1)S(1)}, bf16[512,512]{1,0:T(8,128)(2,1)}, u32[]{:S(2)}, u32[]{:S(2)}) collective-permute-start(bf16[512,512]{1,0:T(8,128)(2,1)S(1)} %bitcast.79), channel_id=1, source_target_pairs={{0,1},{1,2},{2,3},{3,0},{4,5},{5,6},{6,7},{7,4},{8,9},{9,10},{10,1... | collective-permute-start | bytes 1572872 | tf_op jit(solution)/shard_map/ppermute | solution.py:306
  31.4 54.6 %collective-permute-start.1 = (bf16[512,512]{1,0:T(8,128)(2,1)S(1)}, bf16[512,512]{1,0:T(8,128)(2,1)}, u32[]{:S(2)}, u32[]{:S(2)}) collective-permute-start(bf16[512,512]{1,0:T(8,128)(2,1)S(1)} %bitcast.80), channel_id=1, source_target_pairs={{0,2},{1,3},{2,0},{3,1},{4,6},{5,7},{6,4},{7,5},{8,10},{9,11},{10,... | collective-permute-start | bytes 1572872 | tf_op jit(solution)/shard_map/ppermute | solution.py:306
  33.8 52.1 %collective-permute-start.2 = (bf16[512,512]{1,0:T(8,128)(2,1)S(1)}, bf16[512,512]{1,0:T(8,128)(2,1)}, u32[]{:S(2)}, u32[]{:S(2)}) collective-permute-start(bf16[512,512]{1,0:T(8,128)(2,1)S(1)} %bitcast.81), channel_id=1, source_target_pairs={{0,3},{1,0},{2,1},{3,2},{4,7},{5,4},{6,5},{7,6},{8,11},{9,8},{10,9... | collective-permute-start | bytes 1572872 | tf_op jit(solution)/shard_map/ppermute | solution.py:306
  83.4 25.3 %collective-permute-start.9 = (bf16[2,768,256]{2,1,0:T(8,128)(2,1)}, bf16[2,768,256]{2,1,0:T(8,128)(2,1)S(1)}, u32[]{:S(2)}, u32[]{:S(2)}) collective-permute-start(bf16[2,768,256]{2,1,0:T(8,128)(2,1)} %get-tuple-element.89), channel_id=1, source_target_pairs={{0,3},{1,2},{2,1},{3,0},{4,7},{5,6},{6,5},{7,4},{8,11},{9,10},{10,... | collective-permute-start | bytes 2359304 | tf_op jit(solution)/shard_map/ppermute | solution.py:264
  97.3 11.0 %collective-permute-start.3 = (bf16[2,512,256]{2,1,0:T(8,128)(2,1)}, bf16[2,512,256]{2,1,0:T(8,128)(2,1)S(1)}, u32[]{:S(2)}, u32[]{:S(2)}) collective-permute-start(bf16[2,512,256]{2,1,0:T(8,128)(2,1)} %get-tuple-element.83), channel_id=1, source_target_pairs={{0,1},{1,0},{2,3},{3,2},{4,5},{5,4},{6,7},{7,6},{8,9},{9,8},{10,11... | collective-permute-start | bytes 1572872 | tf_op jit(solution)/shard_map/ppermute | solution.py:264
  97.4 27.8 %collective-permute-start.7 = (bf16[2,768,256]{2,1,0:T(8,128)(2,1)S(1)}, bf16[2,768,256]{2,1,0:T(8,128)(2,1)S(1)}, u32[]{:S(2)}, u32[]{:S(2)}) collective-permute-start(bf16[2,768,256]{2,1,0:T(8,128)(2,1)S(1)} %copy-done.29), channel_id=1, source_target_pairs={{0,1},{1,0},{2,3},{3,2},{4,5},{5,4},{6,7},{7,6},{8,9},{9,8},{10,11... | collective-permute-start | bytes 2359304 | tf_op jit(solution)/shard_map/ppermute | solution.py:264
  98.9 26.7 %collective-permute-start.5 = (bf16[2,512,256]{2,1,0:T(8,128)(2,1)}, bf16[2,512,256]{2,1,0:T(8,128)(2,1)S(1)}, u32[]{:S(2)}, u32[]{:S(2)}) collective-permute-start(bf16[2,512,256]{2,1,0:T(8,128)(2,1)} %get-tuple-element.85), channel_id=1, source_target_pairs={{0,3},{1,2},{2,1},{3,0},{4,7},{5,6},{6,5},{7,4},{8,11},{9,10},{10,... | collective-permute-start | bytes 1572872 | tf_op jit(solution)/shard_map/ppermute | solution.py:264
  108.4 17.3 %collective-permute-start.4 = (bf16[512,256]{1,0:T(8,128)(2,1)S(1)}, bf16[512,256]{1,0:T(8,128)(2,1)S(1)}, u32[]{:S(2)}, u32[]{:S(2)}) collective-permute-start(bf16[512,256]{1,0:T(8,128)(2,1)S(1)} %fusion.3), channel_id=1, source_target_pairs={{0,3},{1,2},{2,1},{3,0},{4,7},{5,6},{6,5},{7,4},{8,11},{9,10},{10,... | collective-permute-start | bytes 786440 | tf_op jit(solution)/shard_map/ppermute | solution.py:264
  108.8 30.7 %collective-permute-start.10 = (bf16[768,256]{1,0:T(8,128)(2,1)S(1)}, bf16[768,256]{1,0:T(8,128)(2,1)S(1)}, u32[]{:S(2)}, u32[]{:S(2)}) collective-permute-start(bf16[768,256]{1,0:T(8,128)(2,1)S(1)} %fusion.2), channel_id=1, source_target_pairs={{0,1},{1,0},{2,3},{3,2},{4,5},{5,4},{6,7},{7,6},{8,9},{9,8},{10,11... | collective-permute-start | bytes 1179656 | tf_op jit(solution)/shard_map/ppermute | solution.py:264
  125.3 14.1 %collective-permute-start.8 = (bf16[768,256]{1,0:T(8,128)(2,1)S(1)}, bf16[768,256]{1,0:T(8,128)(2,1)S(1)}, u32[]{:S(2)}, u32[]{:S(2)}) collective-permute-start(bf16[768,256]{1,0:T(8,128)(2,1)S(1)} %fusion.1), channel_id=1, source_target_pairs={{0,3},{1,2},{2,1},{3,0},{4,7},{5,6},{6,5},{7,4},{8,11},{9,10},{10,... | collective-permute-start | bytes 1179656 | tf_op jit(solution)/shard_map/ppermute | solution.py:264
  125.6 13.6 %collective-permute-start.6 = (bf16[512,256]{1,0:T(8,128)(2,1)S(1)}, bf16[512,256]{1,0:T(8,128)(2,1)S(1)}, u32[]{:S(2)}, u32[]{:S(2)}) collective-permute-start(bf16[512,256]{1,0:T(8,128)(2,1)S(1)} %fusion.4), channel_id=1, source_target_pairs={{0,1},{1,0},{2,3},{3,2},{4,5},{5,4},{6,7},{7,6},{8,9},{9,8},{10,11... | collective-permute-start | bytes 786440 | tf_op jit(solution)/shard_map/ppermute | solution.py:264
  140.9 27.3 %all-to-all-start.2 = ((bf16[32,40,512]{2,1,0:T(8,128)(2,1)}), bf16[32,40,512]{2,1,0:T(8,128)(2,1)}, u32[]{:S(2)}, u32[]{:S(2)}) async-start(bf16[32,40,512]{2,1,0:T(8,128)(2,1)} %pad_maximum_fusion), calls=%async_computation.2 | async-start | bytes 2621440 | tf_op jit(solution)/shard_map/all_to_all | solution.py:666
  170.9 13.2 %collective-permute-start.11 = (bf16[512,512]{1,0:T(8,128)(2,1)S(1)}, bf16[512,512]{1,0:T(8,128)(2,1)S(1)}, u32[]{:S(2)}, u32[]{:S(2)}) collective-permute-start(bf16[512,512]{1,0:T(8,128)(2,1)S(1)} %fusion.a), channel_id=1, source_target_pairs={{0,1},{1,2},{2,3},{3,0},{4,5},{5,6},{6,7},{7,4},{8,9},{9,10},{10,1... | collective-permute-start | bytes 1572872 | tf_op jit(solution)/shard_map/ppermute | solution.py:306
  171.0 13.9 %collective-permute-start.12 = (bf16[512,512]{1,0:T(8,128)(2,1)S(1)}, bf16[512,512]{1,0:T(8,128)(2,1)S(1)}, u32[]{:S(2)}, u32[]{:S(2)}) collective-permute-start(bf16[512,512]{1,0:T(8,128)(2,1)S(1)} %fusion.a), channel_id=1, source_target_pairs={{0,3},{1,0},{2,1},{3,2},{4,7},{5,4},{6,5},{7,6},{8,11},{9,8},{10,9... | collective-permute-start | bytes 1572872 | tf_op jit(solution)/shard_map/ppermute | solution.py:306
  175.7 3.1 %collective-permute-start.15 = (f32[264,128]{1,0:T(8,128)S(1)}, f32[264,128]{1,0:T(8,128)S(1)}, u32[]{:S(2)}, u32[]{:S(2)}) collective-permute-start(f32[264,128]{1,0:T(8,128)S(1)} %get-tuple-element.93.refs_0_), channel_id=1, source_target_pairs={{0,4},{4,0},{1,5},{5,1},{2,6},{6,2},{3,7},{7,3},{8,12},{12,8},{9,1... | collective-permute-start | bytes 405512 | tf_op jit(solution)/shard_map/ppermute | solution.py:306
  179.5 8.9 %collective-permute-start.16 = (f32[264,128]{1,0:T(8,128)S(1)}, f32[264,128]{1,0:T(8,128)S(1)}, u32[]{:S(2)}, u32[]{:S(2)}) collective-permute-start(f32[264,128]{1,0:T(8,128)S(1)} %get-tuple-element.94.refs_0_), channel_id=1, source_target_pairs={{0,8},{8,16},{16,24},{24,0},{1,9},{9,17},{17,25},{25,1},{2,10},{10... | collective-permute-start | bytes 405512 | tf_op jit(solution)/shard_map/ppermute | solution.py:306
  179.5 8.9 %collective-permute-start.17 = (f32[264,128]{1,0:T(8,128)S(1)}, f32[264,128]{1,0:T(8,128)S(1)}, u32[]{:S(2)}, u32[]{:S(2)}) collective-permute-start(f32[264,128]{1,0:T(8,128)S(1)} %get-tuple-element.94.refs_0_), channel_id=1, source_target_pairs={{0,16},{8,24},{16,0},{24,8},{1,17},{9,25},{17,1},{25,9},{2,18},{10... | collective-permute-start | bytes 405512 | tf_op jit(solution)/shard_map/ppermute | solution.py:306
  181.1 7.7 %collective-permute-start.18 = (f32[264,128]{1,0:T(8,128)S(1)}, f32[264,128]{1,0:T(8,128)S(1)}, u32[]{:S(2)}, u32[]{:S(2)}) collective-permute-start(f32[264,128]{1,0:T(8,128)S(1)} %get-tuple-element.94.refs_0_), channel_id=1, source_target_pairs={{0,24},{8,0},{16,8},{24,16},{1,25},{9,1},{17,9},{25,17},{2,26},{10... | collective-permute-start | bytes 405512 | tf_op jit(solution)/shard_map/ppermute | solution.py:306
  184.8 19.2 %collective-permute-start.13 = (bf16[256,512]{1,0:T(8,128)(2,1)}, bf16[256,512]{1,0:T(8,128)(2,1)}, u32[]{:S(2)}, u32[]{:S(2)}) collective-permute-start(bf16[256,512]{1,0:T(8,128)(2,1)} %slice.44), channel_id=1, source_target_pairs={{0,1},{1,2},{2,3},{3,0},{4,5},{5,6},{6,7},{7,4},{8,9},{9,10},{10,1... | collective-permute-start | bytes 786440 | tf_op jit(solution)/shard_map/ppermute | solution.py:306
  185.6 19.5 %collective-permute-start.14 = (bf16[256,512]{1,0:T(8,128)(2,1)}, bf16[256,512]{1,0:T(8,128)(2,1)}, u32[]{:S(2)}, u32[]{:S(2)}) collective-permute-start(bf16[256,512]{1,0:T(8,128)(2,1)} %slice.45), channel_id=1, source_target_pairs={{0,3},{1,0},{2,1},{3,2},{4,7},{5,4},{6,5},{7,6},{8,11},{9,8},{10,9... | collective-permute-start | bytes 786440 | tf_op jit(solution)/shard_map/ppermute | solution.py:306
  189.6 5.4 %collective-permute-start.19 = (f32[264,128]{1,0:T(8,128)S(1)}, f32[264,128]{1,0:T(8,128)S(1)}, u32[]{:S(2)}, u32[]{:S(2)}) collective-permute-start(f32[264,128]{1,0:T(8,128)S(1)} %get-tuple-element.95.refs_0_), channel_id=1, source_target_pairs={{0,32},{32,64},{64,96},{96,0},{1,33},{33,65},{65,97},{97,1},{2,34}... | collective-permute-start | bytes 405512 | tf_op jit(solution)/shard_map/ppermute | solution.py:306
  191.7 7.1 %collective-permute-start.20 = (f32[264,128]{1,0:T(8,128)S(1)}, f32[264,128]{1,0:T(8,128)S(1)}, u32[]{:S(2)}, u32[]{:S(2)}) collective-permute-start(f32[264,128]{1,0:T(8,128)S(1)} %get-tuple-element.95.refs_0_), channel_id=1, source_target_pairs={{0,64},{32,96},{64,0},{96,32},{1,65},{33,97},{65,1},{97,33},{2,66}... | collective-permute-start | bytes 405512 | tf_op jit(solution)/shard_map/ppermute | solution.py:306
  192.9 5.9 %collective-permute-start.21 = (f32[264,128]{1,0:T(8,128)S(1)}, f32[264,128]{1,0:T(8,128)S(1)}, u32[]{:S(2)}, u32[]{:S(2)}) collective-permute-start(f32[264,128]{1,0:T(8,128)S(1)} %get-tuple-element.95.refs_0_), channel_id=1, source_target_pairs={{0,96},{32,0},{64,32},{96,64},{1,97},{33,1},{65,33},{97,65},{2,98}... | collective-permute-start | bytes 405512 | tf_op jit(solution)/shard_map/ppermute | solution.py:306
  207.8 55.2 %all-to-all-start.3 = ((bf16[32,64,256]{2,1,0:T(8,128)(2,1)}), bf16[32,64,256]{2,1,0:T(8,128)(2,1)}, u32[]{:S(2)}, u32[]{:S(2)}) async-start(bf16[32,64,256]{2,1,0:T(8,128)(2,1)} %bitcast.34), calls=%async_computation.3 | async-start | bytes 2097152 | tf_op jit(solution)/shard_map/all_to_all | solution.py:735
  220.5 11.6 %collective-permute-start.23 = (bf16[256,128]{1,0:T(8,128)(2,1)S(1)}, bf16[256,128]{1,0:T(8,128)(2,1)S(1)}, u32[]{:S(2)}, u32[]{:S(2)}) collective-permute-start(bf16[256,128]{1,0:T(8,128)(2,1)S(1)} %get-tuple-element.109.refs_0_), channel_id=1, source_target_pairs={{0,8},{8,16},{16,24},{24,0},{1,9},{9,17},{17,25},{25,1},{2,10},{10... | collective-permute-start | bytes 196616 | tf_op jit(solution)/shard_map/ppermute | solution.py:306
  221.9 11.6 %collective-permute-start.24 = (bf16[256,128]{1,0:T(8,128)(2,1)S(1)}, bf16[256,128]{1,0:T(8,128)(2,1)S(1)}, u32[]{:S(2)}, u32[]{:S(2)}) collective-permute-start(bf16[256,128]{1,0:T(8,128)(2,1)S(1)} %get-tuple-element.109.refs_0_), channel_id=1, source_target_pairs={{0,16},{8,24},{16,0},{24,8},{1,17},{9,25},{17,1},{25,9},{2,18},{10... | collective-permute-start | bytes 196616 | tf_op jit(solution)/shard_map/ppermute | solution.py:306
  224.3 9.2 %collective-permute-start.25 = (bf16[256,128]{1,0:T(8,128)(2,1)S(1)}, bf16[256,128]{1,0:T(8,128)(2,1)S(1)}, u32[]{:S(2)}, u32[]{:S(2)}) collective-permute-start(bf16[256,128]{1,0:T(8,128)(2,1)S(1)} %get-tuple-element.109.refs_0_), channel_id=1, source_target_pairs={{0,24},{8,0},{16,8},{24,16},{1,25},{9,1},{17,9},{25,17},{2,26},{10... | collective-permute-start | bytes 196616 | tf_op jit(solution)/shard_map/ppermute | solution.py:306
  233.6 26.5 %collective-permute-start.26 = (bf16[256,128]{1,0:T(8,128)(2,1)S(1)}, bf16[256,128]{1,0:T(8,128)(2,1)S(1)}, u32[]{:S(2)}, u32[]{:S(2)}) collective-permute-start(bf16[256,128]{1,0:T(8,128)(2,1)S(1)} %get-tuple-element.110.refs_0_), channel_id=1, source_target_pairs={{0,32},{32,64},{64,96},{96,0},{1,33},{33,65},{65,97},{97,1},{2,34}... | collective-permute-start | bytes 196616 | tf_op jit(solution)/shard_map/ppermute | solution.py:306
  234.8 25.3 %collective-permute-start.27 = (bf16[256,128]{1,0:T(8,128)(2,1)S(1)}, bf16[256,128]{1,0:T(8,128)(2,1)S(1)}, u32[]{:S(2)}, u32[]{:S(2)}) collective-permute-start(bf16[256,128]{1,0:T(8,128)(2,1)S(1)} %get-tuple-element.110.refs_0_), channel_id=1, source_target_pairs={{0,64},{32,96},{64,0},{96,32},{1,65},{33,97},{65,1},{97,33},{2,66}... | collective-permute-start | bytes 196616 | tf_op jit(solution)/shard_map/ppermute | solution.py:306
  237.3 22.9 %collective-permute-start.28 = (bf16[256,128]{1,0:T(8,128)(2,1)S(1)}, bf16[256,128]{1,0:T(8,128)(2,1)S(1)}, u32[]{:S(2)}, u32[]{:S(2)}) collective-permute-start(bf16[256,128]{1,0:T(8,128)(2,1)S(1)} %get-tuple-element.110.refs_0_), channel_id=1, source_target_pairs={{0,96},{32,0},{64,32},{96,64},{1,97},{33,1},{65,33},{97,65},{2,98}... | collective-permute-start | bytes 196616 | tf_op jit(solution)/shard_map/ppermute | solution.py:306
  (31 other events, 268.7 us)
